TPU v7x, 512 devices: a whole 4x4x16 slice. The times are simulated.
512 devices in a mesh: pp: 16 (over y, x), tp: 32 (over z, core).
Axes of the slice: x: 4, y: 4, z: 16, core: 2. Of those that a mesh axis runs over, the one named last changes fastest.
Arguments:
- entry_stream_rows: bfloat16 [1024, 2048], P('pp', 'tp'), may hold values from -21 to 21
- layer_rescale_factor: float32 [16, 2048], P('pp'), may hold values from 0.1 to 1.9
- probe_projection: bfloat16 [16, 2048, 2048], P('pp', 'tp'), may hold values from -0.125 to 0.125
- retention_projection: bfloat16 [16, 2048, 2048], P('pp', 'tp'), may hold values from -0.125 to 0.125
- candidate_projection: bfloat16 [16, 2048, 2048], P('pp', 'tp'), may hold values from -0.125 to 0.125
- emission_filter_matrix: bfloat16 [16, 2048, 2048], P('pp', 'tp'), may hold values from -0.125 to 0.125
- retention_minimum: float32 [16, 2048], P('pp', 'tp'), may hold values from 0.88 to 0.9921875
- decay_spike: float32 [16, 128, 32], P('pp', None, 'tp'), may hold values from -2.1 to 0
- per_group_scale: float32 [16, 64], P('pp'), may hold values from 0.1 to 1.9
Outputs:
- outputs: bfloat16 [1024, 2048], P('pp', 'tp')
All inputs are finite; a program needn't handle non-finite values.
Results may differ from a plain program's by a relative error of at most 0.03.
Values may be sent and summed in bfloat16 or wider, within the bound.
No kernel may reach another device: no remote copies, remote signals or barrier semaphores. Data moves between devices by JAX's collectives and lax.ppermute only.
A program may use at most 64 MiB of HBM per device.

v0:
```python
import jax
import jax.numpy as jnp
from jax import lax
from jax.sharding import PartitionSpec as P

HEAD = 64
SEG = 64


EPSILON = 1e-06


def shifted(array, axis, by):
    devices = lax.axis_size(axis)
    pairs = [(i, i + by) for i in range(devices) if 0 <= i + by < devices]
    return lax.ppermute(array, axis, pairs)


def from_root(array, axis, root):
    return lax.dynamic_index_in_dim(lax.all_gather(array, axis), root, 0, keepdims=False)


def segment_scan(queries, key_in, log_forget, values, memory):
    head_count = queries.shape[0]
    length = queries.shape[1]
    blocks_count = length // SEG

    def split_blocks(tensor):
        return tensor.reshape(head_count, blocks_count, SEG, tensor.shape[-1]).transpose(1, 0, 2, 3)

    lower_mask = jnp.tril(jnp.ones((SEG, SEG), dtype=bool))[None]

    def one_block(memory_in, pieces):
        block_query, block_key, block_forget, block_value = pieces
        running = jnp.cumsum(block_forget, axis=1)
        query_scaled = block_query * jnp.exp(running)
        key_scaled = block_key * jnp.exp(-running)
        scores = jnp.einsum("hid,hjd->hij", query_scaled, key_scaled)
        scores = jnp.where(lower_mask, scores, 0.0)
        mixed_out = jnp.einsum("hij,hjv->hiv", scores, block_value)
        mixed_out = mixed_out + jnp.einsum("hid,hdv->hiv", query_scaled, memory_in)
        ending = running[:, -1:, :]
        carried_in = jnp.einsum("hjd,hjv->hdv", block_key * jnp.exp(ending - running), block_value)
        memory_out = jnp.exp(ending[:, 0, :])[:, :, None] * memory_in + carried_in
        return (memory_out, mixed_out)

    memory, mixed_out = lax.scan(
        one_block,
        memory,
        (
            split_blocks(queries),
            split_blocks(key_in),
            split_blocks(log_forget),
            split_blocks(values),
        ),
    )
    return (mixed_out.transpose(1, 0, 2, 3).reshape(head_count, length, values.shape[-1]), memory)


def head_norm(mixed_out, channel_gain):
    return (
        mixed_out
        * lax.rsqrt(jnp.mean(mixed_out * mixed_out, axis=-1, keepdims=True) + EPSILON)
        * channel_gain
    )


def shards(
    entry_stream_rows,
    layer_rescale_factor,
    probe_projection,
    retention_projection,
    candidate_projection,
    emission_filter_matrix,
    retention_minimum,
    decay_spike,
    per_group_scale,
):
    sections = lax.axis_size("pp")
    layer_ordinal = lax.axis_index("pp")
    own_rows = entry_stream_rows.shape[0]
    seq_len = 2 * own_rows
    columns = entry_stream_rows.shape[1]
    head_here = columns // HEAD
    model_width = layer_rescale_factor.shape[1]
    micro_count = sections // 2
    per_sequence = seq_len // seq_len
    unit_count = micro_count * per_sequence
    total_steps = unit_count + sections - 1
    entering = lax.all_gather(entry_stream_rows, "pp", axis=0, tiled=True)
    weights = jnp.concatenate(
        [
            probe_projection[0],
            retention_projection[0],
            candidate_projection[0],
            emission_filter_matrix[0],
        ],
        axis=0,
    )
    input_gain = layer_rescale_factor[0]
    lower_edge = retention_minimum[0].reshape(head_here, 1, HEAD)
    spike_collection = decay_spike[0].T
    out_gain = per_group_scale[0]

    def add_piece(piece_in):
        wide_piece = piece_in.astype(jnp.float32)
        scaled = (wide_piece * input_gain[None, :]).astype(jnp.bfloat16)
        product = lax.dot_general(
            scaled, weights, (((1,), (1,)), ((), ())), preferred_element_type=jnp.float32
        )
        return (product, jnp.sum(wide_piece * wide_piece, axis=1))

    def one_step(step_index, carried):
        incoming, memory, finished = carried
        unit_index = step_index - layer_ordinal
        first_slot = jnp.clip(step_index, 0, unit_count - 1)
        fresh_rows = lax.dynamic_slice_in_dim(entering, first_slot * seq_len, seq_len, 0)
        current = jnp.where(layer_ordinal == 0, fresh_rows, incoming)
        projected, squares = add_piece(lax.all_gather(current, "tp", axis=1, tiled=True))
        inverse = lax.rsqrt(squares / model_width + EPSILON)[:, None]
        projected = projected * inverse

        def per_head(role_index):
            picked = projected[:, role_index * columns : (role_index + 1) * columns]
            return picked.reshape(seq_len, head_here, HEAD).transpose(1, 0, 2)

        query_pre = per_head(0)
        forget_pre = per_head(1)
        input_pre = per_head(2)
        gate_pre = per_head(3)
        offset = unit_index % per_sequence * seq_len
        current_surge = spike_collection[:, :, None]
        log_forget = (
            jnp.logaddexp(
                jnp.log(lower_edge), jnp.log1p(-lower_edge) + jax.nn.log_sigmoid(forget_pre)
            )
            + current_surge
        )
        key_in = (1.0 - lower_edge) * jax.nn.sigmoid(-forget_pre)
        queries = jax.nn.silu(query_pre)
        memory = jnp.where(offset == 0, jnp.zeros_like(memory), memory)
        mixed_out, memory = segment_scan(queries, key_in, log_forget, input_pre, memory)
        branch = head_norm(mixed_out, out_gain) * jax.nn.silu(gate_pre)
        branch = branch.transpose(1, 0, 2).reshape(seq_len, columns)
        result = (current.astype(jnp.float32) + branch).astype(jnp.bfloat16)
        passed = shifted(result, "pp", 1)
        out_slot = jnp.clip(unit_index, 0, unit_count - 1)
        write_here = (layer_ordinal == sections - 1) & (unit_index >= 0) & (unit_index < unit_count)
        updated = lax.dynamic_update_slice_in_dim(finished, result, out_slot * seq_len, 0)
        finished = jnp.where(write_here, updated, finished)
        return (passed, memory, finished)

    start_state = (
        jnp.zeros((seq_len, columns), jnp.bfloat16),
        jnp.zeros((head_here, HEAD, HEAD), jnp.float32),
        jnp.zeros((unit_count * seq_len, columns), jnp.bfloat16),
    )
    carried_out = lax.fori_loop(0, total_steps, one_step, start_state)
    everything = from_root(carried_out[2], "pp", sections - 1)
    return lax.dynamic_slice_in_dim(everything, layer_ordinal * own_rows, own_rows, 0)


def solution(mesh):
    in_specs = (
        P("pp", "tp"),
        P("pp", None),
        P("pp", "tp", None),
        P("pp", "tp", None),
        P("pp", "tp", None),
        P("pp", "tp", None),
        P("pp", "tp"),
        P("pp", None, "tp"),
        P("pp", None),
    )
    out_specs = P("pp", "tp")
    return jax.shard_map(shards, mesh=mesh, in_specs=in_specs, out_specs=out_specs, check_vma=False)
```

profile of v0, /device:TPU:1, one launch (start us, length us, event | category | flops | bytes accessed | tf_op | source)
XLA Modules:
  0.0 1040.1 jit_solution(864880211558230233)
XLA Ops:
  7.3 19.7 %all_gather.20 = bf16[1024,64]{1,0:T(8,128)(2,1)S(1)} all-gather(bf16[64,64]{1,0:T(8,128)(2,1)} %param.13), channel_id=1, replica_groups=mesh['pp'=16,'tp'=32] {'pp'}, dimensions={0}, use_global_device_ids=true | all-gather | bytes 139264 | tf_op jit(solution)/shard_map/all_gather | solution.py:90
  28.3 930.2 %while.59 = (s32[]{:T(128)}, bf16[128,64]{1,0:T(8,128)(2,1)S(1)}, bf16[1024,64]{1,0:T(8,128)(2,1)S(1)}, pred[]{:T(512)}, bf16[1024,64]{1,0:T(8,128)(2,1)S(1)}, /...) while((s32[]{:T(128)}, bf16[128,64]{1,0:T(8,128)(2,1)S(1)}, ...), condition=%wide.region_6.7_spmd, body=%wide.region_0.6_spmd.sunk | while | flops 138551632 | bytes 3955077 | solution.py:158
  28.5 43.4 %all_gather.24 = bf16[128,2048]{0,1:T(8,128)(2,1)S(1)} all-gather(bf16[128,64]{0,1:T(8,128)(2,1)S(1)} %copy.20), channel_id=1, replica_groups=mesh['pp'=16,'tp'=32] {'tp'}, dimensions={1}, use_global_device_ids=true | all-gather | bytes 540672 | tf_op jit(solution)/shard_map/while/body/eval_jaxpr/all_gather | solution.py:119
  79.0 29.1 %all_gather.24 = bf16[128,2048]{0,1:T(8,128)(2,1)S(1)} all-gather(bf16[128,64]{0,1:T(8,128)(2,1)S(1)} %copy.20), channel_id=1, replica_groups=mesh['pp'=16,'tp'=32] {'tp'}, dimensions={1}, use_global_device_ids=true | all-gather | bytes 540672 | tf_op jit(solution)/shard_map/while/body/eval_jaxpr/all_gather | solution.py:119
  111.2 3.9 collective-permute-start
  116.3 31.0 %all_gather.24 = bf16[128,2048]{0,1:T(8,128)(2,1)S(1)} all-gather(bf16[128,64]{0,1:T(8,128)(2,1)S(1)} %copy.20), channel_id=1, replica_groups=mesh['pp'=16,'tp'=32] {'tp'}, dimensions={1}, use_global_device_ids=true | all-gather | bytes 540672 | tf_op jit(solution)/shard_map/while/body/eval_jaxpr/all_gather | solution.py:119
  150.5 3.9 collective-permute-start
  155.6 29.1 %all_gather.24 = bf16[128,2048]{0,1:T(8,128)(2,1)S(1)} all-gather(bf16[128,64]{0,1:T(8,128)(2,1)S(1)} %copy.20), channel_id=1, replica_groups=mesh['pp'=16,'tp'=32] {'tp'}, dimensions={1}, use_global_device_ids=true | all-gather | bytes 540672 | tf_op jit(solution)/shard_map/while/body/eval_jaxpr/all_gather | solution.py:119
  187.8 3.9 collective-permute-start
  192.9 31.0 %all_gather.24 = bf16[128,2048]{0,1:T(8,128)(2,1)S(1)} all-gather(bf16[128,64]{0,1:T(8,128)(2,1)S(1)} %copy.20), channel_id=1, replica_groups=mesh['pp'=16,'tp'=32] {'tp'}, dimensions={1}, use_global_device_ids=true | all-gather | bytes 540672 | tf_op jit(solution)/shard_map/while/body/eval_jaxpr/all_gather | solution.py:119
  227.1 3.9 collective-permute-start
  232.2 29.1 %all_gather.24 = bf16[128,2048]{0,1:T(8,128)(2,1)S(1)} all-gather(bf16[128,64]{0,1:T(8,128)(2,1)S(1)} %copy.20), channel_id=1, replica_groups=mesh['pp'=16,'tp'=32] {'tp'}, dimensions={1}, use_global_device_ids=true | all-gather | bytes 540672 | tf_op jit(solution)/shard_map/while/body/eval_jaxpr/all_gather | solution.py:119
  264.4 5.3 collective-permute-start
  270.9 31.0 %all_gather.24 = bf16[128,2048]{0,1:T(8,128)(2,1)S(1)} all-gather(bf16[128,64]{0,1:T(8,128)(2,1)S(1)} %copy.20), channel_id=1, replica_groups=mesh['pp'=16,'tp'=32] {'tp'}, dimensions={1}, use_global_device_ids=true | all-gather | bytes 540672 | tf_op jit(solution)/shard_map/while/body/eval_jaxpr/all_gather | solution.py:119
  305.0 6.1 collective-permute-start
  312.2 29.1 %all_gather.24 = bf16[128,2048]{0,1:T(8,128)(2,1)S(1)} all-gather(bf16[128,64]{0,1:T(8,128)(2,1)S(1)} %copy.20), channel_id=1, replica_groups=mesh['pp'=16,'tp'=32] {'tp'}, dimensions={1}, use_global_device_ids=true | all-gather | bytes 540672 | tf_op jit(solution)/shard_map/while/body/eval_jaxpr/all_gather | solution.py:119
  344.5 6.0 collective-permute-start
  351.7 31.0 %all_gather.24 = bf16[128,2048]{0,1:T(8,128)(2,1)S(1)} all-gather(bf16[128,64]{0,1:T(8,128)(2,1)S(1)} %copy.20), channel_id=1, replica_groups=mesh['pp'=16,'tp'=32] {'tp'}, dimensions={1}, use_global_device_ids=true | all-gather | bytes 540672 | tf_op jit(solution)/shard_map/while/body/eval_jaxpr/all_gather | solution.py:119
  385.8 6.1 collective-permute-start
  393.0 29.1 %all_gather.24 = bf16[128,2048]{0,1:T(8,128)(2,1)S(1)} all-gather(bf16[128,64]{0,1:T(8,128)(2,1)S(1)} %copy.20), channel_id=1, replica_groups=mesh['pp'=16,'tp'=32] {'tp'}, dimensions={1}, use_global_device_ids=true | all-gather | bytes 540672 | tf_op jit(solution)/shard_map/while/body/eval_jaxpr/all_gather | solution.py:119
  425.3 6.1 collective-permute-start
  432.5 31.0 %all_gather.24 = bf16[128,2048]{0,1:T(8,128)(2,1)S(1)} all-gather(bf16[128,64]{0,1:T(8,128)(2,1)S(1)} %copy.20), channel_id=1, replica_groups=mesh['pp'=16,'tp'=32] {'tp'}, dimensions={1}, use_global_device_ids=true | all-gather | bytes 540672 | tf_op jit(solution)/shard_map/while/body/eval_jaxpr/all_gather | solution.py:119
  466.7 6.0 collective-permute-start
  473.8 29.1 %all_gather.24 = bf16[128,2048]{0,1:T(8,128)(2,1)S(1)} all-gather(bf16[128,64]{0,1:T(8,128)(2,1)S(1)} %copy.20), channel_id=1, replica_groups=mesh['pp'=16,'tp'=32] {'tp'}, dimensions={1}, use_global_device_ids=true | all-gather | bytes 540672 | tf_op jit(solution)/shard_map/while/body/eval_jaxpr/all_gather | solution.py:119
  506.1 6.1 collective-permute-start
  513.3 31.0 %all_gather.24 = bf16[128,2048]{0,1:T(8,128)(2,1)S(1)} all-gather(bf16[128,64]{0,1:T(8,128)(2,1)S(1)} %copy.20), channel_id=1, replica_groups=mesh['pp'=16,'tp'=32] {'tp'}, dimensions={1}, use_global_device_ids=true | all-gather | bytes 540672 | tf_op jit(solution)/shard_map/while/body/eval_jaxpr/all_gather | solution.py:119
  547.5 6.1 collective-permute-start
  554.6 29.1 %all_gather.24 = bf16[128,2048]{0,1:T(8,128)(2,1)S(1)} all-gather(bf16[128,64]{0,1:T(8,128)(2,1)S(1)} %copy.20), channel_id=1, replica_groups=mesh['pp'=16,'tp'=32] {'tp'}, dimensions={1}, use_global_device_ids=true | all-gather | bytes 540672 | tf_op jit(solution)/shard_map/while/body/eval_jaxpr/all_gather | solution.py:119
  586.9 6.0 collective-permute-start
  594.1 31.0 %all_gather.24 = bf16[128,2048]{0,1:T(8,128)(2,1)S(1)} all-gather(bf16[128,64]{0,1:T(8,128)(2,1)S(1)} %copy.20), channel_id=1, replica_groups=mesh['pp'=16,'tp'=32] {'tp'}, dimensions={1}, use_global_device_ids=true | all-gather | bytes 540672 | tf_op jit(solution)/shard_map/while/body/eval_jaxpr/all_gather | solution.py:119
  628.3 6.1 collective-permute-start
  635.4 29.1 %all_gather.24 = bf16[128,2048]{0,1:T(8,128)(2,1)S(1)} all-gather(bf16[128,64]{0,1:T(8,128)(2,1)S(1)} %copy.20), channel_id=1, replica_groups=mesh['pp'=16,'tp'=32] {'tp'}, dimensions={1}, use_global_device_ids=true | all-gather | bytes 540672 | tf_op jit(solution)/shard_map/while/body/eval_jaxpr/all_gather | solution.py:119
  667.7 6.1 collective-permute-start
  674.9 31.0 %all_gather.24 = bf16[128,2048]{0,1:T(8,128)(2,1)S(1)} all-gather(bf16[128,64]{0,1:T(8,128)(2,1)S(1)} %copy.20), channel_id=1, replica_groups=mesh['pp'=16,'tp'=32] {'tp'}, dimensions={1}, use_global_device_ids=true | all-gather | bytes 540672 | tf_op jit(solution)/shard_map/while/body/eval_jaxpr/all_gather | solution.py:119
  709.1 6.0 collective-permute-start
  716.2 29.1 %all_gather.24 = bf16[128,2048]{0,1:T(8,128)(2,1)S(1)} all-gather(bf16[128,64]{0,1:T(8,128)(2,1)S(1)} %copy.20), channel_id=1, replica_groups=mesh['pp'=16,'tp'=32] {'tp'}, dimensions={1}, use_global_device_ids=true | all-gather | bytes 540672 | tf_op jit(solution)/shard_map/while/body/eval_jaxpr/all_gather | solution.py:119
  748.5 6.1 collective-permute-start
  755.7 31.0 %all_gather.24 = bf16[128,2048]{0,1:T(8,128)(2,1)S(1)} all-gather(bf16[128,64]{0,1:T(8,128)(2,1)S(1)} %copy.20), channel_id=1, replica_groups=mesh['pp'=16,'tp'=32] {'tp'}, dimensions={1}, use_global_device_ids=true | all-gather | bytes 540672 | tf_op jit(solution)/shard_map/while/body/eval_jaxpr/all_gather | solution.py:119
  789.9 6.1 collective-permute-start
  797.0 29.1 %all_gather.24 = bf16[128,2048]{0,1:T(8,128)(2,1)S(1)} all-gather(bf16[128,64]{0,1:T(8,128)(2,1)S(1)} %copy.20), channel_id=1, replica_groups=mesh['pp'=16,'tp'=32] {'tp'}, dimensions={1}, use_global_device_ids=true | all-gather | bytes 540672 | tf_op jit(solution)/shard_map/while/body/eval_jaxpr/all_gather | solution.py:119
  829.3 6.0 collective-permute-start
  836.5 31.0 %all_gather.24 = bf16[128,2048]{0,1:T(8,128)(2,1)S(1)} all-gather(bf16[128,64]{0,1:T(8,128)(2,1)S(1)} %copy.20), channel_id=1, replica_groups=mesh['pp'=16,'tp'=32] {'tp'}, dimensions={1}, use_global_device_ids=true | all-gather | bytes 540672 | tf_op jit(solution)/shard_map/while/body/eval_jaxpr/all_gather | solution.py:119
  870.7 6.1 collective-permute-start
  877.8 29.1 %all_gather.24 = bf16[128,2048]{0,1:T(8,128)(2,1)S(1)} all-gather(bf16[128,64]{0,1:T(8,128)(2,1)S(1)} %copy.20), channel_id=1, replica_groups=mesh['pp'=16,'tp'=32] {'tp'}, dimensions={1}, use_global_device_ids=true | all-gather | bytes 540672 | tf_op jit(solution)/shard_map/while/body/eval_jaxpr/all_gather | solution.py:119
  910.1 6.1 collective-permute-start
  917.3 31.0 %all_gather.24 = bf16[128,2048]{0,1:T(8,128)(2,1)S(1)} all-gather(bf16[128,64]{0,1:T(8,128)(2,1)S(1)} %copy.20), channel_id=1, replica_groups=mesh['pp'=16,'tp'=32] {'tp'}, dimensions={1}, use_global_device_ids=true | all-gather | bytes 540672 | tf_op jit(solution)/shard_map/while/body/eval_jaxpr/all_gather | solution.py:119
  951.5 6.0 collective-permute-start
  959.3 72.4 %all-gather.3.cloned.1.call-done = bf16[16384,64]{1,0:T(8,128)(2,1)} async-done(((bf16[1024,64]{1,0:T(8,128)(2,1)}), bf16[16384,64]{1,0:T(8,128)(2,1)}) %all-gather.3.cloned.1.call-update) | async-done | bytes 2097168 | tf_op jit(solution)/shard_map/all_gather | solution.py:20
  (709 shorter events, 136.6 us)
Async XLA Ops:
  6.5 21.7 %copy-start.4 = (f32[1,64]{1,0:T(1,128)S(1)}, f32[1,64]{1,0:T(1,128)}, u32[]{:S(2)}) copy-start(f32[1,64]{1,0:T(1,128)} %param.19) | copy-start | bytes 772
  6.5 21.7 %copy-start.3 = (f32[1,64]{1,0:T(1,128)S(1)}, f32[1,64]{1,0:T(1,128)}, u32[]{:S(2)}) copy-start(f32[1,64]{1,0:T(1,128)} %param.21) | copy-start | bytes 772
  6.5 21.7 %copy-start.2 = (f32[1,128,1]{1,2,0:T(1,128)S(1)}, f32[1,128,1]{1,2,0:T(1,128)}, u32[]{:S(2)}) copy-start(f32[1,128,1]{1,2,0:T(1,128)} %param.20) | copy-start | bytes 1540
  6.5 21.7 %copy-start.1 = (f32[1,2048]{1,0:T(1,128)S(1)}, f32[1,2048]{1,0:T(1,128)}, u32[]{:S(2)}) copy-start(f32[1,2048]{1,0:T(1,128)} %param.14) | copy-start | bytes 24580
  6.5 1025.1 %all-gather.3.cloned.1.call-start = ((), (), s32[]{:S(2)}) async-start(), calls=%async_computation | async-start | bytes 4456448 | tf_op jit(solution)/shard_map/all_gather | solution.py:20
  75.0 3.8 collective-permute-start
  111.2 5.0 collective-permute-start
  150.5 5.0 collective-permute-start
  187.8 5.0 collective-permute-start
  227.1 5.0 collective-permute-start
  264.4 6.3 collective-permute-start
  305.0 7.1 collective-permute-start
  344.5 7.1 collective-permute-start
  385.8 7.1 collective-permute-start
  425.3 7.1 collective-permute-start
  466.7 7.1 collective-permute-start
  506.1 7.1 collective-permute-start
  547.5 7.1 collective-permute-start
  586.9 7.1 collective-permute-start
  628.3 7.1 collective-permute-start
  667.7 7.1 collective-permute-start
  709.1 7.1 collective-permute-start
  748.5 7.1 collective-permute-start
  789.9 7.1 collective-permute-start
  829.3 7.1 collective-permute-start
  870.7 7.1 collective-permute-start
  910.1 7.1 collective-permute-start
  951.5 7.1 collective-permute-start
  958.5 0.7 copy-start
Sparse Core Ops, SparseCore 0:
  959.4 72.2 all-gather.2
where the time goes:
time: 1040 us
  blocking collectives  724 us (70%)
  starting transfers between devices  127 us (12%)
  waiting for transfers between devices  95.4 us (9%)
  matrix products  47.4 us (5%)
  other arithmetic  23.2 us (2%)
  between operations  13.5 us (1%)
    all_gather x23, blocking collectives, one_step(): lax.all_gather(current, 'tp', axis=1, tiled=True)  704 us
    ppermute x23, starting transfers between devices, shifted(): return lax.ppermute(array, axis, pairs)  127 us
    all_gather x1, waiting for transfers between devices, from_root(): lax.all_gather(array, axis)  72.4 us
    ppermute x23, waiting for transfers between devices, shifted(): return lax.ppermute(array, axis, pairs)  23 us
  transfers between devices with their start and end apart: 24, of which 24 were waited for; matrix products, arithmetic and copies ran while one was open for 0% of the time, Pallas kernels for 0%

commit v1 on v0

v1 whole, which is shorter than its diff:
```python
import jax
import jax.numpy as jnp
from jax import lax
from jax.experimental import pallas as pl
from jax.experimental.pallas import tpu as pltpu
from jax.sharding import PartitionSpec as P

HEAD = 64
SEG = 64
EPSILON = 1e-06
NT = (((1,), (1,)), ((), ()))
NN = (((1,), (0,)), ((), ()))
TN = (((0,), (0,)), ((), ()))


def section_kernel(flags, got, gain, weights, edge, spike, out_gain, state_in, result, state_out, scaled, inverse):
    pair = pl.program_id(0)
    first, base, core = flags[0], flags[2], flags[3]
    width = got.shape[-1]
    rows = got.shape[1]

    @pl.when(pair == 0)
    def _():
        total = jnp.zeros((rows, 1), jnp.float32)
        for part in range(2):
            wide = got[base + part].astype(jnp.float32)
            columns = pl.ds(part * width, width)
            scaled[:, columns] = (wide * gain[:, columns]).astype(jnp.bfloat16)
            total = total + jnp.sum(wide * wide, axis=1, keepdims=True)
        inverse[...] = jnp.broadcast_to(lax.rsqrt(total / (2 * width) + EPSILON), inverse.shape)

    matrix = weights[...].reshape(8 * HEAD, 2 * width)
    product = lax.dot_general(scaled[...], matrix, NT, preferred_element_type=jnp.float32)
    scale = inverse[...]
    tiles = [product[:, 128 * k : 128 * k + 128] * scale for k in range(4)]
    rolled = [pltpu.roll(tile, HEAD, 1) for tile in tiles]
    low = lax.broadcasted_iota(jnp.int32, (rows, 128), 1) < HEAD
    query_pre = jnp.where(low, tiles[0], rolled[2])
    forget_pre = jnp.where(low, rolled[0], tiles[2])
    values = jnp.where(low, tiles[1], rolled[3]).astype(jnp.bfloat16)
    gate_pre = jnp.where(low, rolled[1], tiles[3])

    lower = edge[0]
    upper = 1.0 - lower
    log_forget = jnp.log(lower + upper * jax.nn.sigmoid(forget_pre)) + spike[0, 0]
    key_in = upper * jax.nn.sigmoid(-forget_pre)
    queries = query_pre * jax.nn.sigmoid(query_pre)

    high = log_forget.astype(jnp.bfloat16)
    rest = (log_forget - high.astype(jnp.float32)).astype(jnp.bfloat16)
    at = lax.broadcasted_iota(jnp.int32, (rows, 2 * rows), 0)
    of = lax.broadcasted_iota(jnp.int32, (rows, 2 * rows), 1)
    of = jnp.where(of >= rows, of - rows, of)
    ones = jnp.where(at >= of, 1.0, 0.0).astype(jnp.bfloat16)
    running = lax.dot_general(ones, jnp.concatenate([high, rest], axis=0), NN, preferred_element_type=jnp.float32)

    query_scaled = queries * jnp.exp(running)
    key_scaled = (key_in * jnp.exp(-running)).astype(jnp.bfloat16)
    stacked = jnp.concatenate(
        [jnp.where(low, query_scaled, 0.0), jnp.where(low, 0.0, query_scaled)], axis=0
    ).astype(jnp.bfloat16)
    scores = lax.dot_general(stacked, key_scaled, NT, preferred_element_type=jnp.float32)
    at = lax.broadcasted_iota(jnp.int32, (2 * rows, rows), 0)
    at = jnp.where(at >= rows, at - rows, at)
    of = lax.broadcasted_iota(jnp.int32, (2 * rows, rows), 1)
    scores = jnp.where(at >= of, scores, 0.0).astype(jnp.bfloat16)
    both = lax.dot_general(scores, values, NN, preferred_element_type=jnp.float32)
    mixed = jnp.where(low, both[:rows], both[rows:])
    state = jnp.where(first == 1, 0.0, state_in[0])
    mixed = mixed + lax.dot_general(
        query_scaled.astype(jnp.bfloat16), state.astype(jnp.bfloat16), NN, preferred_element_type=jnp.float32
    )

    at = lax.broadcasted_iota(jnp.int32, (128, 128), 0) < HEAD
    of = lax.broadcasted_iota(jnp.int32, (128, 128), 1) < HEAD
    same = at == of

    @pl.when(first == 1)
    def _():
        ending = running[rows - 1 :, :]
        kept = (key_in * jnp.exp(ending - running)).astype(jnp.bfloat16)
        carried = lax.dot_general(kept, values, TN, preferred_element_type=jnp.float32)
        state_out[0] = jnp.where(same, carried, 0.0)

    @pl.when(first != 1)
    def _():
        state_out[0] = state_in[0]

    mean = jnp.where(same, 1.0 / HEAD, 0.0).astype(jnp.bfloat16)
    square = mixed * mixed
    high = square.astype(jnp.bfloat16)
    rest = (square - high.astype(jnp.float32)).astype(jnp.bfloat16)
    average = lax.dot_general(high, mean, NN, preferred_element_type=jnp.float32) + lax.dot_general(
        rest, mean, NN, preferred_element_type=jnp.float32
    )
    branch = mixed * lax.rsqrt(average + EPSILON) * out_gain[...] * (gate_pre * jax.nn.sigmoid(gate_pre))
    own = got[base + core, :, pl.ds(pl.multiple_of(pair * 128, 128), 128)].astype(jnp.float32)
    result[...] = (own + branch).astype(jnp.bfloat16)


def section(flags, got, gain, weights, edge, spike, out_gain, state):
    rows, width = got.shape[1:]
    pairs = weights.shape[0] // 2
    return pl.pallas_call(
        section_kernel,
        out_shape=(
            jax.ShapeDtypeStruct((rows, width), jnp.bfloat16),
            jax.ShapeDtypeStruct(state.shape, state.dtype),
        ),
        grid_spec=pltpu.PrefetchScalarGridSpec(
            num_scalar_prefetch=1,
            grid=(pairs,),
            in_specs=[
                pl.BlockSpec(got.shape, lambda g, f: (0, 0, 0)),
                pl.BlockSpec(gain.shape, lambda g, f: (0, 0)),
                pl.BlockSpec((2,) + weights.shape[1:], lambda g, f: (g, 0, 0, 0)),
                pl.BlockSpec((1, 1, 128), lambda g, f: (g, 0, 0)),
                pl.BlockSpec((1, 1, rows, 128), lambda g, f: (f[1], g, 0, 0)),
                pl.BlockSpec((1, 128), lambda g, f: (0, 0)),
                pl.BlockSpec((1, 128, 128), lambda g, f: (g, 0, 0)),
            ],
            out_specs=[
                pl.BlockSpec((rows, 128), lambda g, f: (0, g)),
                pl.BlockSpec((1, 128, 128), lambda g, f: (g, 0, 0)),
            ],
            scratch_shapes=[
                pltpu.VMEM((rows, 2 * width), jnp.bfloat16),
                pltpu.VMEM((rows, 128), jnp.float32),
            ],
        ),
        input_output_aliases={7: 1},
        cost_estimate=pl.CostEstimate(
            flops=2 * rows * weights.size, bytes_accessed=2 * weights.size, transcendentals=0
        ),
    )(flags, got, gain, weights, edge, spike, out_gain, state)


def shards(
    entry_stream_rows,
    layer_rescale_factor,
    probe_projection,
    retention_projection,
    candidate_projection,
    emission_filter_matrix,
    retention_minimum,
    decay_spike,
    per_group_scale,
):
    sections = lax.axis_size("pp")
    members = lax.axis_size("tp")
    chips = members // 2
    layer = lax.axis_index("pp")
    core = lax.axis_index("tp") % 2
    chip = lax.axis_index("tp") // 2
    model_width = layer_rescale_factor.shape[1]
    half_width = model_width // 2
    pairs = chips // 2
    same_core = [[c + 2 * z for z in range(chips)] for c in range(2)]

    def by_core(array):
        split = array.reshape(array.shape[:-1] + (chips, 2, HEAD))
        return jnp.swapaxes(split, -3, -2).reshape(array.shape)

    local = jnp.stack(
        [probe_projection[0], retention_projection[0], candidate_projection[0], emission_filter_matrix[0]]
    )
    weights = lax.all_gather(by_core(local), "tp", axis_index_groups=same_core)
    gain = by_core(layer_rescale_factor)
    small = jnp.concatenate([retention_minimum[0], decay_spike[0, :, 0]])
    small = lax.all_gather(small, "tp", axis_index_groups=same_core)
    edge = small[:, :HEAD].reshape(pairs, 1, 128)
    spike = small[:, HEAD:].reshape(pairs, 2, 2, SEG)
    spike = jnp.broadcast_to(spike.transpose(2, 0, 3, 1)[..., None], (2, pairs, SEG, 2, HEAD))
    spike = spike.reshape(2, pairs, SEG, 128)
    out_gain = jnp.tile(per_group_scale, (1, 2))

    def gathered_line(block):
        whole = lax.all_gather(block, "tp", axis_index_groups=same_core)
        return whole.transpose(1, 0, 2).reshape(block.shape[0], half_width)

    def between(array, pairs_of):
        moves = [
            (a * members + t, b * members + t)
            for a, b, z in pairs_of
            for t in (2 * z, 2 * z + 1)
        ]
        return lax.ppermute(array, ("pp", "tp"), moves)

    micro = sections // 2
    entering = gathered_line(entry_stream_rows)
    entry = [between(entering, [(2 * k + u, 0, 2 * k) for k in range(micro)]) for u in range(2)]

    def groups(odd):
        lines = [((2 * i + 1) % sections, (2 * i + 2) % sections) if odd else (2 * i, 2 * i + 1) for i in range(micro)]
        return [
            [a * members + 2 * z, a * members + 2 * z + 1, b * members + 2 * z, b * members + 2 * z + 1]
            for a, b in lines
            for z in range(chips)
        ]

    def slot(index, odd, current, state):
        got = lax.all_gather(current, ("pp", "tp"), axis_index_groups=groups(odd))
        first = (index == layer).astype(jnp.int32)
        base = jnp.where(layer == 0, 2, 0) if odd else jnp.zeros((), jnp.int32)
        flags = jnp.stack([first, 1 - first, base.astype(jnp.int32), core.astype(jnp.int32)])
        return section(flags, got, gain, weights, edge, spike, out_gain, state)

    def two_slots(turn, carried):
        current, state = carried
        fresh = jnp.where(turn == 0, entry[0], entry[1])
        current = jnp.where(layer == 0, fresh, current)
        current, state = slot(2 * turn, True, current, state)
        return slot(2 * turn + 1, False, current, state)

    start = (jnp.zeros((SEG, half_width), jnp.bfloat16), jnp.zeros((pairs, 128, 128), jnp.float32))
    carried = lax.fori_loop(0, micro, two_slots, start)
    last = sections - 1
    finished = [between(carried[0], [(last, 2 * k, 2 * k) for k in range(micro)])]
    carried = two_slots(micro, carried)
    finished.append(between(carried[0], [(last, 2 * k + 1, 2 * k) for k in range(micro)]))
    mine = jnp.where(layer % 2 == 0, finished[0], finished[1])
    spread = mine.reshape(SEG, chips, HEAD).transpose(1, 0, 2)
    received = lax.all_to_all(spread, "tp", 0, 0, axis_index_groups=same_core)
    return lax.dynamic_index_in_dim(received, layer // 2 * 2, 0, keepdims=False)


def solution(mesh):
    in_specs = (
        P("pp", "tp"),
        P("pp", None),
        P("pp", "tp", None),
        P("pp", "tp", None),
        P("pp", "tp", None),
        P("pp", "tp", None),
        P("pp", "tp"),
        P("pp", None, "tp"),
        P("pp", None),
    )
    out_specs = P("pp", "tp")
    return jax.shard_map(shards, mesh=mesh, in_specs=in_specs, out_specs=out_specs, check_vma=False)
```

time: 1040 us -> 735 us (0.71)
  the two profiles are of different devices: /device:TPU:1 before, /device:TPU:16 now
where the time goes in v1:
time: 735 us; the launch traced here: 730 us
  Pallas kernels  269 us (37%)
  blocking collectives  258 us (35%)
  waiting for transfers between devices  106 us (14%)
  local copies, waits for them, and re-layouts  42.7 us (6%)
  starting transfers between devices  26.9 us (4%)
  between operations  14.3 us (2%)
  other arithmetic  13 us (2%)
    pallas_call x18, Pallas kernels, section(): pl.pallas_call(section_kernel, out_shape=(jax.ShapeDtypeStruct((rows, wid...  269 us
    all_gather x18, blocking collectives, slot(): got = lax.all_gather(current, ('pp', 'tp'), axis_index_groups=groups(odd))  163 us
    all_gather x1, waiting for transfers between devices, shards(): weights = lax.all_gather(by_core(local), 'tp', axis_index_groups=same_core)  91.7 us
    unnamed x1, blocking collectives  56.1 us
    all_gather x1, blocking collectives, gathered_line(): whole = lax.all_gather(block, 'tp', axis_index_groups=same_core)  38.8 us
    all_to_all x1, starting transfers between devices, shards(): received = lax.all_to_all(spread, 'tp', 0, 0, axis_index_groups=same_core)  24.2 us
    all_to_all x1, waiting for transfers between devices, shards(): received = lax.all_to_all(spread, 'tp', 0, 0, axis_index_groups=same_core)  14.7 us
  transfers between devices with their start and end apart: 6, of which 2 were waited for; matrix products, arithmetic and copies ran while one was open for 1% of the time, Pallas kernels for 0%

profile of v1, /device:TPU:16, one launch (start us, length us, event | category | flops | bytes accessed | tf_op | source)
XLA Modules:
  0.0 730.3 jit_solution(11065729235948795074)
XLA Ops:
  7.9 2.2 reshape.34
  10.1 1.7 copy.33
  11.7 4.3 all_gather_reshape.3
  16.1 38.8 %all-gather.2 = bf16[1024,64]{1,0:T(8,128)(2,1)S(1)} all-gather(bf16[64,64]{1,0:T(8,128)(2,1)S(1)} %copy-done), channel_id=4, replica_groups={{0,2,4,6,8,10,12,14,16,18,20,22,24,26,28,30},{1,3,5,7,9,11,13,15,17,19,..., dimensions={0}, use_global_device_ids=true | all-gather | bytes 139264 | tf_op jit(solution)/shard_map/all_gather | solution.py:178
  59.4 56.1 %all-reduce = f32[3072]{0:T(1024)S(1)} all-reduce(f32[3072]{0:T(1024)S(1)} %maximum_dynamic-update-slice_fusion), channel_id=5, replica_groups={{0,2,4,6,8,10,12,14,16,18,20,22,24,26,28,30},{1,3,5,7,9,11,13,15,17,19,..., use_global_device_ids=true, to_apply=%add | all-reduce | flops 3072 | bytes 24576
  118.7 1.4 reshape.37.spike
  121.4 91.7 %all-gather.14.cloned.1.call-done.weights = bf16[16,4,64,2048]{3,2,1,0:T(8,128)(2,1)} async-done(((bf16[1,4,64,2048]{3,2,1,0:T(8,128)(2,1)}), bf16[16,4,64,2048]{3,2,1,0:T(8,128)(2,1)}) %all-gather.14.cloned.1.call-update) | async-done | bytes 16777232 | tf_op jit(solution)/shard_map/all_gather | solution.py:167
  213.2 419.9 %while.17 = (s32[]{:T(128)}, bf16[64,1024]{1,0:T(8,128)(2,1)S(1)}, f32[8,128,128]{2,1,0:T(8,128)S(1)}, s32[]{:T(128)}, s32[]{:T(128)}, /*index=5*/s32[]{:T(128)}...) while((s32[]{:T(128)}, bf16[64,1024]{1,0:T(8,128)(2,1)S(1)}, ...), condition=%wide.region_1.2_spmd.clone, body=%wide.region_0.1_spmd.clone.sunk | while | flops 2147614720 | bytes 36972604 | solution.py:216
  213.8 9.2 %all-gather.10 = bf16[256,1024]{1,0:T(8,128)(2,1)} all-gather(bf16[64,1024]{1,0:T(8,128)(2,1)S(1)} %select_select_fusion.2), channel_id=2, replica_groups={{32,33,64,65},{34,35,66,67},{36,37,68,69},{38,39,70,71},{40,41,72,73},{..., dimensions={0}, use_global_device_ids=true | all-gather | bytes 655360 | tf_op jit(solution)/shard_map/while/body/eval_jaxpr/all_gather | solution.py:202
  224.2 1.4 reshape.68.spike
  226.2 15.1 %eval_jaxpr.12 = (bf16[64,1024]{1,0:T(8,128)(2,1)}, f32[8,128,128]{2,1,0:T(8,128)S(1)}) custom-call(s32[4]{0:T(128)} %add_add_fusion.7.flags, bf16[4,64,1024]{2,1,0:T(8,128)(2,1)} %bitcast.57, f32[1,2048]{1,0:T(1,128)S(1)} %get-tuple-element.497.gain, bf16[16,4,64,2048]{3,2,1,0:T(8,128)(2,1)} %get-tuple-element.498.weights, ...), custom_call_target="tpu_custom_call", output_to_operand_aliasing={{1}: (7, {})} | custom-call | flops 1073741824 | bytes 16777216 | tf_op jit(solution)/shard_map/while/body/eval_jaxpr/pallas_call | solution.py:104
  241.4 7.9 %all-gather.11 = bf16[256,1024]{1,0:T(8,128)(2,1)} all-gather(bf16[64,1024]{1,0:T(8,128)(2,1)} %get-tuple-element.448), channel_id=3, replica_groups={{0,1,32,33},{2,3,34,35},{4,5,36,37},{6,7,38,39},{8,9,40,41},{10,11,42,4..., dimensions={0}, use_global_device_ids=true | all-gather | bytes 655360 | tf_op jit(solution)/shard_map/while/body/eval_jaxpr/all_gather | solution.py:202
  249.9 14.5 %eval_jaxpr.13 = (bf16[64,1024]{1,0:T(8,128)(2,1)S(1)}, f32[8,128,128]{2,1,0:T(8,128)S(1)}) custom-call(s32[4]{0:T(128)} %add_add_fusion.6.flags, bf16[4,64,1024]{2,1,0:T(8,128)(2,1)} %bitcast.56, f32[1,2048]{1,0:T(1,128)S(1)} %get-tuple-element.497.gain, bf16[16,4,64,2048]{3,2,1,0:T(8,128)(2,1)} %get-tuple-element.498.weights, ...), custom_call_target="tpu_custom_call", output_to_operand_aliasing={{1}: (7, {})} | custom-call | flops 1073741824 | bytes 16777216 | tf_op jit(solution)/shard_map/while/body/eval_jaxpr/pallas_call | solution.py:104
  265.1 9.8 %all-gather.10 = bf16[256,1024]{1,0:T(8,128)(2,1)} all-gather(bf16[64,1024]{1,0:T(8,128)(2,1)S(1)} %select_select_fusion.2), channel_id=2, replica_groups={{32,33,64,65},{34,35,66,67},{36,37,68,69},{38,39,70,71},{40,41,72,73},{..., dimensions={0}, use_global_device_ids=true | all-gather | bytes 655360 | tf_op jit(solution)/shard_map/while/body/eval_jaxpr/all_gather | solution.py:202
  278.2 15.1 %eval_jaxpr.12 = (bf16[64,1024]{1,0:T(8,128)(2,1)}, f32[8,128,128]{2,1,0:T(8,128)S(1)}) custom-call(s32[4]{0:T(128)} %add_add_fusion.7.flags, bf16[4,64,1024]{2,1,0:T(8,128)(2,1)} %bitcast.57, f32[1,2048]{1,0:T(1,128)S(1)} %get-tuple-element.497.gain, bf16[16,4,64,2048]{3,2,1,0:T(8,128)(2,1)} %get-tuple-element.498.weights, ...), custom_call_target="tpu_custom_call", output_to_operand_aliasing={{1}: (7, {})} | custom-call | flops 1073741824 | bytes 16777216 | tf_op jit(solution)/shard_map/while/body/eval_jaxpr/pallas_call | solution.py:104
  293.3 7.9 %all-gather.11 = bf16[256,1024]{1,0:T(8,128)(2,1)} all-gather(bf16[64,1024]{1,0:T(8,128)(2,1)} %get-tuple-element.448), channel_id=3, replica_groups={{0,1,32,33},{2,3,34,35},{4,5,36,37},{6,7,38,39},{8,9,40,41},{10,11,42,4..., dimensions={0}, use_global_device_ids=true | all-gather | bytes 655360 | tf_op jit(solution)/shard_map/while/body/eval_jaxpr/all_gather | solution.py:202
  301.9 14.5 %eval_jaxpr.13 = (bf16[64,1024]{1,0:T(8,128)(2,1)S(1)}, f32[8,128,128]{2,1,0:T(8,128)S(1)}) custom-call(s32[4]{0:T(128)} %add_add_fusion.6.flags, bf16[4,64,1024]{2,1,0:T(8,128)(2,1)} %bitcast.56, f32[1,2048]{1,0:T(1,128)S(1)} %get-tuple-element.497.gain, bf16[16,4,64,2048]{3,2,1,0:T(8,128)(2,1)} %get-tuple-element.498.weights, ...), custom_call_target="tpu_custom_call", output_to_operand_aliasing={{1}: (7, {})} | custom-call | flops 1073741824 | bytes 16777216 | tf_op jit(solution)/shard_map/while/body/eval_jaxpr/pallas_call | solution.py:104
  317.0 9.8 %all-gather.10 = bf16[256,1024]{1,0:T(8,128)(2,1)} all-gather(bf16[64,1024]{1,0:T(8,128)(2,1)S(1)} %select_select_fusion.2), channel_id=2, replica_groups={{32,33,64,65},{34,35,66,67},{36,37,68,69},{38,39,70,71},{40,41,72,73},{..., dimensions={0}, use_global_device_ids=true | all-gather | bytes 655360 | tf_op jit(solution)/shard_map/while/body/eval_jaxpr/all_gather | solution.py:202
  330.2 15.1 %eval_jaxpr.12 = (bf16[64,1024]{1,0:T(8,128)(2,1)}, f32[8,128,128]{2,1,0:T(8,128)S(1)}) custom-call(s32[4]{0:T(128)} %add_add_fusion.7.flags, bf16[4,64,1024]{2,1,0:T(8,128)(2,1)} %bitcast.57, f32[1,2048]{1,0:T(1,128)S(1)} %get-tuple-element.497.gain, bf16[16,4,64,2048]{3,2,1,0:T(8,128)(2,1)} %get-tuple-element.498.weights, ...), custom_call_target="tpu_custom_call", output_to_operand_aliasing={{1}: (7, {})} | custom-call | flops 1073741824 | bytes 16777216 | tf_op jit(solution)/shard_map/while/body/eval_jaxpr/pallas_call | solution.py:104
  345.3 7.9 %all-gather.11 = bf16[256,1024]{1,0:T(8,128)(2,1)} all-gather(bf16[64,1024]{1,0:T(8,128)(2,1)} %get-tuple-element.448), channel_id=3, replica_groups={{0,1,32,33},{2,3,34,35},{4,5,36,37},{6,7,38,39},{8,9,40,41},{10,11,42,4..., dimensions={0}, use_global_device_ids=true | all-gather | bytes 655360 | tf_op jit(solution)/shard_map/while/body/eval_jaxpr/all_gather | solution.py:202
  353.8 14.5 %eval_jaxpr.13 = (bf16[64,1024]{1,0:T(8,128)(2,1)S(1)}, f32[8,128,128]{2,1,0:T(8,128)S(1)}) custom-call(s32[4]{0:T(128)} %add_add_fusion.6.flags, bf16[4,64,1024]{2,1,0:T(8,128)(2,1)} %bitcast.56, f32[1,2048]{1,0:T(1,128)S(1)} %get-tuple-element.497.gain, bf16[16,4,64,2048]{3,2,1,0:T(8,128)(2,1)} %get-tuple-element.498.weights, ...), custom_call_target="tpu_custom_call", output_to_operand_aliasing={{1}: (7, {})} | custom-call | flops 1073741824 | bytes 16777216 | tf_op jit(solution)/shard_map/while/body/eval_jaxpr/pallas_call | solution.py:104
  369.0 9.8 %all-gather.10 = bf16[256,1024]{1,0:T(8,128)(2,1)} all-gather(bf16[64,1024]{1,0:T(8,128)(2,1)S(1)} %select_select_fusion.2), channel_id=2, replica_groups={{32,33,64,65},{34,35,66,67},{36,37,68,69},{38,39,70,71},{40,41,72,73},{..., dimensions={0}, use_global_device_ids=true | all-gather | bytes 655360 | tf_op jit(solution)/shard_map/while/body/eval_jaxpr/all_gather | solution.py:202
  380.0 1.4 reshape.68.spike
  382.1 15.1 %eval_jaxpr.12 = (bf16[64,1024]{1,0:T(8,128)(2,1)}, f32[8,128,128]{2,1,0:T(8,128)S(1)}) custom-call(s32[4]{0:T(128)} %add_add_fusion.7.flags, bf16[4,64,1024]{2,1,0:T(8,128)(2,1)} %bitcast.57, f32[1,2048]{1,0:T(1,128)S(1)} %get-tuple-element.497.gain, bf16[16,4,64,2048]{3,2,1,0:T(8,128)(2,1)} %get-tuple-element.498.weights, ...), custom_call_target="tpu_custom_call", output_to_operand_aliasing={{1}: (7, {})} | custom-call | flops 1073741824 | bytes 16777216 | tf_op jit(solution)/shard_map/while/body/eval_jaxpr/pallas_call | solution.py:104
  397.2 7.9 %all-gather.11 = bf16[256,1024]{1,0:T(8,128)(2,1)} all-gather(bf16[64,1024]{1,0:T(8,128)(2,1)} %get-tuple-element.448), channel_id=3, replica_groups={{0,1,32,33},{2,3,34,35},{4,5,36,37},{6,7,38,39},{8,9,40,41},{10,11,42,4..., dimensions={0}, use_global_device_ids=true | all-gather | bytes 655360 | tf_op jit(solution)/shard_map/while/body/eval_jaxpr/all_gather | solution.py:202
  405.8 14.5 %eval_jaxpr.13 = (bf16[64,1024]{1,0:T(8,128)(2,1)S(1)}, f32[8,128,128]{2,1,0:T(8,128)S(1)}) custom-call(s32[4]{0:T(128)} %add_add_fusion.6.flags, bf16[4,64,1024]{2,1,0:T(8,128)(2,1)} %bitcast.56, f32[1,2048]{1,0:T(1,128)S(1)} %get-tuple-element.497.gain, bf16[16,4,64,2048]{3,2,1,0:T(8,128)(2,1)} %get-tuple-element.498.weights, ...), custom_call_target="tpu_custom_call", output_to_operand_aliasing={{1}: (7, {})} | custom-call | flops 1073741824 | bytes 16777216 | tf_op jit(solution)/shard_map/while/body/eval_jaxpr/pallas_call | solution.py:104
  420.9 13.0 %all-gather.10 = bf16[256,1024]{1,0:T(8,128)(2,1)} all-gather(bf16[64,1024]{1,0:T(8,128)(2,1)S(1)} %select_select_fusion.2), channel_id=2, replica_groups={{32,33,64,65},{34,35,66,67},{36,37,68,69},{38,39,70,71},{40,41,72,73},{..., dimensions={0}, use_global_device_ids=true | all-gather | bytes 655360 | tf_op jit(solution)/shard_map/while/body/eval_jaxpr/all_gather | solution.py:202
  437.2 16.1 %eval_jaxpr.12 = (bf16[64,1024]{1,0:T(8,128)(2,1)}, f32[8,128,128]{2,1,0:T(8,128)S(1)}) custom-call(s32[4]{0:T(128)} %add_add_fusion.7.flags, bf16[4,64,1024]{2,1,0:T(8,128)(2,1)} %bitcast.57, f32[1,2048]{1,0:T(1,128)S(1)} %get-tuple-element.497.gain, bf16[16,4,64,2048]{3,2,1,0:T(8,128)(2,1)} %get-tuple-element.498.weights, ...), custom_call_target="tpu_custom_call", output_to_operand_aliasing={{1}: (7, {})} | custom-call | flops 1073741824 | bytes 16777216 | tf_op jit(solution)/shard_map/while/body/eval_jaxpr/pallas_call | solution.py:104
  453.4 7.9 %all-gather.11 = bf16[256,1024]{1,0:T(8,128)(2,1)} all-gather(bf16[64,1024]{1,0:T(8,128)(2,1)} %get-tuple-element.448), channel_id=3, replica_groups={{0,1,32,33},{2,3,34,35},{4,5,36,37},{6,7,38,39},{8,9,40,41},{10,11,42,4..., dimensions={0}, use_global_device_ids=true | all-gather | bytes 655360 | tf_op jit(solution)/shard_map/while/body/eval_jaxpr/all_gather | solution.py:202
  461.9 14.5 %eval_jaxpr.13 = (bf16[64,1024]{1,0:T(8,128)(2,1)S(1)}, f32[8,128,128]{2,1,0:T(8,128)S(1)}) custom-call(s32[4]{0:T(128)} %add_add_fusion.6.flags, bf16[4,64,1024]{2,1,0:T(8,128)(2,1)} %bitcast.56, f32[1,2048]{1,0:T(1,128)S(1)} %get-tuple-element.497.gain, bf16[16,4,64,2048]{3,2,1,0:T(8,128)(2,1)} %get-tuple-element.498.weights, ...), custom_call_target="tpu_custom_call", output_to_operand_aliasing={{1}: (7, {})} | custom-call | flops 1073741824 | bytes 16777216 | tf_op jit(solution)/shard_map/while/body/eval_jaxpr/pallas_call | solution.py:104
  477.1 9.8 %all-gather.10 = bf16[256,1024]{1,0:T(8,128)(2,1)} all-gather(bf16[64,1024]{1,0:T(8,128)(2,1)S(1)} %select_select_fusion.2), channel_id=2, replica_groups={{32,33,64,65},{34,35,66,67},{36,37,68,69},{38,39,70,71},{40,41,72,73},{..., dimensions={0}, use_global_device_ids=true | all-gather | bytes 655360 | tf_op jit(solution)/shard_map/while/body/eval_jaxpr/all_gather | solution.py:202
  490.2 15.1 %eval_jaxpr.12 = (bf16[64,1024]{1,0:T(8,128)(2,1)}, f32[8,128,128]{2,1,0:T(8,128)S(1)}) custom-call(s32[4]{0:T(128)} %add_add_fusion.7.flags, bf16[4,64,1024]{2,1,0:T(8,128)(2,1)} %bitcast.57, f32[1,2048]{1,0:T(1,128)S(1)} %get-tuple-element.497.gain, bf16[16,4,64,2048]{3,2,1,0:T(8,128)(2,1)} %get-tuple-element.498.weights, ...), custom_call_target="tpu_custom_call", output_to_operand_aliasing={{1}: (7, {})} | custom-call | flops 1073741824 | bytes 16777216 | tf_op jit(solution)/shard_map/while/body/eval_jaxpr/pallas_call | solution.py:104
  505.3 8.4 %all-gather.11 = bf16[256,1024]{1,0:T(8,128)(2,1)} all-gather(bf16[64,1024]{1,0:T(8,128)(2,1)} %get-tuple-element.448), channel_id=3, replica_groups={{0,1,32,33},{2,3,34,35},{4,5,36,37},{6,7,38,39},{8,9,40,41},{10,11,42,4..., dimensions={0}, use_global_device_ids=true | all-gather | bytes 655360 | tf_op jit(solution)/shard_map/while/body/eval_jaxpr/all_gather | solution.py:202
  514.3 14.5 %eval_jaxpr.13 = (bf16[64,1024]{1,0:T(8,128)(2,1)S(1)}, f32[8,128,128]{2,1,0:T(8,128)S(1)}) custom-call(s32[4]{0:T(128)} %add_add_fusion.6.flags, bf16[4,64,1024]{2,1,0:T(8,128)(2,1)} %bitcast.56, f32[1,2048]{1,0:T(1,128)S(1)} %get-tuple-element.497.gain, bf16[16,4,64,2048]{3,2,1,0:T(8,128)(2,1)} %get-tuple-element.498.weights, ...), custom_call_target="tpu_custom_call", output_to_operand_aliasing={{1}: (7, {})} | custom-call | flops 1073741824 | bytes 16777216 | tf_op jit(solution)/shard_map/while/body/eval_jaxpr/pallas_call | solution.py:104
  529.5 9.8 %all-gather.10 = bf16[256,1024]{1,0:T(8,128)(2,1)} all-gather(bf16[64,1024]{1,0:T(8,128)(2,1)S(1)} %select_select_fusion.2), channel_id=2, replica_groups={{32,33,64,65},{34,35,66,67},{36,37,68,69},{38,39,70,71},{40,41,72,73},{..., dimensions={0}, use_global_device_ids=true | all-gather | bytes 655360 | tf_op jit(solution)/shard_map/while/body/eval_jaxpr/all_gather | solution.py:202
  542.6 15.1 %eval_jaxpr.12 = (bf16[64,1024]{1,0:T(8,128)(2,1)}, f32[8,128,128]{2,1,0:T(8,128)S(1)}) custom-call(s32[4]{0:T(128)} %add_add_fusion.7.flags, bf16[4,64,1024]{2,1,0:T(8,128)(2,1)} %bitcast.57, f32[1,2048]{1,0:T(1,128)S(1)} %get-tuple-element.497.gain, bf16[16,4,64,2048]{3,2,1,0:T(8,128)(2,1)} %get-tuple-element.498.weights, ...), custom_call_target="tpu_custom_call", output_to_operand_aliasing={{1}: (7, {})} | custom-call | flops 1073741824 | bytes 16777216 | tf_op jit(solution)/shard_map/while/body/eval_jaxpr/pallas_call | solution.py:104
  557.8 7.9 %all-gather.11 = bf16[256,1024]{1,0:T(8,128)(2,1)} all-gather(bf16[64,1024]{1,0:T(8,128)(2,1)} %get-tuple-element.448), channel_id=3, replica_groups={{0,1,32,33},{2,3,34,35},{4,5,36,37},{6,7,38,39},{8,9,40,41},{10,11,42,4..., dimensions={0}, use_global_device_ids=true | all-gather | bytes 655360 | tf_op jit(solution)/shard_map/while/body/eval_jaxpr/all_gather | solution.py:202
  566.3 14.5 %eval_jaxpr.13 = (bf16[64,1024]{1,0:T(8,128)(2,1)S(1)}, f32[8,128,128]{2,1,0:T(8,128)S(1)}) custom-call(s32[4]{0:T(128)} %add_add_fusion.6.flags, bf16[4,64,1024]{2,1,0:T(8,128)(2,1)} %bitcast.56, f32[1,2048]{1,0:T(1,128)S(1)} %get-tuple-element.497.gain, bf16[16,4,64,2048]{3,2,1,0:T(8,128)(2,1)} %get-tuple-element.498.weights, ...), custom_call_target="tpu_custom_call", output_to_operand_aliasing={{1}: (7, {})} | custom-call | flops 1073741824 | bytes 16777216 | tf_op jit(solution)/shard_map/while/body/eval_jaxpr/pallas_call | solution.py:104
  581.4 9.8 %all-gather.10 = bf16[256,1024]{1,0:T(8,128)(2,1)} all-gather(bf16[64,1024]{1,0:T(8,128)(2,1)S(1)} %select_select_fusion.2), channel_id=2, replica_groups={{32,33,64,65},{34,35,66,67},{36,37,68,69},{38,39,70,71},{40,41,72,73},{..., dimensions={0}, use_global_device_ids=true | all-gather | bytes 655360 | tf_op jit(solution)/shard_map/while/body/eval_jaxpr/all_gather | solution.py:202
  594.6 15.1 %eval_jaxpr.12 = (bf16[64,1024]{1,0:T(8,128)(2,1)}, f32[8,128,128]{2,1,0:T(8,128)S(1)}) custom-call(s32[4]{0:T(128)} %add_add_fusion.7.flags, bf16[4,64,1024]{2,1,0:T(8,128)(2,1)} %bitcast.57, f32[1,2048]{1,0:T(1,128)S(1)} %get-tuple-element.497.gain, bf16[16,4,64,2048]{3,2,1,0:T(8,128)(2,1)} %get-tuple-element.498.weights, ...), custom_call_target="tpu_custom_call", output_to_operand_aliasing={{1}: (7, {})} | custom-call | flops 1073741824 | bytes 16777216 | tf_op jit(solution)/shard_map/while/body/eval_jaxpr/pallas_call | solution.py:104
  609.7 8.2 %all-gather.11 = bf16[256,1024]{1,0:T(8,128)(2,1)} all-gather(bf16[64,1024]{1,0:T(8,128)(2,1)} %get-tuple-element.448), channel_id=3, replica_groups={{0,1,32,33},{2,3,34,35},{4,5,36,37},{6,7,38,39},{8,9,40,41},{10,11,42,4..., dimensions={0}, use_global_device_ids=true | all-gather | bytes 655360 | tf_op jit(solution)/shard_map/while/body/eval_jaxpr/all_gather | solution.py:202
  618.5 14.5 %eval_jaxpr.13 = (bf16[64,1024]{1,0:T(8,128)(2,1)S(1)}, f32[8,128,128]{2,1,0:T(8,128)S(1)}) custom-call(s32[4]{0:T(128)} %add_add_fusion.6.flags, bf16[4,64,1024]{2,1,0:T(8,128)(2,1)} %bitcast.56, f32[1,2048]{1,0:T(1,128)S(1)} %get-tuple-element.497.gain, bf16[16,4,64,2048]{3,2,1,0:T(8,128)(2,1)} %get-tuple-element.498.weights, ...), custom_call_target="tpu_custom_call", output_to_operand_aliasing={{1}: (7, {})} | custom-call | flops 1073741824 | bytes 16777216 | tf_op jit(solution)/shard_map/while/body/eval_jaxpr/pallas_call | solution.py:104
  633.1 9.8 %all-gather.4 = bf16[256,1024]{1,0:T(8,128)(2,1)} all-gather(bf16[64,1024]{1,0:T(8,128)(2,1)S(1)} %broadcast_select_fusion), channel_id=6, replica_groups={{32,33,64,65},{34,35,66,67},{36,37,68,69},{38,39,70,71},{40,41,72,73},{..., dimensions={0}, use_global_device_ids=true | all-gather | bytes 655360 | tf_op jit(solution)/shard_map/all_gather | solution.py:202
  642.9 15.1 %shard_map.91 = (bf16[64,1024]{1,0:T(8,128)(2,1)}, f32[8,128,128]{2,1,0:T(8,128)S(1)}) custom-call(s32[4]{0:T(128)} %add_add_fusion.3.flags, bf16[4,64,1024]{2,1,0:T(8,128)(2,1)} %bitcast.60, f32[1,2048]{1,0:T(1,128)S(1)} %get-tuple-element.515, bf16[16,4,64,2048]{3,2,1,0:T(8,128)(2,1)} %get-tuple-element.508, ...), custom_call_target="tpu_custom_call", output_to_operand_aliasing={{1}: (7, {})} | custom-call | flops 1073741824 | bytes 16777216 | tf_op jit(solution)/shard_map/pallas_call | solution.py:104
  658.0 7.9 %all-gather.5 = bf16[256,1024]{1,0:T(8,128)(2,1)} all-gather(bf16[64,1024]{1,0:T(8,128)(2,1)} %get-tuple-element.263), channel_id=7, replica_groups={{0,1,32,33},{2,3,34,35},{4,5,36,37},{6,7,38,39},{8,9,40,41},{10,11,42,4..., dimensions={0}, use_global_device_ids=true | all-gather | bytes 655360 | tf_op jit(solution)/shard_map/all_gather | solution.py:202
  665.9 15.1 %shard_map.92 = (bf16[64,1024]{1,0:T(8,128)(2,1)}, f32[8,128,128]{2,1,0:T(8,128)S(1)}) custom-call(s32[4]{0:T(128)} %add_add_fusion.2.flags, bf16[4,64,1024]{2,1,0:T(8,128)(2,1)} %bitcast.59, f32[1,2048]{1,0:T(1,128)S(1)} %get-tuple-element.515, bf16[16,4,64,2048]{3,2,1,0:T(8,128)(2,1)} %get-tuple-element.508, ...), custom_call_target="tpu_custom_call", output_to_operand_aliasing={{1}: (7, {})} | custom-call | flops 1073741824 | bytes 16777216 | tf_op jit(solution)/shard_map/pallas_call | solution.py:104
  683.6 24.2 %all-to-all-start = ((bf16[16,2,2048]{2,1,0:T(2,128)(2,1)}), bf16[16,2,2048]{2,1,0:T(2,128)(2,1)S(1)}, u32[]{:S(2)}, u32[]{:S(2)}) async-start(bf16[16,2,2048]{2,1,0:T(2,128)(2,1)} %reshape.65), calls=%async_computation | async-start | bytes 262144 | tf_op jit(solution)/shard_map/all_to_all | solution.py:223
  707.9 14.7 %all-to-all-done = bf16[16,2,2048]{2,1,0:T(2,128)(2,1)S(1)} async-done(((bf16[16,2,2048]{2,1,0:T(2,128)(2,1)}), bf16[16,2,2048]{2,1,0:T(2,128)(2,1)S(1)}, u32[]{:S(2)}, u32[]{:S(2)}) %all-to-all-start) | async-done | bytes 131104 | tf_op jit(solution)/shard_map/all_to_all | solution.py:223
  (105 shorter events, 46.1 us)
Async XLA Ops:
  6.5 206.6 %all-gather.14.cloned.1.call-start = ((), (), s32[]{:S(2)}) async-start(), calls=%async_computation.1 | async-start | bytes 17825792 | tf_op jit(solution)/shard_map/all_gather | solution.py:167
  11.7 4.3 copy-start
  11.7 46.8 %copy-start.2 = (f32[1,128,1]{1,2,0:T(1,128)S(1)}, f32[1,128,1]{1,2,0:T(1,128)}, u32[]{:S(2)}) copy-start(f32[1,128,1]{1,2,0:T(1,128)} %param.18) | copy-start | bytes 1540
  11.7 46.9 %copy-start.3 = (f32[1,64]{1,0:T(1,128)S(1)}, f32[1,64]{1,0:T(1,128)}, u32[]{:S(2)}) copy-start(f32[1,64]{1,0:T(1,128)} %param.17) | copy-start | bytes 772
  16.0 100.6 %copy-start.1 = (f32[1,2048]{1,0:T(1,128)S(1)}, f32[1,2048]{1,0:T(1,128)}, u32[]{:S(2)}) copy-start(f32[1,2048]{1,0:T(1,128)} %param.12) | copy-start | bytes 24580
  55.3 64.8 %copy-start.4 = (f32[1,64]{1,0:T(1,128)S(1)}, f32[1,64]{1,0:T(1,128)}, u32[]{:S(2)}) copy-start(f32[1,64]{1,0:T(1,128)} %param.19) | copy-start | bytes 772
  55.3 66.2 %collective-permute-start.1 = (bf16[64,1024]{1,0:T(8,128)(2,1)S(1)}, bf16[64,1024]{1,0:T(8,128)(2,1)S(1)}, u32[]{:S(2)}, u32[]{:S(2)}) collective-permute-start(bf16[64,1024]{1,0:T(8,128)(2,1)S(1)} %reshape.31), channel_id=1, source_target_pairs={{32,0},{33,1},{100,4},{101,5},{168,8},{169,9},{236,12},{237,13},{3... | collective-permute-start | bytes 393224 | tf_op jit(solution)/shard_map/ppermute | solution.py:187
  55.9 65.5 %collective-permute-start = (bf16[64,1024]{1,0:T(8,128)(2,1)S(1)}, bf16[64,1024]{1,0:T(8,128)(2,1)S(1)}, u32[]{:S(2)}, u32[]{:S(2)}) collective-permute-start(bf16[64,1024]{1,0:T(8,128)(2,1)S(1)} %reshape.31), channel_id=1, source_target_pairs={{0,0},{1,1},{68,4},{69,5},{136,8},{137,9},{204,12},{205,13},{272,1... | collective-permute-start | bytes 393224 | tf_op jit(solution)/shard_map/ppermute | solution.py:187
  681.0 1.4 collective-permute-start.3
  681.7 0.7 collective-permute-start.2
  683.6 39.0 %all-to-all-start = ((bf16[16,2,2048]{2,1,0:T(2,128)(2,1)}), bf16[16,2,2048]{2,1,0:T(2,128)(2,1)S(1)}, u32[]{:S(2)}, u32[]{:S(2)}) async-start(bf16[16,2,2048]{2,1,0:T(2,128)(2,1)} %reshape.65), calls=%async_computation | async-start | bytes 262144 | tf_op jit(solution)/shard_map/all_to_all | solution.py:223
Sparse Core Ops, SparseCore 0:
  16.2 196.8 all-gather.13

commit v2 on v1

v2 whole, which is shorter than its diff:
```python
import jax
import jax.numpy as jnp
from jax import lax
from jax.experimental import pallas as pl
from jax.experimental.pallas import tpu as pltpu
from jax.sharding import PartitionSpec as P

HEAD = 64
SEG = 64
EPSILON = 1e-06
NT = (((1,), (1,)), ((), ()))
NN = (((1,), (0,)), ((), ()))
TN = (((0,), (0,)), ((), ()))


def section_kernel(flags, got, gain, weights, edge, spike, out_gain, state_in, result, state, scaled, product):
    first, unit, base, core = flags[0], flags[1], flags[2], flags[3]
    rows, width = got.shape[1:]
    groups = weights.shape[0] // 4
    low = lax.broadcasted_iota(jnp.int32, (rows, 128), 1) < HEAD

    total = jnp.zeros((rows, 128), jnp.float32)
    for tile in range(width // 128):
        columns = pl.ds(tile * 128, 128)
        even = got[base, :, columns].astype(jnp.float32)
        odd = got[base + 1, :, columns].astype(jnp.float32)
        total = total + even * even + odd * odd
        left = jnp.where(low, even, pltpu.roll(odd, HEAD, 1))
        right = jnp.where(low, pltpu.roll(even, HEAD, 1), odd)
        for step, wide in enumerate((left, right)):
            columns = pl.ds((2 * tile + step) * 128, 128)
            scaled[:, columns] = (wide * gain[:, columns]).astype(jnp.bfloat16)
    total = jnp.sum(total, axis=1, keepdims=True)
    scale = jnp.broadcast_to(lax.rsqrt(total / (2 * width) + EPSILON), (rows, 128))

    at = lax.broadcasted_iota(jnp.int32, (rows, 2 * rows), 0)
    of = lax.broadcasted_iota(jnp.int32, (rows, 2 * rows), 1)
    ones = jnp.where(at >= jnp.where(of >= rows, of - rows, of), 1.0, 0.0).astype(jnp.bfloat16)
    at = lax.broadcasted_iota(jnp.int32, (2 * rows, rows), 0)
    of = lax.broadcasted_iota(jnp.int32, (2 * rows, rows), 1)
    causal = jnp.where(at >= rows, at - rows, at) >= of
    same = (lax.broadcasted_iota(jnp.int32, (128, 128), 0) < HEAD) == (
        lax.broadcasted_iota(jnp.int32, (128, 128), 1) < HEAD
    )
    mean = jnp.where(same, 1.0 / HEAD, 0.0).astype(jnp.bfloat16)
    mean = jnp.concatenate([mean, mean], axis=0)

    def halves(array):
        high = array.astype(jnp.bfloat16)
        return high, (array - high.astype(jnp.float32)).astype(jnp.bfloat16)

    def mix(pair, start):
        tiles = [product[:, start + 128 * k : start + 128 * k + 128] * scale for k in range(4)]
        rolled = [pltpu.roll(tile, HEAD, 1) for tile in tiles]
        query_pre = jnp.where(low, tiles[0], rolled[2])
        forget_pre = jnp.where(low, rolled[0], tiles[2])
        values = jnp.where(low, tiles[1], rolled[3]).astype(jnp.bfloat16)
        gate_pre = jnp.where(low, rolled[1], tiles[3])

        lower = edge[pair]
        upper = 1.0 - lower
        log_forget = jnp.log(lower + upper * jax.nn.sigmoid(forget_pre)) + spike[unit, pair]
        key_in = upper * jax.nn.sigmoid(-forget_pre)
        queries = query_pre * jax.nn.sigmoid(query_pre)
        running = lax.dot_general(
            ones, jnp.concatenate(halves(log_forget), axis=0), NN, preferred_element_type=jnp.float32
        )
        query_scaled = queries * jnp.exp(running)
        key_scaled = (key_in * jnp.exp(-running)).astype(jnp.bfloat16)
        stacked = jnp.concatenate(
            [jnp.where(low, query_scaled, 0.0), jnp.where(low, 0.0, query_scaled)], axis=0
        ).astype(jnp.bfloat16)
        scores = lax.dot_general(stacked, key_scaled, NT, preferred_element_type=jnp.float32)
        scores = jnp.where(causal, scores, 0.0).astype(jnp.bfloat16)
        both = lax.dot_general(scores, values, NN, preferred_element_type=jnp.float32)
        before = state[pair]
        mixed = jnp.where(low, both[:rows], both[rows:]) + lax.dot_general(
            query_scaled.astype(jnp.bfloat16),
            jnp.where(first == 1, 0.0, before).astype(jnp.bfloat16),
            NN,
            preferred_element_type=jnp.float32,
        )
        kept = (key_in * jnp.exp(running[rows - 1 :, :] - running)).astype(jnp.bfloat16)
        carried = lax.dot_general(kept, values, TN, preferred_element_type=jnp.float32)
        state[pair] = jnp.where(first == 1, jnp.where(same, carried, 0.0), before)
        average = lax.dot_general(
            jnp.concatenate(halves(mixed * mixed), axis=1), mean, NN, preferred_element_type=jnp.float32
        )
        branch = mixed * lax.rsqrt(average + EPSILON) * out_gain[...] * (gate_pre * jax.nn.sigmoid(gate_pre))
        columns = pl.ds(pl.multiple_of(pair * 128, 128), 128)
        own = got[base + core, :, columns].astype(jnp.float32)
        result[:, columns] = (own + branch).astype(jnp.bfloat16)

    def turn(index, _):
        now = jnp.maximum(index - 1, 0)
        mix(2 * now, 0)
        mix(2 * now + 1, 512)
        after = jnp.minimum(index, groups - 1)
        for head in range(4):
            product[:, 256 * head : 256 * head + 256] = lax.dot_general(
                scaled[...], weights[4 * after + head], NN, preferred_element_type=jnp.float32
            )
        return 0

    lax.fori_loop(0, groups + 1, turn, 0)


def hold_kernel(source, held, semaphores):
    copies = [
        pltpu.make_async_copy(source.at[head], held.at[head], semaphores.at[head]) for head in range(source.shape[0])
    ]
    for copy in copies:
        copy.start()
    for copy in copies:
        copy.wait()


def hold(weights):
    return pl.pallas_call(
        hold_kernel,
        out_shape=pltpu.VMEM(weights.shape, weights.dtype),
        in_specs=[pl.BlockSpec(memory_space=pltpu.HBM)],
        out_specs=pl.BlockSpec(memory_space=pltpu.VMEM),
        scratch_shapes=[pltpu.SemaphoreType.DMA((weights.shape[0],))],
        compiler_params=pltpu.CompilerParams(vmem_limit_bytes=1 << 20),
        cost_estimate=pl.CostEstimate(flops=0, bytes_accessed=4 * weights.size, transcendentals=0),
    )(weights)


def section(flags, got, gain, weights, edge, spike, out_gain, state):
    rows, width = got.shape[1:]
    return pl.pallas_call(
        section_kernel,
        out_shape=(
            jax.ShapeDtypeStruct((rows, width), jnp.bfloat16),
            jax.ShapeDtypeStruct(state.shape, state.dtype),
        ),
        in_specs=[pl.BlockSpec(memory_space=pltpu.SMEM)] + [pl.BlockSpec(memory_space=pltpu.VMEM)] * 7,
        out_specs=[pl.BlockSpec(memory_space=pltpu.VMEM)] * 2,
        scratch_shapes=[
            pltpu.VMEM((rows, 2 * width), jnp.bfloat16),
            pltpu.VMEM((rows, width), jnp.float32),
        ],
        input_output_aliases={7: 1},
        compiler_params=pltpu.CompilerParams(vmem_limit_bytes=24 << 20),
        cost_estimate=pl.CostEstimate(
            flops=2 * rows * weights.size, bytes_accessed=2 * weights.size, transcendentals=0
        ),
    )(flags, got, gain, weights, edge, spike, out_gain, state)


def shards(
    entry_stream_rows,
    layer_rescale_factor,
    probe_projection,
    retention_projection,
    candidate_projection,
    emission_filter_matrix,
    retention_minimum,
    decay_spike,
    per_group_scale,
):
    sections = lax.axis_size("pp")
    members = lax.axis_size("tp")
    chips = members // 2
    line = lax.axis_index("pp")
    across = 4
    turned = line // across % 2 == 1
    layer = jnp.where(turned, line + across - 1 - 2 * (line % across), line)
    place = [s + across - 1 - 2 * (s % across) if s // across % 2 else s for s in range(sections)]
    core = lax.axis_index("tp") % 2
    half_width = layer_rescale_factor.shape[1] // 2
    pairs = chips // 2
    same_core = [[c + 2 * z for z in range(chips)] for c in range(2)]

    def to_place(array):
        moved = lax.ppermute(array, "pp", [(s, place[s]) for s in range(sections) if place[s] != s])
        return jnp.where(turned, moved, array)

    local = jnp.stack(
        [probe_projection[0], retention_projection[0], candidate_projection[0], emission_filter_matrix[0]]
    )
    local = local.reshape(4 * HEAD, 2 * half_width).T
    weights = lax.all_gather(to_place(local), "tp", axis_index_groups=same_core)
    weights = hold(pltpu.with_memory_space_constraint(weights, pltpu.HBM))
    small = jnp.concatenate(
        [layer_rescale_factor[0], per_group_scale[0], retention_minimum[0], decay_spike[0, :, 0]]
    )
    small = to_place(small)
    gain = small[None, : 2 * half_width]
    out_gain = jnp.tile(small[None, 2 * half_width : 2 * half_width + HEAD], (1, 2))
    small = lax.all_gather(small[2 * half_width + HEAD :], "tp", axis_index_groups=same_core)
    edge = small[:, :HEAD].reshape(pairs, 1, 128)
    spike = small[:, HEAD:].reshape(pairs, 2, 2, SEG)
    spike = jnp.broadcast_to(spike.transpose(2, 0, 3, 1)[..., None], (2, pairs, SEG, 2, HEAD))
    spike = spike.reshape(2, pairs, SEG, 128)
    gain, out_gain, edge, spike = lax.optimization_barrier((gain, out_gain, edge, spike))

    def gathered_line(block):
        whole = lax.all_gather(block, "tp", axis_index_groups=same_core)
        return whole.transpose(1, 0, 2).reshape(block.shape[0], half_width)

    def between(array, pairs_of):
        moves = [
            (a * members + t, b * members + t)
            for a, b, z in pairs_of
            for t in (2 * z, 2 * z + 1)
        ]
        return lax.ppermute(array, ("pp", "tp"), moves)

    micro = sections // 2
    entering = gathered_line(entry_stream_rows)
    entry = [between(entering, [(2 * k + u, 0, 2 * k) for k in range(micro)]) for u in range(2)]

    def groups(odd):
        lines = [(2 * i + odd, (2 * i + 1 + odd) % sections) for i in range(micro)]
        lines = [(place[a], place[b]) for a, b in lines]
        return [
            [a * members + 2 * z, a * members + 2 * z + 1, b * members + 2 * z, b * members + 2 * z + 1]
            for a, b in lines
            for z in range(chips)
        ]

    def slot(index, odd, current, state):
        got = lax.all_gather(current, ("pp", "tp"), axis_index_groups=groups(odd))
        first = (index == layer).astype(jnp.int32)
        base = jnp.where(layer == 0, 2, 0) if odd else jnp.zeros((), jnp.int32)
        flags = jnp.stack([first, 1 - first, base.astype(jnp.int32), core.astype(jnp.int32)])
        return section(flags, got, gain, weights, edge, spike, out_gain, state)

    def two_slots(turn, carried):
        current, state = carried
        fresh = jnp.where(turn == 0, entry[0], entry[1])
        current = jnp.where(layer == 0, fresh, current)
        current, state = slot(2 * turn, True, current, state)
        return slot(2 * turn + 1, False, current, state)

    start = (jnp.zeros((SEG, half_width), jnp.bfloat16), jnp.zeros((pairs, 128, 128), jnp.float32))
    carried = start
    for turn in range(micro):
        carried = two_slots(turn, carried)
    last = place[sections - 1]
    finished = [between(carried[0], [(last, 2 * k, 2 * k) for k in range(micro)])]
    carried = two_slots(micro, carried)
    finished.append(between(carried[0], [(last, 2 * k + 1, 2 * k) for k in range(micro)]))
    mine = jnp.where(line % 2 == 0, finished[0], finished[1])
    spread = mine.reshape(SEG, chips, HEAD).transpose(1, 0, 2)
    received = lax.all_to_all(spread, "tp", 0, 0, axis_index_groups=same_core)
    return lax.dynamic_index_in_dim(received, line // 2 * 2, 0, keepdims=False)


def solution(mesh):
    in_specs = (
        P("pp", "tp"),
        P("pp", None),
        P("pp", "tp", None),
        P("pp", "tp", None),
        P("pp", "tp", None),
        P("pp", "tp", None),
        P("pp", "tp"),
        P("pp", None, "tp"),
        P("pp", None),
    )
    out_specs = P("pp", "tp")
    return jax.shard_map(shards, mesh=mesh, in_specs=in_specs, out_specs=out_specs, check_vma=False)
```

time: 735 us -> 575 us (0.78)
  Pallas kernels: 269 us -> 166 us
  local copies, waits for them, and re-layouts: 42.7 us -> 7.6 us
  waiting for transfers between devices: 106 us -> 95.8 us
  other arithmetic: 13 us -> 4.01 us
    pallas_call x18, Pallas kernels: 269 us -> 160 us  [section(): pl.pallas_call(section_kernel, out_shape=(jax.ShapeDtypeStruct((rows, wid...]
    reshape x9 -> x1, local copies, waits for them, and re-layouts: 12.6 us -> 0.58 us  [shards(): spike = spike.reshape(2, pairs, SEG, 128)]
    all_gather x1, waiting for transfers between devices: 91.7 us -> 81 us  [shards(): weights = lax.all_gather(to_place(local), 'tp', axis_index_groups=same_core)]
    another operation x19 -> x2, local copies, waits for them, and re-layouts: 10.2 us -> 0.09 us  [shards(): jnp.tile(small[None, 2 * half_width:2 * half_width + HEAD], (1, 2))]
    broadcast_in_dim x9 -> x1, local copies, waits for them, and re-layouts: 11 us -> 1.24 us  [shards(): jnp.broadcast_to(spike.transpose(2, 0, 3, 1)[..., None], (2, pairs, SEG,...]
    another operation x18, other arithmetic: 10.7 us -> 1.39 us  [slot(): jnp.stack([first, 1 - first, base.astype(jnp.int32), core.astype(jnp.int3...]
  transfers between devices with their start and end apart: 6 -> 8, of which waited for: 2 -> 2; matrix products, arithmetic and copies ran while one was open for 1% -> 1% of each run, Pallas kernels for 0% -> 4%
where the time goes in v2:
time: 575 us; the launch traced here: 574 us
  blocking collectives  259 us (45%)
  Pallas kernels  166 us (29%)
  waiting for transfers between devices  95.8 us (17%)
  starting transfers between devices  26.5 us (5%)
  between operations  14.7 us (3%)
  local copies, waits for them, and re-layouts  7.6 us (1%)
    all_gather x18, blocking collectives, slot(): got = lax.all_gather(current, ('pp', 'tp'), axis_index_groups=groups(odd))  167 us
    pallas_call x18, Pallas kernels, section(): pl.pallas_call(section_kernel, out_shape=(jax.ShapeDtypeStruct((rows, wid...  160 us
    all_gather x1, waiting for transfers between devices, shards(): weights = lax.all_gather(to_place(local), 'tp', axis_index_groups=same_core)  81 us
    unnamed x1, blocking collectives  55.6 us
    all_gather x1, blocking collectives, gathered_line(): whole = lax.all_gather(block, 'tp', axis_index_groups=same_core)  37 us
    all_to_all x1, starting transfers between devices, shards(): received = lax.all_to_all(spread, 'tp', 0, 0, axis_index_groups=same_core)  22.4 us
    all_to_all x1, waiting for transfers between devices, shards(): received = lax.all_to_all(spread, 'tp', 0, 0, axis_index_groups=same_core)  14.7 us
  transfers between devices with their start and end apart: 8, of which 2 were waited for; matrix products, arithmetic and copies ran while one was open for 1% of the time, Pallas kernels for 4%

profile of v2, /device:TPU:16, one launch (start us, length us, event | category | flops | bytes accessed | tf_op | source)
XLA Modules:
  0.0 574.2 jit_solution(3933062911826962174)
XLA Ops:
  6.5 1.3 pad_maximum_fusion
  9.2 1.1 broadcast_select_fusion
  10.3 37.0 %all-gather = bf16[1024,64]{1,0:T(8,128)(2,1)S(1)} all-gather(bf16[64,64]{1,0:T(8,128)(2,1)} %param.9), channel_id=2, replica_groups={{0,2,4,6,8,10,12,14,16,18,20,22,24,26,28,30},{1,3,5,7,9,11,13,15,17,19,..., dimensions={0}, use_global_device_ids=true | all-gather | bytes 139264 | tf_op jit(solution)/shard_map/all_gather | solution.py:200
  49.1 0.8 concatenate.3
  52.1 1.3 dynamic-slice
  54.2 55.6 %all-reduce = f32[3072]{0:T(1024)S(1)} all-reduce(f32[3072]{0:T(1024)S(1)} %slice_dynamic-update-slice_fusion), channel_id=4, replica_groups={{0,2,4,6,8,10,12,14,16,18,20,22,24,26,28,30},{1,3,5,7,9,11,13,15,17,19,..., use_global_device_ids=true, to_apply=%add | all-reduce | flops 3072 | bytes 24576
  110.3 1.2 broadcast_in_dim.17
  112.3 39.4 %all-gather.1 = bf16[256,1024]{1,0:T(8,128)(2,1)S(1)} all-gather(bf16[64,1024]{1,0:T(8,128)(2,1)S(1)} %broadcast_select_fusion.9), channel_id=3, replica_groups={{32,33,64,65},{34,35,66,67},{36,37,68,69},{38,39,70,71},{40,41,72,73},{..., dimensions={0}, use_global_device_ids=true | all-gather | bytes 655360 | tf_op jit(solution)/shard_map/all_gather | solution.py:225
  151.8 81.0 %all-gather.23.cloned.1.call-done = bf16[32768,256]{1,0:T(8,128)(2,1)} async-done(((bf16[2048,256]{1,0:T(8,128)(2,1)}), bf16[32768,256]{1,0:T(8,128)(2,1)}) %all-gather.23.cloned.1.call-update) | async-done | bytes 16777232 | tf_op jit(solution)/shard_map/all_gather | solution.py:184
  232.8 5.9 %shard_map.91.weights = bf16[16,2048,256]{2,1,0:T(8,128)(2,1)S(1)} custom-call(bf16[16,2048,256]{2,1,0:T(8,128)(2,1)} %bitcast.112), custom_call_target="tpu_custom_call" | custom-call | bytes 33554432 | tf_op jit(solution)/shard_map/pallas_call | solution.py:119
  238.8 8.9 %shard_map.92 = (bf16[64,1024]{1,0:T(8,128)(2,1)S(1)}, f32[8,128,128]{2,1,0:T(8,128)S(1)}) custom-call(s32[4]{0:T(128)S(1)} %add_add_fusion.7.flags, bf16[4,64,1024]{2,1,0:T(8,128)(2,1)S(1)} %bitcast.94, f32[1,2048]{1,0:T(1,128)S(1)} %bitcast.76, bf16[16,2048,256]{2,1,0:T(8,128)(2,1)S(1)} %shard_map.91.weights, ...), custom_call_target="tpu_custom_call", output_to_operand_aliasing={{1}: (7, {})} | custom-call | flops 1073741824 | bytes 16777216 | tf_op jit(solution)/shard_map/pallas_call | solution.py:132
  247.7 7.1 %all-gather.4 = bf16[256,1024]{1,0:T(8,128)(2,1)S(1)} all-gather(bf16[64,1024]{1,0:T(8,128)(2,1)S(1)} %get-tuple-element.48), channel_id=6, replica_groups={{0,1,32,33},{2,3,34,35},{4,5,36,37},{6,7,38,39},{8,9,40,41},{10,11,42,4..., dimensions={0}, use_global_device_ids=true | all-gather | bytes 655360 | tf_op jit(solution)/shard_map/all_gather | solution.py:225
  254.8 8.9 %shard_map.93 = (bf16[64,1024]{1,0:T(8,128)(2,1)S(1)}, f32[8,128,128]{2,1,0:T(8,128)S(1)}) custom-call(s32[4]{0:T(128)S(1)} %fusion.7.flags, bf16[4,64,1024]{2,1,0:T(8,128)(2,1)S(1)} %bitcast.96, f32[1,2048]{1,0:T(1,128)S(1)} %bitcast.77, bf16[16,2048,256]{2,1,0:T(8,128)(2,1)S(1)} %shard_map.91.weights, ...), custom_call_target="tpu_custom_call", output_to_operand_aliasing={{1}: (7, {})} | custom-call | flops 1073741824 | bytes 16777216 | tf_op jit(solution)/shard_map/pallas_call | solution.py:132
  263.8 7.4 %all-gather.5 = bf16[256,1024]{1,0:T(8,128)(2,1)S(1)} all-gather(bf16[64,1024]{1,0:T(8,128)(2,1)S(1)} %broadcast_select_fusion.8), channel_id=7, replica_groups={{32,33,64,65},{34,35,66,67},{36,37,68,69},{38,39,70,71},{40,41,72,73},{..., dimensions={0}, use_global_device_ids=true | all-gather | bytes 655360 | tf_op jit(solution)/shard_map/all_gather | solution.py:225
  271.2 8.9 %shard_map.94 = (bf16[64,1024]{1,0:T(8,128)(2,1)S(1)}, f32[8,128,128]{2,1,0:T(8,128)S(1)}) custom-call(s32[4]{0:T(128)S(1)} %add_add_fusion.6.flags, bf16[4,64,1024]{2,1,0:T(8,128)(2,1)S(1)} %bitcast.97, f32[1,2048]{1,0:T(1,128)S(1)} %bitcast.78, bf16[16,2048,256]{2,1,0:T(8,128)(2,1)S(1)} %shard_map.91.weights, ...), custom_call_target="tpu_custom_call", output_to_operand_aliasing={{1}: (7, {})} | custom-call | flops 1073741824 | bytes 16777216 | tf_op jit(solution)/shard_map/pallas_call | solution.py:132
  280.1 7.3 %all-gather.6 = bf16[256,1024]{1,0:T(8,128)(2,1)S(1)} all-gather(bf16[64,1024]{1,0:T(8,128)(2,1)S(1)} %get-tuple-element.52), channel_id=8, replica_groups={{0,1,32,33},{2,3,34,35},{4,5,36,37},{6,7,38,39},{8,9,40,41},{10,11,42,4..., dimensions={0}, use_global_device_ids=true | all-gather | bytes 655360 | tf_op jit(solution)/shard_map/all_gather | solution.py:225
  287.4 8.9 %shard_map.95 = (bf16[64,1024]{1,0:T(8,128)(2,1)S(1)}, f32[8,128,128]{2,1,0:T(8,128)S(1)}) custom-call(s32[4]{0:T(128)S(1)} %fusion.6.flags, bf16[4,64,1024]{2,1,0:T(8,128)(2,1)S(1)} %bitcast.98, f32[1,2048]{1,0:T(1,128)S(1)} %bitcast.79, bf16[16,2048,256]{2,1,0:T(8,128)(2,1)S(1)} %shard_map.91.weights, ...), custom_call_target="tpu_custom_call", output_to_operand_aliasing={{1}: (7, {})} | custom-call | flops 1073741824 | bytes 16777216 | tf_op jit(solution)/shard_map/pallas_call | solution.py:132
  296.3 7.3 %all-gather.7 = bf16[256,1024]{1,0:T(8,128)(2,1)S(1)} all-gather(bf16[64,1024]{1,0:T(8,128)(2,1)S(1)} %broadcast_select_fusion.7), channel_id=9, replica_groups={{32,33,64,65},{34,35,66,67},{36,37,68,69},{38,39,70,71},{40,41,72,73},{..., dimensions={0}, use_global_device_ids=true | all-gather | bytes 655360 | tf_op jit(solution)/shard_map/all_gather | solution.py:225
  303.6 8.9 %shard_map.96 = (bf16[64,1024]{1,0:T(8,128)(2,1)S(1)}, f32[8,128,128]{2,1,0:T(8,128)S(1)}) custom-call(s32[4]{0:T(128)S(1)} %add_add_fusion.5.flags, bf16[4,64,1024]{2,1,0:T(8,128)(2,1)S(1)} %bitcast.99, f32[1,2048]{1,0:T(1,128)S(1)} %bitcast.80, bf16[16,2048,256]{2,1,0:T(8,128)(2,1)S(1)} %shard_map.91.weights, ...), custom_call_target="tpu_custom_call", output_to_operand_aliasing={{1}: (7, {})} | custom-call | flops 1073741824 | bytes 16777216 | tf_op jit(solution)/shard_map/pallas_call | solution.py:132
  312.5 7.5 %all-gather.8 = bf16[256,1024]{1,0:T(8,128)(2,1)S(1)} all-gather(bf16[64,1024]{1,0:T(8,128)(2,1)S(1)} %get-tuple-element.56), channel_id=10, replica_groups={{0,1,32,33},{2,3,34,35},{4,5,36,37},{6,7,38,39},{8,9,40,41},{10,11,42,4..., dimensions={0}, use_global_device_ids=true | all-gather | bytes 655360 | tf_op jit(solution)/shard_map/all_gather | solution.py:225
  320.0 8.9 %shard_map.97 = (bf16[64,1024]{1,0:T(8,128)(2,1)S(1)}, f32[8,128,128]{2,1,0:T(8,128)S(1)}) custom-call(s32[4]{0:T(128)S(1)} %fusion.5.flags, bf16[4,64,1024]{2,1,0:T(8,128)(2,1)S(1)} %bitcast.100, f32[1,2048]{1,0:T(1,128)S(1)} %bitcast.81, bf16[16,2048,256]{2,1,0:T(8,128)(2,1)S(1)} %shard_map.91.weights, ...), custom_call_target="tpu_custom_call", output_to_operand_aliasing={{1}: (7, {})} | custom-call | flops 1073741824 | bytes 16777216 | tf_op jit(solution)/shard_map/pallas_call | solution.py:132
  328.9 7.3 %all-gather.9 = bf16[256,1024]{1,0:T(8,128)(2,1)S(1)} all-gather(bf16[64,1024]{1,0:T(8,128)(2,1)S(1)} %broadcast_select_fusion.6), channel_id=11, replica_groups={{32,33,64,65},{34,35,66,67},{36,37,68,69},{38,39,70,71},{40,41,72,73},{..., dimensions={0}, use_global_device_ids=true | all-gather | bytes 655360 | tf_op jit(solution)/shard_map/all_gather | solution.py:225
  336.2 8.9 %shard_map.98 = (bf16[64,1024]{1,0:T(8,128)(2,1)S(1)}, f32[8,128,128]{2,1,0:T(8,128)S(1)}) custom-call(s32[4]{0:T(128)S(1)} %add_add_fusion.4.flags, bf16[4,64,1024]{2,1,0:T(8,128)(2,1)S(1)} %bitcast.101, f32[1,2048]{1,0:T(1,128)S(1)} %bitcast.82, bf16[16,2048,256]{2,1,0:T(8,128)(2,1)S(1)} %shard_map.91.weights, ...), custom_call_target="tpu_custom_call", output_to_operand_aliasing={{1}: (7, {})} | custom-call | flops 1073741824 | bytes 16777216 | tf_op jit(solution)/shard_map/pallas_call | solution.py:132
  345.1 7.3 %all-gather.10 = bf16[256,1024]{1,0:T(8,128)(2,1)S(1)} all-gather(bf16[64,1024]{1,0:T(8,128)(2,1)S(1)} %get-tuple-element.60), channel_id=12, replica_groups={{0,1,32,33},{2,3,34,35},{4,5,36,37},{6,7,38,39},{8,9,40,41},{10,11,42,4..., dimensions={0}, use_global_device_ids=true | all-gather | bytes 655360 | tf_op jit(solution)/shard_map/all_gather | solution.py:225
  352.4 8.9 %shard_map.99 = (bf16[64,1024]{1,0:T(8,128)(2,1)S(1)}, f32[8,128,128]{2,1,0:T(8,128)S(1)}) custom-call(s32[4]{0:T(128)S(1)} %fusion.4.flags, bf16[4,64,1024]{2,1,0:T(8,128)(2,1)S(1)} %bitcast.102, f32[1,2048]{1,0:T(1,128)S(1)} %bitcast.83, bf16[16,2048,256]{2,1,0:T(8,128)(2,1)S(1)} %shard_map.91.weights, ...), custom_call_target="tpu_custom_call", output_to_operand_aliasing={{1}: (7, {})} | custom-call | flops 1073741824 | bytes 16777216 | tf_op jit(solution)/shard_map/pallas_call | solution.py:132
  361.3 7.3 %all-gather.11 = bf16[256,1024]{1,0:T(8,128)(2,1)S(1)} all-gather(bf16[64,1024]{1,0:T(8,128)(2,1)S(1)} %broadcast_select_fusion.5), channel_id=13, replica_groups={{32,33,64,65},{34,35,66,67},{36,37,68,69},{38,39,70,71},{40,41,72,73},{..., dimensions={0}, use_global_device_ids=true | all-gather | bytes 655360 | tf_op jit(solution)/shard_map/all_gather | solution.py:225
  368.6 8.9 %shard_map.100 = (bf16[64,1024]{1,0:T(8,128)(2,1)S(1)}, f32[8,128,128]{2,1,0:T(8,128)S(1)}) custom-call(s32[4]{0:T(128)S(1)} %add_add_fusion.3.flags, bf16[4,64,1024]{2,1,0:T(8,128)(2,1)S(1)} %bitcast.103, f32[1,2048]{1,0:T(1,128)S(1)} %bitcast.84, bf16[16,2048,256]{2,1,0:T(8,128)(2,1)S(1)} %shard_map.91.weights, ...), custom_call_target="tpu_custom_call", output_to_operand_aliasing={{1}: (7, {})} | custom-call | flops 1073741824 | bytes 16777216 | tf_op jit(solution)/shard_map/pallas_call | solution.py:132
  377.5 7.3 %all-gather.12 = bf16[256,1024]{1,0:T(8,128)(2,1)S(1)} all-gather(bf16[64,1024]{1,0:T(8,128)(2,1)S(1)} %get-tuple-element.64), channel_id=14, replica_groups={{0,1,32,33},{2,3,34,35},{4,5,36,37},{6,7,38,39},{8,9,40,41},{10,11,42,4..., dimensions={0}, use_global_device_ids=true | all-gather | bytes 655360 | tf_op jit(solution)/shard_map/all_gather | solution.py:225
  384.8 8.9 %shard_map.101 = (bf16[64,1024]{1,0:T(8,128)(2,1)S(1)}, f32[8,128,128]{2,1,0:T(8,128)S(1)}) custom-call(s32[4]{0:T(128)S(1)} %fusion.3.flags, bf16[4,64,1024]{2,1,0:T(8,128)(2,1)S(1)} %bitcast.104, f32[1,2048]{1,0:T(1,128)S(1)} %bitcast.85, bf16[16,2048,256]{2,1,0:T(8,128)(2,1)S(1)} %shard_map.91.weights, ...), custom_call_target="tpu_custom_call", output_to_operand_aliasing={{1}: (7, {})} | custom-call | flops 1073741824 | bytes 16777216 | tf_op jit(solution)/shard_map/pallas_call | solution.py:132
  393.7 7.3 %all-gather.13 = bf16[256,1024]{1,0:T(8,128)(2,1)S(1)} all-gather(bf16[64,1024]{1,0:T(8,128)(2,1)S(1)} %broadcast_select_fusion.4), channel_id=15, replica_groups={{32,33,64,65},{34,35,66,67},{36,37,68,69},{38,39,70,71},{40,41,72,73},{..., dimensions={0}, use_global_device_ids=true | all-gather | bytes 655360 | tf_op jit(solution)/shard_map/all_gather | solution.py:225
  401.0 8.9 %shard_map.102 = (bf16[64,1024]{1,0:T(8,128)(2,1)S(1)}, f32[8,128,128]{2,1,0:T(8,128)S(1)}) custom-call(s32[4]{0:T(128)S(1)} %add_add_fusion.2.flags, bf16[4,64,1024]{2,1,0:T(8,128)(2,1)S(1)} %bitcast.105, f32[1,2048]{1,0:T(1,128)S(1)} %bitcast.86, bf16[16,2048,256]{2,1,0:T(8,128)(2,1)S(1)} %shard_map.91.weights, ...), custom_call_target="tpu_custom_call", output_to_operand_aliasing={{1}: (7, {})} | custom-call | flops 1073741824 | bytes 16777216 | tf_op jit(solution)/shard_map/pallas_call | solution.py:132
  409.9 7.3 %all-gather.14 = bf16[256,1024]{1,0:T(8,128)(2,1)S(1)} all-gather(bf16[64,1024]{1,0:T(8,128)(2,1)S(1)} %get-tuple-element.68), channel_id=16, replica_groups={{0,1,32,33},{2,3,34,35},{4,5,36,37},{6,7,38,39},{8,9,40,41},{10,11,42,4..., dimensions={0}, use_global_device_ids=true | all-gather | bytes 655360 | tf_op jit(solution)/shard_map/all_gather | solution.py:225
  417.2 8.9 %shard_map.103 = (bf16[64,1024]{1,0:T(8,128)(2,1)S(1)}, f32[8,128,128]{2,1,0:T(8,128)S(1)}) custom-call(s32[4]{0:T(128)S(1)} %fusion.2.flags, bf16[4,64,1024]{2,1,0:T(8,128)(2,1)S(1)} %bitcast.106, f32[1,2048]{1,0:T(1,128)S(1)} %bitcast.87, bf16[16,2048,256]{2,1,0:T(8,128)(2,1)S(1)} %shard_map.91.weights, ...), custom_call_target="tpu_custom_call", output_to_operand_aliasing={{1}: (7, {})} | custom-call | flops 1073741824 | bytes 16777216 | tf_op jit(solution)/shard_map/pallas_call | solution.py:132
  426.1 7.3 %all-gather.15 = bf16[256,1024]{1,0:T(8,128)(2,1)S(1)} all-gather(bf16[64,1024]{1,0:T(8,128)(2,1)S(1)} %broadcast_select_fusion.3), channel_id=17, replica_groups={{32,33,64,65},{34,35,66,67},{36,37,68,69},{38,39,70,71},{40,41,72,73},{..., dimensions={0}, use_global_device_ids=true | all-gather | bytes 655360 | tf_op jit(solution)/shard_map/all_gather | solution.py:225
  433.4 8.9 %shard_map.104 = (bf16[64,1024]{1,0:T(8,128)(2,1)S(1)}, f32[8,128,128]{2,1,0:T(8,128)S(1)}) custom-call(s32[4]{0:T(128)S(1)} %add_add_fusion.1.flags, bf16[4,64,1024]{2,1,0:T(8,128)(2,1)S(1)} %bitcast.107, f32[1,2048]{1,0:T(1,128)S(1)} %bitcast.88, bf16[16,2048,256]{2,1,0:T(8,128)(2,1)S(1)} %shard_map.91.weights, ...), custom_call_target="tpu_custom_call", output_to_operand_aliasing={{1}: (7, {})} | custom-call | flops 1073741824 | bytes 16777216 | tf_op jit(solution)/shard_map/pallas_call | solution.py:132
  442.3 8.1 %all-gather.16 = bf16[256,1024]{1,0:T(8,128)(2,1)S(1)} all-gather(bf16[64,1024]{1,0:T(8,128)(2,1)S(1)} %get-tuple-element.72), channel_id=18, replica_groups={{0,1,32,33},{2,3,34,35},{4,5,36,37},{6,7,38,39},{8,9,40,41},{10,11,42,4..., dimensions={0}, use_global_device_ids=true | all-gather | bytes 655360 | tf_op jit(solution)/shard_map/all_gather | solution.py:225
  450.4 8.9 %shard_map.105 = (bf16[64,1024]{1,0:T(8,128)(2,1)S(1)}, f32[8,128,128]{2,1,0:T(8,128)S(1)}) custom-call(s32[4]{0:T(128)S(1)} %fusion.1.flags, bf16[4,64,1024]{2,1,0:T(8,128)(2,1)S(1)} %bitcast.108, f32[1,2048]{1,0:T(1,128)S(1)} %bitcast.89, bf16[16,2048,256]{2,1,0:T(8,128)(2,1)S(1)} %shard_map.91.weights, ...), custom_call_target="tpu_custom_call", output_to_operand_aliasing={{1}: (7, {})} | custom-call | flops 1073741824 | bytes 16777216 | tf_op jit(solution)/shard_map/pallas_call | solution.py:132
  459.3 7.5 %all-gather.17 = bf16[256,1024]{1,0:T(8,128)(2,1)S(1)} all-gather(bf16[64,1024]{1,0:T(8,128)(2,1)S(1)} %broadcast_select_fusion.2), channel_id=19, replica_groups={{32,33,64,65},{34,35,66,67},{36,37,68,69},{38,39,70,71},{40,41,72,73},{..., dimensions={0}, use_global_device_ids=true | all-gather | bytes 655360 | tf_op jit(solution)/shard_map/all_gather | solution.py:225
  466.8 8.9 %shard_map.106 = (bf16[64,1024]{1,0:T(8,128)(2,1)S(1)}, f32[8,128,128]{2,1,0:T(8,128)S(1)}) custom-call(s32[4]{0:T(128)S(1)} %add_add_fusion.flags, bf16[4,64,1024]{2,1,0:T(8,128)(2,1)S(1)} %bitcast.109, f32[1,2048]{1,0:T(1,128)S(1)} %bitcast.90, bf16[16,2048,256]{2,1,0:T(8,128)(2,1)S(1)} %shard_map.91.weights, ...), custom_call_target="tpu_custom_call", output_to_operand_aliasing={{1}: (7, {})} | custom-call | flops 1073741824 | bytes 16777216 | tf_op jit(solution)/shard_map/pallas_call | solution.py:132
  475.7 8.5 %all-gather.18 = bf16[256,1024]{1,0:T(8,128)(2,1)S(1)} all-gather(bf16[64,1024]{1,0:T(8,128)(2,1)S(1)} %get-tuple-element.76), channel_id=20, replica_groups={{0,1,32,33},{2,3,34,35},{4,5,36,37},{6,7,38,39},{8,9,40,41},{10,11,42,4..., dimensions={0}, use_global_device_ids=true | all-gather | bytes 655360 | tf_op jit(solution)/shard_map/all_gather | solution.py:225
  484.2 8.9 %shard_map.107 = (bf16[64,1024]{1,0:T(8,128)(2,1)S(1)}, f32[8,128,128]{2,1,0:T(8,128)S(1)}) custom-call(s32[4]{0:T(128)S(1)} %fusion.flags, bf16[4,64,1024]{2,1,0:T(8,128)(2,1)S(1)} %bitcast.110, f32[1,2048]{1,0:T(1,128)S(1)} %bitcast.91, bf16[16,2048,256]{2,1,0:T(8,128)(2,1)S(1)} %shard_map.91.weights, ...), custom_call_target="tpu_custom_call", output_to_operand_aliasing={{1}: (7, {})} | custom-call | flops 1073741824 | bytes 16777216 | tf_op jit(solution)/shard_map/pallas_call | solution.py:132
  493.2 7.3 %all-gather.19 = bf16[256,1024]{1,0:T(8,128)(2,1)S(1)} all-gather(bf16[64,1024]{1,0:T(8,128)(2,1)S(1)} %broadcast_select_fusion.1), channel_id=21, replica_groups={{32,33,64,65},{34,35,66,67},{36,37,68,69},{38,39,70,71},{40,41,72,73},{..., dimensions={0}, use_global_device_ids=true | all-gather | bytes 655360 | tf_op jit(solution)/shard_map/all_gather | solution.py:225
  500.4 8.9 %shard_map.108 = (bf16[64,1024]{1,0:T(8,128)(2,1)S(1)}, f32[8,128,128]{2,1,0:T(8,128)S(1)}) custom-call(s32[4]{0:T(128)S(1)} %add_add_fusion.8.flags, bf16[4,64,1024]{2,1,0:T(8,128)(2,1)S(1)} %bitcast.111, f32[1,2048]{1,0:T(1,128)S(1)} %bitcast.92, bf16[16,2048,256]{2,1,0:T(8,128)(2,1)S(1)} %shard_map.91.weights, ...), custom_call_target="tpu_custom_call", output_to_operand_aliasing={{1}: (7, {})} | custom-call | flops 1073741824 | bytes 16777216 | tf_op jit(solution)/shard_map/pallas_call | solution.py:132
  509.4 8.5 %all-gather.20 = bf16[256,1024]{1,0:T(8,128)(2,1)S(1)} all-gather(bf16[64,1024]{1,0:T(8,128)(2,1)S(1)} %get-tuple-element.80), channel_id=22, replica_groups={{0,1,32,33},{2,3,34,35},{4,5,36,37},{6,7,38,39},{8,9,40,41},{10,11,42,4..., dimensions={0}, use_global_device_ids=true | all-gather | bytes 655360 | tf_op jit(solution)/shard_map/all_gather | solution.py:225
  517.8 8.9 %shard_map.109 = (bf16[64,1024]{1,0:T(8,128)(2,1)S(1)}, f32[8,128,128]{2,1,0:T(8,128)S(1)}) custom-call(s32[4]{0:T(128)S(1)} %fusion.8.flags, bf16[4,64,1024]{2,1,0:T(8,128)(2,1)S(1)} %bitcast.95, f32[1,2048]{1,0:T(1,128)S(1)} %bitcast.93, bf16[16,2048,256]{2,1,0:T(8,128)(2,1)S(1)} %shard_map.91.weights, ...), custom_call_target="tpu_custom_call", output_to_operand_aliasing={{1}: (7, {})} | custom-call | flops 1073741824 | bytes 16777216 | tf_op jit(solution)/shard_map/pallas_call | solution.py:132
  528.4 0.9 reshape.57
  529.3 22.4 %all-to-all-start = ((bf16[16,2,2048]{2,1,0:T(2,128)(2,1)}), bf16[16,2,2048]{2,1,0:T(2,128)(2,1)S(1)}, u32[]{:S(2)}, u32[]{:S(2)}) async-start(bf16[16,2,2048]{2,1,0:T(2,128)(2,1)} %reshape.57), calls=%async_computation | async-start | bytes 262144 | tf_op jit(solution)/shard_map/all_to_all | solution.py:248
  551.8 14.7 %all-to-all-done = bf16[16,2,2048]{2,1,0:T(2,128)(2,1)S(1)} async-done(((bf16[16,2,2048]{2,1,0:T(2,128)(2,1)}), bf16[16,2,2048]{2,1,0:T(2,128)(2,1)S(1)}, u32[]{:S(2)}, u32[]{:S(2)}) %all-to-all-start) | async-done | bytes 131104 | tf_op jit(solution)/shard_map/all_to_all | solution.py:248
  (64 shorter events, 9.1 us)
Async XLA Ops:
  6.5 226.2 %all-gather.23.cloned.1.call-start = ((), (), s32[]{:S(2)}) async-start(), calls=%async_computation.1 | async-start | bytes 17825792 | tf_op jit(solution)/shard_map/all_gather | solution.py:184
  8.4 0.8 collective-permute-start.3
  47.7 64.6 %collective-permute-start.1 = (bf16[64,1024]{1,0:T(8,128)(2,1)S(1)}, bf16[64,1024]{1,0:T(8,128)(2,1)S(1)}, u32[]{:S(2)}, u32[]{:S(2)}) collective-permute-start(bf16[64,1024]{1,0:T(8,128)(2,1)S(1)} %reshape.25), channel_id=1, source_target_pairs={{0,0},{1,1},{68,4},{69,5},{136,8},{137,9},{204,12},{205,13},{272,1... | collective-permute-start | bytes 393224 | tf_op jit(solution)/shard_map/ppermute | solution.py:209
  48.4 215.3 %collective-permute-start = (bf16[64,1024]{1,0:T(8,128)(2,1)S(1)}, bf16[64,1024]{1,0:T(8,128)(2,1)S(1)}, u32[]{:S(2)}, u32[]{:S(2)}) collective-permute-start(bf16[64,1024]{1,0:T(8,128)(2,1)S(1)} %reshape.25), channel_id=1, source_target_pairs={{32,0},{33,1},{100,4},{101,5},{168,8},{169,9},{236,12},{237,13},{3... | collective-permute-start | bytes 393224 | tf_op jit(solution)/shard_map/ppermute | solution.py:209
  49.9 4.1 collective-permute-start.2
  526.7 1.4 collective-permute-start.5
  527.4 0.7 collective-permute-start.4
  529.3 37.2 %all-to-all-start = ((bf16[16,2,2048]{2,1,0:T(2,128)(2,1)}), bf16[16,2,2048]{2,1,0:T(2,128)(2,1)S(1)}, u32[]{:S(2)}, u32[]{:S(2)}) async-start(bf16[16,2,2048]{2,1,0:T(2,128)(2,1)} %reshape.57), calls=%async_computation | async-start | bytes 262144 | tf_op jit(solution)/shard_map/all_to_all | solution.py:248
Sparse Core Ops, SparseCore 0:
  10.4 222.2 all-gather.22

commit v3 on v2

v3 whole, which is shorter than its diff:
```python
import functools

import jax
import jax.numpy as jnp
from jax import lax
from jax.experimental import pallas as pl
from jax.experimental.pallas import tpu as pltpu
from jax.sharding import PartitionSpec as P

HEAD = 64
SEG = 64
EPSILON = 1e-06
NT = (((1,), (1,)), ((), ()))
NN = (((1,), (0,)), ((), ()))
TN = (((0,), (0,)), ((), ()))
ABREAST = 8


def section_kernel(
    slot,
    got,
    gain,
    weights,
    edge,
    spike,
    out_gain,
    state_in,
    keys_in,
    values_in,
    result,
    state,
    last_keys,
    last_values,
    scaled,
    product,
):
    line = lax.axis_index("pp")
    core = lax.axis_index("tp") % 2
    first = (line == slot).astype(jnp.int32)
    pairs = weights.shape[0] // 2

    @pl.when(line == slot - 1)
    def _():
        at = lax.broadcasted_iota(jnp.int32, (128, 128), 0) < HEAD
        of = lax.broadcasted_iota(jnp.int32, (128, 128), 1) < HEAD
        for pair in range(pairs):
            carried = lax.dot_general(last_keys[pair], last_values[pair], TN, preferred_element_type=jnp.float32)
            state[pair] = jnp.where(at == of, carried, 0.0)

    @pl.when((line == slot) | (line == slot - 2))
    def _():
        run_section(
            first, core, got, gain, weights, edge, spike, out_gain, result, state, last_keys, last_values, scaled, product
        )


def run_section(
    first, core, got, gain, weights, edge, spike, out_gain, result, state, last_keys, last_values, scaled, product
):
    rows, width = got.shape[1:]
    heads = weights.shape[0]
    low = lax.broadcasted_iota(jnp.int32, (rows, 128), 1) < HEAD

    total = jnp.zeros((rows, 128), jnp.float32)
    for tile in range(width // 128):
        columns = pl.ds(tile * 128, 128)
        even = got[0, :, columns].astype(jnp.float32)
        odd = got[1, :, columns].astype(jnp.float32)
        total = total + even * even + odd * odd
        left = jnp.where(low, even, pltpu.roll(odd, HEAD, 1))
        right = jnp.where(low, pltpu.roll(even, HEAD, 1), odd)
        for step, wide in enumerate((left, right)):
            columns = pl.ds((2 * tile + step) * 128, 128)
            scaled[:, columns] = (wide * gain[:, columns]).astype(jnp.bfloat16)
    total = jnp.sum(total, axis=1, keepdims=True)
    scale = jnp.broadcast_to(lax.rsqrt(total / (2 * width) + EPSILON), (rows, 128))

    at = lax.broadcasted_iota(jnp.int32, (rows, 2 * rows), 0)
    of = lax.broadcasted_iota(jnp.int32, (rows, 2 * rows), 1)
    ones = jnp.where(at >= jnp.where(of >= rows, of - rows, of), 1.0, 0.0).astype(jnp.bfloat16)
    at = lax.broadcasted_iota(jnp.int32, (2 * rows, rows), 0)
    of = lax.broadcasted_iota(jnp.int32, (2 * rows, rows), 1)
    causal = jnp.where(at >= rows, at - rows, at) >= of
    same = (lax.broadcasted_iota(jnp.int32, (128, 128), 0) < HEAD) == (
        lax.broadcasted_iota(jnp.int32, (128, 128), 1) < HEAD
    )
    mean = jnp.where(same, 1.0 / HEAD, 0.0).astype(jnp.bfloat16)

    def multiply(head, _):
        product[head] = lax.dot_general(scaled[...], weights[head], NN, preferred_element_type=jnp.float32)
        return 0

    lax.fori_loop(0, heads, multiply, 0, unroll=4)

    def several(index, _):
        pairs = [ABREAST * index + step for step in range(ABREAST)]
        queries, keys, forgets, values, gates = [], [], [], [], []
        for pair in pairs:
            tiles = [product[2 * pair + k // 2, :, 128 * (k % 2) : 128 * (k % 2) + 128] * scale for k in range(4)]
            rolled = [pltpu.roll(tile, HEAD, 1) for tile in tiles]
            query_pre = jnp.where(low, tiles[0], rolled[2])
            forget_pre = jnp.where(low, rolled[0], tiles[2])
            gate_pre = jnp.where(low, rolled[1], tiles[3])
            values.append(jnp.where(low, tiles[1], rolled[3]).astype(jnp.bfloat16))
            gates.append(gate_pre * jax.nn.sigmoid(gate_pre) * out_gain[...])
            queries.append(query_pre * jax.nn.sigmoid(query_pre))
            lower = edge[pair]
            upper = 1.0 - lower
            opposite = jnp.exp(jnp.minimum(-forget_pre, 80.0))
            kept = 1.0 / (1.0 + opposite)
            forgets.append(jnp.log(lower + upper * kept) + spike[1 - first, pair])
            keys.append(upper * (opposite * kept))

        running = []
        for step in range(0, ABREAST, 2):
            wide = jnp.concatenate(forgets[step : step + 2], axis=1)
            high = wide.astype(jnp.bfloat16)
            rest = (wide - high.astype(jnp.float32)).astype(jnp.bfloat16)
            wide = lax.dot_general(
                ones, jnp.concatenate([high, rest], axis=0), NN, preferred_element_type=jnp.float32
            )
            running += [wide[:, :128], wide[:, 128:]]

        squares, mixes = [], []
        for step, pair in enumerate(pairs):
            query_scaled = queries[step] * jnp.exp(running[step])
            key_scaled = (keys[step] * jnp.exp(-running[step])).astype(jnp.bfloat16)
            stacked = jnp.concatenate(
                [jnp.where(low, query_scaled, 0.0), jnp.where(low, 0.0, query_scaled)], axis=0
            ).astype(jnp.bfloat16)
            scores = lax.dot_general(stacked, key_scaled, NT, preferred_element_type=jnp.float32)
            scores = jnp.where(causal, scores, 0.0).astype(jnp.bfloat16)
            before = jnp.where(first == 1, 0.0, state[pair]).astype(jnp.bfloat16)
            both = lax.dot_general(
                jnp.concatenate([stacked, scores], axis=1),
                jnp.concatenate([before, values[step]], axis=0),
                NN,
                preferred_element_type=jnp.float32,
            )
            mixed = jnp.where(low, both[:rows], both[rows:])
            mixes.append(mixed)
            squares.append((mixed * mixed).astype(jnp.bfloat16))
            ending = running[step][rows - 1 :, :]
            last_keys[pair] = (keys[step] * jnp.exp(ending - running[step])).astype(jnp.bfloat16)
            last_values[pair] = values[step]

        average = lax.dot_general(
            jnp.concatenate(squares, axis=0), mean, NN, preferred_element_type=jnp.float32
        )
        for step, pair in enumerate(pairs):
            inverse = lax.rsqrt(average[rows * step : rows * step + rows] + EPSILON)
            columns = pl.ds(pl.multiple_of(pair * 128, 128), 128)
            own = got[core, :, columns].astype(jnp.float32)
            result[:, columns] = (own + mixes[step] * inverse * gates[step]).astype(jnp.bfloat16)
        return 0

    lax.fori_loop(0, heads // 2 // ABREAST, several, 0)


def hold_kernel(source, held, semaphores):
    copies = [
        pltpu.make_async_copy(source.at[head], held.at[head], semaphores.at[head]) for head in range(source.shape[0])
    ]
    for copy in copies:
        copy.start()
    for copy in copies:
        copy.wait()


def hold(weights):
    return pl.pallas_call(
        hold_kernel,
        out_shape=pltpu.VMEM(weights.shape, weights.dtype),
        in_specs=[pl.BlockSpec(memory_space=pltpu.HBM)],
        out_specs=pl.BlockSpec(memory_space=pltpu.VMEM),
        scratch_shapes=[pltpu.SemaphoreType.DMA((weights.shape[0],))],
        compiler_params=pltpu.CompilerParams(vmem_limit_bytes=1 << 20),
        cost_estimate=pl.CostEstimate(flops=0, bytes_accessed=4 * weights.size, transcendentals=0),
    )(weights)


def section(slot, got, gain, weights, edge, spike, out_gain, kept):
    rows, width = got.shape[1:]
    return pl.pallas_call(
        functools.partial(section_kernel, slot),
        out_shape=(
            jax.ShapeDtypeStruct((rows, width), jnp.bfloat16),
        )
        + tuple(jax.ShapeDtypeStruct(array.shape, array.dtype) for array in kept),
        in_specs=[pl.BlockSpec(memory_space=pltpu.VMEM)] * 9,
        out_specs=[pl.BlockSpec(memory_space=pltpu.VMEM)] * 4,
        scratch_shapes=[
            pltpu.VMEM((rows, 2 * width), jnp.bfloat16),
            pltpu.VMEM((weights.shape[0], rows, weights.shape[2]), jnp.float32),
        ],
        input_output_aliases={6: 1, 7: 2, 8: 3},
        compiler_params=pltpu.CompilerParams(vmem_limit_bytes=24 << 20),
        cost_estimate=pl.CostEstimate(
            flops=2 * rows * weights.size, bytes_accessed=2 * weights.size, transcendentals=0
        ),
    )(got, gain, weights, edge, spike, out_gain, *kept)


def shards(
    entry_stream_rows,
    layer_rescale_factor,
    probe_projection,
    retention_projection,
    candidate_projection,
    emission_filter_matrix,
    retention_minimum,
    decay_spike,
    per_group_scale,
):
    sections = lax.axis_size("pp")
    members = lax.axis_size("tp")
    chips = members // 2
    line = lax.axis_index("pp")
    half_width = layer_rescale_factor.shape[1] // 2
    pairs = chips // 2
    same_core = [[c + 2 * z for z in range(chips)] for c in range(2)]

    local = jnp.stack(
        [probe_projection[0], retention_projection[0], candidate_projection[0], emission_filter_matrix[0]]
    )
    local = local.reshape(4 * HEAD, 2 * half_width).T
    weights = lax.all_gather(local, "tp", axis_index_groups=same_core)
    weights = hold(pltpu.with_memory_space_constraint(weights, pltpu.HBM))
    small = jnp.concatenate(
        [layer_rescale_factor[0], per_group_scale[0], retention_minimum[0], decay_spike[0, :, 0]]
    )
    gain = small[None, : 2 * half_width]
    out_gain = jnp.tile(small[None, 2 * half_width : 2 * half_width + HEAD], (1, 2))
    small = lax.all_gather(small[2 * half_width + HEAD :], "tp", axis_index_groups=same_core)
    edge = small[:, :HEAD].reshape(pairs, 1, 128)
    spike = small[:, HEAD:].reshape(pairs, 2, 2, SEG)
    spike = jnp.broadcast_to(spike.transpose(2, 0, 3, 1)[..., None], (2, pairs, SEG, 2, HEAD))
    spike = spike.reshape(2, pairs, SEG, 128)
    gain, out_gain, edge, spike = lax.optimization_barrier((gain, out_gain, edge, spike))

    def gathered_line(block):
        whole = lax.all_gather(block, "tp", axis_index_groups=same_core)
        return whole.transpose(1, 0, 2).reshape(block.shape[0], half_width)

    def between(array, pairs_of):
        moves = [
            (a * members + t, b * members + t)
            for a, b, z in pairs_of
            for t in (2 * z, 2 * z + 1)
        ]
        return lax.ppermute(array, ("pp", "tp"), moves)

    micro = sections // 2
    entering = gathered_line(entry_stream_rows)
    entry = [between(entering, [(2 * k + u, 0, 2 * k) for k in range(micro)]) for u in range(2)]

    def groups(slot):
        paired, found = set(), []
        for unit in range(2):
            a, b = slot - 2 * unit - 1, slot - 2 * unit
            if a >= 0 and b < sections:
                paired |= {a, b}
                found += [[l * members + 2 * z + c for l in (a, b) for c in range(2)] for z in range(chips)]
        for l in range(sections):
            if l not in paired:
                found += [[l * members + 4 * z + t for t in range(4)] for z in range(pairs)]
        return found

    current = jnp.zeros((SEG, half_width), jnp.bfloat16)
    kept = (jnp.zeros((pairs, 128, 128), jnp.float32),) + (jnp.zeros((pairs, SEG, 128), jnp.bfloat16),) * 2
    finished = []
    for slot in range(sections + 2):
        if slot in (0, 2):
            current = jnp.where(line == 0, entry[slot // 2], current)
        got = lax.all_gather(current, ("pp", "tp"), axis_index_groups=groups(slot))
        current, *kept = section(slot, got, gain, weights, edge, spike, out_gain, kept)
        if slot in (sections - 1, sections + 1):
            unit = len(finished)
            finished.append(between(current, [(sections - 1, 2 * k + unit, 2 * k) for k in range(micro)]))
    mine = jnp.where(line % 2 == 0, finished[0], finished[1])
    spread = mine.reshape(SEG, chips, HEAD).transpose(1, 0, 2)
    received = lax.all_to_all(spread, "tp", 0, 0, axis_index_groups=same_core)
    return lax.dynamic_index_in_dim(received, line // 2 * 2, 0, keepdims=False)


def solution(mesh):
    in_specs = (
        P("pp", "tp"),
        P("pp", None),
        P("pp", "tp", None),
        P("pp", "tp", None),
        P("pp", "tp", None),
        P("pp", "tp", None),
        P("pp", "tp"),
        P("pp", None, "tp"),
        P("pp", None),
    )
    out_specs = P("pp", "tp")
    return jax.shard_map(shards, mesh=mesh, in_specs=in_specs, out_specs=out_specs, check_vma=False)
```

time: 575 us -> 465 us (0.81); the launches traced: 574 us -> 456 us
  Pallas kernels: 166 us -> 16.3 us
  starting transfers between devices: 26.5 us -> 50.8 us
  blocking collectives: 259 us -> 265 us
    pallas_call x18, Pallas kernels: 160 us -> 10.3 us  [section(): pl.pallas_call(functools.partial(section_kernel, slot), out_shape=(jax.Sh...]
    all_to_all x1, starting transfers between devices: 22.4 us -> 48.1 us  [shards(): received = lax.all_to_all(spread, 'tp', 0, 0, axis_index_groups=same_core)]
  transfers between devices with their start and end apart: 8 -> 6, of which waited for: 2 -> 2; matrix products, arithmetic and copies ran while one was open for 1% -> 1% of each run, Pallas kernels for 4% -> 1%
where the time goes in v3:
time: 465 us; the launch traced here: 456 us
  blocking collectives  265 us (57%)
  waiting for transfers between devices  99 us (21%)
  starting transfers between devices  50.8 us (11%)
  Pallas kernels  16.3 us (4%)
  between operations  14.8 us (3%)
  local copies, waits for them, and re-layouts  8.1 us (2%)
    all_gather x18, blocking collectives, shards(): got = lax.all_gather(current, ('pp', 'tp'), axis_index_groups=groups(slot))  170 us
    all_gather x1, waiting for transfers between devices, shards(): weights = lax.all_gather(local, 'tp', axis_index_groups=same_core)  84.2 us
    unnamed x1, blocking collectives  55.9 us
    all_to_all x1, starting transfers between devices, shards(): received = lax.all_to_all(spread, 'tp', 0, 0, axis_index_groups=same_core)  48.1 us
    all_gather x1, blocking collectives, gathered_line(): whole = lax.all_gather(block, 'tp', axis_index_groups=same_core)  39 us
    all_to_all x1, waiting for transfers between devices, shards(): received = lax.all_to_all(spread, 'tp', 0, 0, axis_index_groups=same_core)  14.7 us
    pallas_call x18, Pallas kernels, section(): pl.pallas_call(functools.partial(section_kernel, slot), out_shape=(jax.Sh...  10.3 us
  transfers between devices with their start and end apart: 6, of which 2 were waited for; matrix products, arithmetic and copies ran while one was open for 1% of the time, Pallas kernels for 1%

profile of v3, /device:TPU:16, one launch (start us, length us, event | category | flops | bytes accessed | tf_op | source)
XLA Modules:
  0.0 456.4 jit_solution(7869946253671439968)
XLA Ops:
  6.5 1.3 pad_maximum_fusion
  7.9 1.3 copy.69
  9.2 39.0 %all-gather = bf16[1024,64]{1,0:T(8,128)(2,1)S(1)} all-gather(bf16[64,64]{1,0:T(8,128)(2,1)} %param.9), channel_id=2, replica_groups={{0,2,4,6,8,10,12,14,16,18,20,22,24,26,28,30},{1,3,5,7,9,11,13,15,17,19,..., dimensions={0}, use_global_device_ids=true | all-gather | bytes 139264 | tf_op jit(solution)/shard_map/all_gather | solution.py:242
  48.2 0.2 copy.74
  48.4 0.2 reshape.25
  48.6 0.7 collective-permute-start.1
  49.3 0.7 collective-permute-start
  50.0 1.3 dynamic-slice
  51.9 0.9 maximum_dynamic-update-slice_fusion
  52.8 55.9 %all-reduce = f32[3072]{0:T(1024)S(1)} all-reduce(f32[3072]{0:T(1024)S(1)} %maximum_dynamic-update-slice_fusion), channel_id=4, replica_groups={{0,2,4,6,8,10,12,14,16,18,20,22,24,26,28,30},{1,3,5,7,9,11,13,15,17,19,..., use_global_device_ids=true, to_apply=%add | all-reduce | flops 3072 | bytes 24576
  109.0 0.2 copy.68
  109.2 1.2 broadcast_in_dim.16
  110.5 0.6 reshape.28.spike
  111.1 0.7 tile.11
  111.8 0.1 tile.12.out_gain
  111.9 10.2 %all-gather.1 = bf16[256,1024]{1,0:T(8,128)(2,1)S(1)} all-gather(bf16[64,1024]{1,0:T(8,128)(2,1)S(1)} %broadcast_select_fusion.1), channel_id=3, replica_groups={{0,1,2,3},{4,5,6,7},{8,9,10,11},{12,13,14,15},{16,17,18,19},{20,21,22,2..., dimensions={0}, use_global_device_ids=true | all-gather | bytes 655360 | tf_op jit(solution)/shard_map/all_gather | solution.py:275
  122.1 84.2 %all-gather.23.cloned.1.call-done = bf16[32768,256]{1,0:T(8,128)(2,1)} async-done(((bf16[2048,256]{1,0:T(8,128)(2,1)}), bf16[32768,256]{1,0:T(8,128)(2,1)}) %all-gather.23.cloned.1.call-update) | async-done | bytes 16777232 | tf_op jit(solution)/shard_map/all_gather | solution.py:227
  206.3 5.9 %shard_map.91.weights = bf16[16,2048,256]{2,1,0:T(8,128)(2,1)S(1)} custom-call(bf16[16,2048,256]{2,1,0:T(8,128)(2,1)} %bitcast.53), custom_call_target="tpu_custom_call" | custom-call | bytes 33554432 | tf_op jit(solution)/shard_map/pallas_call | solution.py:171
  212.4 6.8 %all-gather.4 = bf16[256,1024]{1,0:T(8,128)(2,1)S(1)} all-gather(bf16[64,1024]{1,0:T(8,128)(2,1)S(1)} %get-tuple-element.82), channel_id=6, replica_groups={{0,1,32,33},{2,3,34,35},{4,5,36,37},{6,7,38,39},{8,9,40,41},{10,11,42,4..., dimensions={0}, use_global_device_ids=true | all-gather | bytes 655360 | tf_op jit(solution)/shard_map/all_gather | solution.py:275
  219.3 7.3 %all-gather.5 = bf16[256,1024]{1,0:T(8,128)(2,1)S(1)} all-gather(bf16[64,1024]{1,0:T(8,128)(2,1)S(1)} %broadcast_select_fusion), channel_id=7, replica_groups={{32,33,64,65},{34,35,66,67},{36,37,68,69},{38,39,70,71},{40,41,72,73},{..., dimensions={0}, use_global_device_ids=true | all-gather | bytes 655360 | tf_op jit(solution)/shard_map/all_gather | solution.py:275
  226.6 7.3 %all-gather.6 = bf16[256,1024]{1,0:T(8,128)(2,1)S(1)} all-gather(bf16[64,1024]{1,0:T(8,128)(2,1)S(1)} %get-tuple-element.90), channel_id=8, replica_groups={{64,65,96,97},{66,67,98,99},{68,69,100,101},{70,71,102,103},{72,73,104,..., dimensions={0}, use_global_device_ids=true | all-gather | bytes 655360 | tf_op jit(solution)/shard_map/all_gather | solution.py:275
  233.8 7.3 %all-gather.7 = bf16[256,1024]{1,0:T(8,128)(2,1)S(1)} all-gather(bf16[64,1024]{1,0:T(8,128)(2,1)S(1)} %get-tuple-element.94), channel_id=9, replica_groups={{96,97,128,129},{98,99,130,131},{100,101,132,133},{102,103,134,135},{10..., dimensions={0}, use_global_device_ids=true | all-gather | bytes 655360 | tf_op jit(solution)/shard_map/all_gather | solution.py:275
  241.1 0.2 shard_map.96
  241.2 7.3 %all-gather.8 = bf16[256,1024]{1,0:T(8,128)(2,1)S(1)} all-gather(bf16[64,1024]{1,0:T(8,128)(2,1)S(1)} %get-tuple-element.98), channel_id=10, replica_groups={{128,129,160,161},{130,131,162,163},{132,133,164,165},{134,135,166,167}..., dimensions={0}, use_global_device_ids=true | all-gather | bytes 655360 | tf_op jit(solution)/shard_map/all_gather | solution.py:275
  248.5 7.3 %all-gather.9 = bf16[256,1024]{1,0:T(8,128)(2,1)S(1)} all-gather(bf16[64,1024]{1,0:T(8,128)(2,1)S(1)} %get-tuple-element.102), channel_id=11, replica_groups={{160,161,192,193},{162,163,194,195},{164,165,196,197},{166,167,198,199}..., dimensions={0}, use_global_device_ids=true | all-gather | bytes 655360 | tf_op jit(solution)/shard_map/all_gather | solution.py:275
  255.8 7.3 %all-gather.10 = bf16[256,1024]{1,0:T(8,128)(2,1)S(1)} all-gather(bf16[64,1024]{1,0:T(8,128)(2,1)S(1)} %get-tuple-element.106), channel_id=12, replica_groups={{192,193,224,225},{194,195,226,227},{196,197,228,229},{198,199,230,231}..., dimensions={0}, use_global_device_ids=true | all-gather | bytes 655360 | tf_op jit(solution)/shard_map/all_gather | solution.py:275
  263.1 42.1 %all-gather.11 = bf16[256,1024]{1,0:T(8,128)(2,1)S(1)} all-gather(bf16[64,1024]{1,0:T(8,128)(2,1)S(1)} %get-tuple-element.110), channel_id=13, replica_groups={{224,225,256,257},{226,227,258,259},{228,229,260,261},{230,231,262,263}..., dimensions={0}, use_global_device_ids=true | all-gather | bytes 655360 | tf_op jit(solution)/shard_map/all_gather | solution.py:275
  305.1 4.7 %shard_map.100 = (bf16[64,1024]{1,0:T(8,128)(2,1)S(1)}, f32[8,128,128]{2,1,0:T(8,128)S(1)}, bf16[8,64,128]{2,1,0:T(8,128)(2,1)S(1)}, bf16[8,64,128]{2,1,0:T(8,128)(2,1)S(1)}) custom-call(bf16[4,64,1024]{2,1,0:T(8,128)(2,1)S(1)} %bitcast.44, f32[1,2048]{1,0:T(1,128)S(1)} %copy-done, ...), custom_call_target="tpu_custom_call", output_to_operand_aliasing={{1}: (6, {}), {2}: (7, {}), {3}: (8, {})} | custom-call | flops 1073741824 | bytes 16777216 | tf_op jit(solution)/shard_map/pallas_call | solution.py:184
  309.9 7.3 %all-gather.12 = bf16[256,1024]{1,0:T(8,128)(2,1)S(1)} all-gather(bf16[64,1024]{1,0:T(8,128)(2,1)S(1)} %get-tuple-element.114), channel_id=14, replica_groups={{256,257,288,289},{258,259,290,291},{260,261,292,293},{262,263,294,295}..., dimensions={0}, use_global_device_ids=true | all-gather | bytes 655360 | tf_op jit(solution)/shard_map/all_gather | solution.py:275
  317.1 0.5 shard_map.101
  317.6 9.4 %all-gather.13 = bf16[256,1024]{1,0:T(8,128)(2,1)S(1)} all-gather(bf16[64,1024]{1,0:T(8,128)(2,1)S(1)} %get-tuple-element.118), channel_id=15, replica_groups={{288,289,320,321},{290,291,322,323},{292,293,324,325},{294,295,326,327}..., dimensions={0}, use_global_device_ids=true | all-gather | bytes 655360 | tf_op jit(solution)/shard_map/all_gather | solution.py:275
  327.0 4.7 %shard_map.102 = (bf16[64,1024]{1,0:T(8,128)(2,1)S(1)}, f32[8,128,128]{2,1,0:T(8,128)S(1)}, bf16[8,64,128]{2,1,0:T(8,128)(2,1)S(1)}, bf16[8,64,128]{2,1,0:T(8,128)(2,1)S(1)}) custom-call(bf16[4,64,1024]{2,1,0:T(8,128)(2,1)S(1)} %bitcast.46, f32[1,2048]{1,0:T(1,128)S(1)} %copy-done, ...), custom_call_target="tpu_custom_call", output_to_operand_aliasing={{1}: (6, {}), {2}: (7, {}), {3}: (8, {})} | custom-call | flops 1073741824 | bytes 16777216 | tf_op jit(solution)/shard_map/pallas_call | solution.py:184
  331.7 7.3 %all-gather.14 = bf16[256,1024]{1,0:T(8,128)(2,1)S(1)} all-gather(bf16[64,1024]{1,0:T(8,128)(2,1)S(1)} %get-tuple-element.122), channel_id=16, replica_groups={{320,321,352,353},{322,323,354,355},{324,325,356,357},{326,327,358,359}..., dimensions={0}, use_global_device_ids=true | all-gather | bytes 655360 | tf_op jit(solution)/shard_map/all_gather | solution.py:275
  339.0 7.3 %all-gather.15 = bf16[256,1024]{1,0:T(8,128)(2,1)S(1)} all-gather(bf16[64,1024]{1,0:T(8,128)(2,1)S(1)} %get-tuple-element.126), channel_id=17, replica_groups={{352,353,384,385},{354,355,386,387},{356,357,388,389},{358,359,390,391}..., dimensions={0}, use_global_device_ids=true | all-gather | bytes 655360 | tf_op jit(solution)/shard_map/all_gather | solution.py:275
  346.3 7.3 %all-gather.16 = bf16[256,1024]{1,0:T(8,128)(2,1)S(1)} all-gather(bf16[64,1024]{1,0:T(8,128)(2,1)S(1)} %get-tuple-element.130), channel_id=18, replica_groups={{384,385,416,417},{386,387,418,419},{388,389,420,421},{390,391,422,423}..., dimensions={0}, use_global_device_ids=true | all-gather | bytes 655360 | tf_op jit(solution)/shard_map/all_gather | solution.py:275
  353.5 7.3 %all-gather.17 = bf16[256,1024]{1,0:T(8,128)(2,1)S(1)} all-gather(bf16[64,1024]{1,0:T(8,128)(2,1)S(1)} %get-tuple-element.134), channel_id=19, replica_groups={{416,417,448,449},{418,419,450,451},{420,421,452,453},{422,423,454,455}..., dimensions={0}, use_global_device_ids=true | all-gather | bytes 655360 | tf_op jit(solution)/shard_map/all_gather | solution.py:275
  360.8 0.2 shard_map.106
  361.1 7.3 %all-gather.18 = bf16[256,1024]{1,0:T(8,128)(2,1)S(1)} all-gather(bf16[64,1024]{1,0:T(8,128)(2,1)S(1)} %get-tuple-element.138), channel_id=20, replica_groups={{448,449,480,481},{450,451,482,483},{452,453,484,485},{454,455,486,487}..., dimensions={0}, use_global_device_ids=true | all-gather | bytes 655360 | tf_op jit(solution)/shard_map/all_gather | solution.py:275
  368.3 7.3 %all-gather.19 = bf16[256,1024]{1,0:T(8,128)(2,1)S(1)} all-gather(bf16[64,1024]{1,0:T(8,128)(2,1)S(1)} %get-tuple-element.142), channel_id=21, replica_groups={{416,417,448,449},{418,419,450,451},{420,421,452,453},{422,423,454,455}..., dimensions={0}, use_global_device_ids=true | all-gather | bytes 655360 | tf_op jit(solution)/shard_map/all_gather | solution.py:275
  375.6 7.3 %all-gather.20 = bf16[256,1024]{1,0:T(8,128)(2,1)S(1)} all-gather(bf16[64,1024]{1,0:T(8,128)(2,1)S(1)} %get-tuple-element.146), channel_id=22, replica_groups={{448,449,480,481},{450,451,482,483},{452,453,484,485},{454,455,486,487}..., dimensions={0}, use_global_device_ids=true | all-gather | bytes 655360 | tf_op jit(solution)/shard_map/all_gather | solution.py:275
  382.9 0.7 collective-permute-start.3
  383.5 0.7 collective-permute-start.2
  384.3 0.2 reshape.30
  384.5 0.9 reshape.57
  385.4 48.1 %all-to-all-start = ((bf16[16,2,2048]{2,1,0:T(2,128)(2,1)}), bf16[16,2,2048]{2,1,0:T(2,128)(2,1)S(1)}, u32[]{:S(2)}, u32[]{:S(2)}) async-start(bf16[16,2,2048]{2,1,0:T(2,128)(2,1)} %reshape.57), calls=%async_computation | async-start | bytes 262144 | tf_op jit(solution)/shard_map/all_to_all | solution.py:282
  433.6 14.7 %all-to-all-done = bf16[16,2,2048]{2,1,0:T(2,128)(2,1)S(1)} async-done(((bf16[16,2,2048]{2,1,0:T(2,128)(2,1)}), bf16[16,2,2048]{2,1,0:T(2,128)(2,1)S(1)}, u32[]{:S(2)}, u32[]{:S(2)}) %all-to-all-start) | async-done | bytes 131104 | tf_op jit(solution)/shard_map/all_to_all | solution.py:282
  448.3 0.2 reshape.58
  448.5 0.6 dynamic-slice_bitcast_fusion
  (34 shorter events, 0.6 us)
Async XLA Ops:
  6.5 199.8 %all-gather.23.cloned.1.call-start = ((), (), s32[]{:S(2)}) async-start(), calls=%async_computation.1 | async-start | bytes 17825792 | tf_op jit(solution)/shard_map/all_gather | solution.py:227
  48.6 63.2 %collective-permute-start.1 = (bf16[64,1024]{1,0:T(8,128)(2,1)S(1)}, bf16[64,1024]{1,0:T(8,128)(2,1)S(1)}, u32[]{:S(2)}, u32[]{:S(2)}) collective-permute-start(bf16[64,1024]{1,0:T(8,128)(2,1)S(1)} %reshape.25), channel_id=1, source_target_pairs={{0,0},{1,1},{68,4},{69,5},{136,8},{137,9},{204,12},{205,13},{272,1... | collective-permute-start | bytes 393224 | tf_op jit(solution)/shard_map/ppermute | solution.py:251
  49.3 169.9 %collective-permute-start = (bf16[64,1024]{1,0:T(8,128)(2,1)S(1)}, bf16[64,1024]{1,0:T(8,128)(2,1)S(1)}, u32[]{:S(2)}, u32[]{:S(2)}) collective-permute-start(bf16[64,1024]{1,0:T(8,128)(2,1)S(1)} %reshape.25), channel_id=1, source_target_pairs={{32,0},{33,1},{100,4},{101,5},{168,8},{169,9},{236,12},{237,13},{3... | collective-permute-start | bytes 393224 | tf_op jit(solution)/shard_map/ppermute | solution.py:251
  206.3 6.0 %copy-start = (f32[1,2048]{1,0:T(1,128)S(1)}, f32[1,2048]{1,0:T(1,128)}, u32[]{:S(2)}) copy-start(f32[1,2048]{1,0:T(1,128)} %gain.17) | copy-start | bytes 24580
  382.9 1.4 collective-permute-start.3
  383.5 0.7 collective-permute-start.2
  385.4 62.9 %all-to-all-start = ((bf16[16,2,2048]{2,1,0:T(2,128)(2,1)}), bf16[16,2,2048]{2,1,0:T(2,128)(2,1)S(1)}, u32[]{:S(2)}, u32[]{:S(2)}) async-start(bf16[16,2,2048]{2,1,0:T(2,128)(2,1)} %reshape.57), calls=%async_computation | async-start | bytes 262144 | tf_op jit(solution)/shard_map/all_to_all | solution.py:282
Sparse Core Ops, SparseCore 0:
  9.4 196.8 all-gather.22

commit v4 on v3

--- a/solution.py
+++ b/solution.py
@@ -28,6 +28,7 @@
     keys_in,
     values_in,
     result,
+    weights_out,
     state,
     last_keys,
     last_values,
@@ -157,26 +158,72 @@
     lax.fori_loop(0, heads // 2 // ABREAST, several, 0)
 
 
-def hold_kernel(source, held, semaphores):
-    copies = [
-        pltpu.make_async_copy(source.at[head], held.at[head], semaphores.at[head]) for head in range(source.shape[0])
-    ]
-    for copy in copies:
-        copy.start()
-    for copy in copies:
-        copy.wait()
-
-
-def hold(weights):
+def hold_kernel(skipped, count, plan, *refs):
+    sources, target, semaphores = refs[skipped : skipped + count], refs[skipped + count], refs[-1]
+    row = lax.axis_index("pp") // 4
+    for rows, moves in plan:
+        wanted = row == rows[0]
+        for other in rows[1:]:
+            wanted = wanted | (row == other)
+
+        @pl.when(wanted)
+        def _():
+            copies = []
+            for index, quarter in moves:
+                source = sources[index]
+                depth = source.shape[1]
+                for head in range(source.shape[0]):
+                    copies.append(
+                        pltpu.make_async_copy(
+                            source.at[head],
+                            target.at[head, pl.ds(quarter * depth, depth)],
+                            semaphores.at[quarter * source.shape[0] + head],
+                        )
+                    )
+            for copy in copies:
+                copy.start()
+            for copy in copies:
+                copy.wait()
+
+
+def hold(plan, sources, before=None, after=None, along=None):
+    heads, depth, columns = sources[0].shape
+    sources = [pltpu.with_memory_space_constraint(source, pltpu.HBM) for source in sources]
+    extra = [array for array in (before, after, along) if array is not None]
+    held = pltpu.VMEM((heads, 4 * depth, columns), sources[0].dtype)
+    outputs = (held,) if along is None else (held, jax.ShapeDtypeStruct(along.shape, along.dtype))
+    aliases = {} if before is None else {0: 0}
+    if along is not None:
+        aliases[len(extra) - 1] = 1
+    results = pl.pallas_call(
+        functools.partial(hold_kernel, len(extra), len(sources), plan),
+        out_shape=outputs,
+        in_specs=[pl.BlockSpec(memory_space=pltpu.VMEM)] * len(extra)
+        + [pl.BlockSpec(memory_space=pltpu.HBM)] * len(sources),
+        out_specs=[pl.BlockSpec(memory_space=pltpu.VMEM)] * len(outputs),
+        scratch_shapes=[pltpu.SemaphoreType.DMA((4 * heads,))],
+        input_output_aliases=aliases,
+        compiler_params=pltpu.CompilerParams(vmem_limit_bytes=24 << 20),
+        cost_estimate=pl.CostEstimate(
+            flops=0, bytes_accessed=4 * len(sources) * sources[0].size, transcendentals=0
+        ),
+    )(*extra, *sources)
+    return results[0] if along is None else results
+
+
+def gate_kernel(*refs):
+    pass
+
+
+def gate(array, after):
     return pl.pallas_call(
-        hold_kernel,
-        out_shape=pltpu.VMEM(weights.shape, weights.dtype),
-        in_specs=[pl.BlockSpec(memory_space=pltpu.HBM)],
-        out_specs=pl.BlockSpec(memory_space=pltpu.VMEM),
-        scratch_shapes=[pltpu.SemaphoreType.DMA((weights.shape[0],))],
+        gate_kernel,
+        out_shape=pltpu.HBM(array.shape, array.dtype),
+        in_specs=[pl.BlockSpec(memory_space=pltpu.HBM), pl.BlockSpec(memory_space=pl.ANY)],
+        out_specs=pl.BlockSpec(memory_space=pltpu.HBM),
+        input_output_aliases={0: 0},
         compiler_params=pltpu.CompilerParams(vmem_limit_bytes=1 << 20),
-        cost_estimate=pl.CostEstimate(flops=0, bytes_accessed=4 * weights.size, transcendentals=0),
-    )(weights)
+    )(pltpu.with_memory_space_constraint(array, pltpu.HBM), after)
 
 
 def section(slot, got, gain, weights, edge, spike, out_gain, kept):
@@ -185,15 +232,16 @@
         functools.partial(section_kernel, slot),
         out_shape=(
             jax.ShapeDtypeStruct((rows, width), jnp.bfloat16),
+            pltpu.VMEM(weights.shape, weights.dtype),
         )
         + tuple(jax.ShapeDtypeStruct(array.shape, array.dtype) for array in kept),
         in_specs=[pl.BlockSpec(memory_space=pltpu.VMEM)] * 9,
-        out_specs=[pl.BlockSpec(memory_space=pltpu.VMEM)] * 4,
+        out_specs=[pl.BlockSpec(memory_space=pltpu.VMEM)] * 5,
         scratch_shapes=[
             pltpu.VMEM((rows, 2 * width), jnp.bfloat16),
             pltpu.VMEM((weights.shape[0], rows, weights.shape[2]), jnp.float32),
         ],
-        input_output_aliases={6: 1, 7: 2, 8: 3},
+        input_output_aliases={2: 1, 6: 2, 7: 3, 8: 4},
         compiler_params=pltpu.CompilerParams(vmem_limit_bytes=24 << 20),
         cost_estimate=pl.CostEstimate(
             flops=2 * rows * weights.size, bytes_accessed=2 * weights.size, transcendentals=0
@@ -224,23 +272,47 @@
         [probe_projection[0], retention_projection[0], candidate_projection[0], emission_filter_matrix[0]]
     )
     local = local.reshape(4 * HEAD, 2 * half_width).T
-    weights = lax.all_gather(local, "tp", axis_index_groups=same_core)
-    weights = hold(pltpu.with_memory_space_constraint(weights, pltpu.HBM))
-    small = jnp.concatenate(
-        [layer_rescale_factor[0], per_group_scale[0], retention_minimum[0], decay_spike[0, :, 0]]
+    quarters = jnp.split(local, 4)
+    row = line // 4
+    last = sections // 4 - 1
+    down = [(x * members + t, (last * 4 + x) * members + t) for x in range(4) for t in range(members)]
+    up = [(b, a) for a, b in down]
+    swapped = lax.ppermute(quarters[3], ("pp", "tp"), down + up)
+    same_lines = [[l * members + t for t in same_core[c]] for l in range(sections) for c in range(2)]
+    blocks = []
+    for index in range(4):
+        ours = jnp.where(row == last, swapped if index == 0 else quarters[index - 1], quarters[index])
+        if index == 3:
+            started = pltpu.with_memory_space_constraint(blocks[0], pltpu.HBM)
+            ours = gate(jnp.where(row == 0, swapped, ours), started)
+        turned = same_lines[index:] + same_lines[:index]
+        blocks.append(lax.all_gather(ours, ("pp", "tp"), axis_index_groups=turned))
+    up = [(b, a) for b, a in up if a % members % 4 < 2]
+    down = [(a, b) for a, b in down if a % members % 4 < 2]
+    returned = lax.ppermute(blocks[0], ("pp", "tp"), up)
+    whole_plan = list(enumerate(range(4)))
+    weights = hold([((0,), whole_plan)], blocks[:3] + [returned])
+    gain = layer_rescale_factor
+    out_gain = jnp.tile(per_group_scale, (1, 2))
+    rest = jnp.concatenate([retention_minimum[0], decay_spike[0, :, 0]])
+    parts = []
+    for _ in range(3):
+        part = lax.reduce_precision(rest, 8, 7)
+        parts.append(part.astype(jnp.bfloat16))
+        rest = rest - part
+    parts = jnp.concatenate(parts).reshape(-1, HEAD)
+    extra = parts.shape[0]
+    padding = jnp.zeros((16 - extra, HEAD), jnp.bfloat16)
+    whole = lax.all_gather(
+        jnp.concatenate([entry_stream_rows, parts, padding]), "tp", axis_index_groups=same_core
     )
-    gain = small[None, : 2 * half_width]
-    out_gain = jnp.tile(small[None, 2 * half_width : 2 * half_width + HEAD], (1, 2))
-    small = lax.all_gather(small[2 * half_width + HEAD :], "tp", axis_index_groups=same_core)
+    entering = whole[:, :SEG].transpose(1, 0, 2).reshape(SEG, half_width)
+    small = whole[:, SEG : SEG + extra].astype(jnp.float32).reshape(chips, 3, 3 * HEAD).sum(axis=1)
     edge = small[:, :HEAD].reshape(pairs, 1, 128)
     spike = small[:, HEAD:].reshape(pairs, 2, 2, SEG)
     spike = jnp.broadcast_to(spike.transpose(2, 0, 3, 1)[..., None], (2, pairs, SEG, 2, HEAD))
     spike = spike.reshape(2, pairs, SEG, 128)
     gain, out_gain, edge, spike = lax.optimization_barrier((gain, out_gain, edge, spike))
-
-    def gathered_line(block):
-        whole = lax.all_gather(block, "tp", axis_index_groups=same_core)
-        return whole.transpose(1, 0, 2).reshape(block.shape[0], half_width)
 
     def between(array, pairs_of):
         moves = [
@@ -251,7 +323,6 @@
         return lax.ppermute(array, ("pp", "tp"), moves)
 
     micro = sections // 2
-    entering = gathered_line(entry_stream_rows)
     entry = [between(entering, [(2 * k + u, 0, 2 * k) for k in range(micro)]) for u in range(2)]
 
     def groups(slot):
@@ -272,8 +343,18 @@
     for slot in range(sections + 2):
         if slot in (0, 2):
             current = jnp.where(line == 0, entry[slot // 2], current)
+        if slot == 4:
+            blocks[3] = gate(blocks[3], current)
+            weights, current = hold(
+                [((1, 2), whole_plan), ((3,), [(1, 0), (2, 1), (3, 2)])], blocks, along=current
+            )
+            sent = lax.ppermute(blocks[3], ("pp", "tp"), down)
+        if slot == 12:
+            weights = hold([((3,), [(0, 3)])], [sent], before=weights)
         got = lax.all_gather(current, ("pp", "tp"), axis_index_groups=groups(slot))
-        current, *kept = section(slot, got, gain, weights, edge, spike, out_gain, kept)
+        if slot == 4:
+            weights = hold([((0,), whole_plan)], blocks[:3] + [returned], before=weights, after=got)
+        current, weights, *kept = section(slot, got, gain, weights, edge, spike, out_gain, kept)
         if slot in (sections - 1, sections + 1):
             unit = len(finished)
             finished.append(between(current, [(sections - 1, 2 * k + unit, 2 * k) for k in range(micro)]))

time: 465 us -> 559 us (1.20)
  waiting for transfers between devices: 99 us -> 264 us
  blocking collectives: 265 us -> 191 us
    all_gather x1 -> x4, waiting for transfers between devices: 84.2 us -> 248 us  [shards(): blocks.append(lax.all_gather(ours, ('pp', 'tp'), axis_index_groups=turned))]
    unnamed x1 -> x0, blocking collectives: 55.9 us -> none
    all_gather x18, blocking collectives: 170 us -> 160 us  [shards(): got = lax.all_gather(current, ('pp', 'tp'), axis_index_groups=groups(slot))]
    all_gather x1, blocking collectives: 39 us -> 31 us  [shards(): lax.all_gather(jnp.concatenate([entry_stream_rows, parts, padding]), 'tp'...]
  transfers between devices with their start and end apart: 6 -> 12, of which waited for: 2 -> 5; matrix products, arithmetic and copies ran while one was open for 1% -> 1% of each run, Pallas kernels for 1% -> 3%
where the time goes in v4:
time: 559 us; the launch traced here: 551 us
  waiting for transfers between devices  264 us (47%)
  blocking collectives  191 us (34%)
  starting transfers between devices  51.7 us (9%)
  Pallas kernels  18.4 us (3%)
  between operations  14 us (3%)
  local copies, waits for them, and re-layouts  8.86 us (2%)
    all_gather x4, waiting for transfers between devices, shards(): blocks.append(lax.all_gather(ours, ('pp', 'tp'), axis_index_groups=turned))  248 us
    all_gather x18, blocking collectives, shards(): got = lax.all_gather(current, ('pp', 'tp'), axis_index_groups=groups(slot))  160 us
    all_to_all x1, starting transfers between devices, shards(): received = lax.all_to_all(spread, 'tp', 0, 0, axis_index_groups=same_core)  44.8 us
    all_gather x1, blocking collectives, shards(): lax.all_gather(jnp.concatenate([entry_stream_rows, parts, padding]), 'tp'...  31 us
    all_to_all x1, waiting for transfers between devices, shards(): received = lax.all_to_all(spread, 'tp', 0, 0, axis_index_groups=same_core)  14.7 us
  transfers between devices with their start and end apart: 12, of which 5 were waited for; matrix products, arithmetic and copies ran while one was open for 1% of the time, Pallas kernels for 3%

profile of v4, /device:TPU:16, one launch (start us, length us, event | category | flops | bytes accessed | tf_op | source)
XLA Modules:
  0.0 551.2 jit_solution(18056607112383421978)
XLA Ops:
  6.5 1.3 pad_maximum_fusion
  8.4 0.7 collective-permute-start.2
  9.1 1.0 select_select_fusion
  10.3 0.7 all-gather.31.cloned.1.call-update
  11.0 0.7 all-gather.33.cloned.1.call-update
  11.7 91.1 %all-gather.29.cloned.1.call-done = bf16[8192,256]{1,0:T(8,128)(2,1)} async-done(((bf16[512,256]{1,0:T(8,128)(2,1)}), bf16[8192,256]{1,0:T(8,128)(2,1)}) %all-gather.29.cloned.1.call-update) | async-done | bytes 4194320 | tf_op jit(solution)/shard_map/all_gather | solution.py:289
  102.9 2.6 collective-permute-start.3
  105.5 0.7 pad_maximum_fusion.1
  106.7 0.8 copy.109
  107.6 31.0 %all-gather.23 = bf16[16,80,64]{1,2,0:T(8,128)(2,1)S(1)} all-gather(bf16[1,80,64]{1,2,0:T(8,128)(2,1)S(1)} %bitcast.75), channel_id=2, replica_groups={{0,2,4,6,8,10,12,14,16,18,20,22,24,26,28,30},{1,3,5,7,9,11,13,15,17,19,..., dimensions={0}, use_global_device_ids=true | all-gather | bytes 174080 | tf_op jit(solution)/shard_map/all_gather | solution.py:306
  138.7 0.7 collective-permute-start.1
  139.4 0.7 collective-permute-start
  141.0 1.2 broadcast_in_dim.20
  142.2 0.6 reshape.43.spike
  143.0 8.8 %all-gather.1 = bf16[256,1024]{1,0:T(8,128)(2,1)S(1)} all-gather(bf16[64,1024]{1,0:T(8,128)(2,1)S(1)} %broadcast_select_fusion.4), channel_id=3, replica_groups={{0,1,2,3},{4,5,6,7},{8,9,10,11},{12,13,14,15},{16,17,18,19},{20,21,22,2..., dimensions={0}, use_global_device_ids=true | all-gather | bytes 655360 | tf_op jit(solution)/shard_map/all_gather | solution.py:354
  151.8 29.4 %all-gather.31.cloned.1.call-done = bf16[8192,256]{1,0:T(8,128)(2,1)} async-done(((bf16[512,256]{1,0:T(8,128)(2,1)}), bf16[8192,256]{1,0:T(8,128)(2,1)}) %all-gather.31.cloned.1.call-update) | async-done | bytes 4194320 | tf_op jit(solution)/shard_map/all_gather | solution.py:289
  181.2 76.0 %all-gather.33.cloned.1.call-done = bf16[8192,256]{1,0:T(8,128)(2,1)} async-done(((bf16[512,256]{1,0:T(8,128)(2,1)}), bf16[8192,256]{1,0:T(8,128)(2,1)}) %all-gather.33.cloned.1.call-update) | async-done | bytes 4194320 | tf_op jit(solution)/shard_map/all_gather | solution.py:289
  257.2 0.6 shard_map.91.weights
  257.9 7.2 %all-gather.5 = bf16[256,1024]{1,0:T(8,128)(2,1)S(1)} all-gather(bf16[64,1024]{1,0:T(8,128)(2,1)S(1)} %get-tuple-element.100), channel_id=7, replica_groups={{0,1,32,33},{2,3,34,35},{4,5,36,37},{6,7,38,39},{8,9,40,41},{10,11,42,4..., dimensions={0}, use_global_device_ids=true | all-gather | bytes 655360 | tf_op jit(solution)/shard_map/all_gather | solution.py:354
  265.2 7.3 %all-gather.6 = bf16[256,1024]{1,0:T(8,128)(2,1)S(1)} all-gather(bf16[64,1024]{1,0:T(8,128)(2,1)S(1)} %broadcast_select_fusion.3), channel_id=8, replica_groups={{32,33,64,65},{34,35,66,67},{36,37,68,69},{38,39,70,71},{40,41,72,73},{..., dimensions={0}, use_global_device_ids=true | all-gather | bytes 655360 | tf_op jit(solution)/shard_map/all_gather | solution.py:354
  272.5 10.0 %all-gather.7 = bf16[256,1024]{1,0:T(8,128)(2,1)S(1)} all-gather(bf16[64,1024]{1,0:T(8,128)(2,1)S(1)} %get-tuple-element.110), channel_id=9, replica_groups={{64,65,96,97},{66,67,98,99},{68,69,100,101},{70,71,102,103},{72,73,104,..., dimensions={0}, use_global_device_ids=true | all-gather | bytes 655360 | tf_op jit(solution)/shard_map/all_gather | solution.py:354
  282.6 51.1 %all-gather.35.cloned.1.call-done = bf16[8192,256]{1,0:T(8,128)(2,1)} async-done(((bf16[512,256]{1,0:T(8,128)(2,1)}), bf16[8192,256]{1,0:T(8,128)(2,1)}) %all-gather.35.cloned.1.call-update) | async-done | bytes 4194320 | tf_op jit(solution)/shard_map/all_gather | solution.py:289
  333.7 0.9 collective-permute-start.4
  334.7 6.3 %shard_map.98 = (bf16[16,2048,256]{2,1,0:T(8,128)(2,1)S(1)}, bf16[64,1024]{1,0:T(8,128)(2,1)S(1)}) custom-call(bf16[64,1024]{1,0:T(8,128)(2,1)S(1)} %get-tuple-element.115.refs_1_.refs_0_, bf16[16,512,256]{2,1,0:T(8,128)(2,1)} %bitcast.60, bf16[16,512,256]{2,1,0:T(8,128)(2,1)} %bitcast.63, ...), custom_call_target="tpu_custom_call", output_to_operand_aliasing={{1}: (0, {})} | custom-call | bytes 33554432 | tf_op jit(solution)/shard_map/pallas_call | solution.py:198
  341.0 7.0 %all-gather.9 = bf16[256,1024]{1,0:T(8,128)(2,1)S(1)} all-gather(bf16[64,1024]{1,0:T(8,128)(2,1)S(1)} %get-tuple-element.116), channel_id=11, replica_groups={{96,97,128,129},{98,99,130,131},{100,101,132,133},{102,103,134,135},{10..., dimensions={0}, use_global_device_ids=true | all-gather | bytes 655360 | tf_op jit(solution)/shard_map/all_gather | solution.py:354
  348.0 0.6 shard_map.99.weights
  348.6 7.3 %all-gather.10 = bf16[256,1024]{1,0:T(8,128)(2,1)S(1)} all-gather(bf16[64,1024]{1,0:T(8,128)(2,1)S(1)} %get-tuple-element.121), channel_id=12, replica_groups={{128,129,160,161},{130,131,162,163},{132,133,164,165},{134,135,166,167}..., dimensions={0}, use_global_device_ids=true | all-gather | bytes 655360 | tf_op jit(solution)/shard_map/all_gather | solution.py:354
  355.9 7.3 %all-gather.11 = bf16[256,1024]{1,0:T(8,128)(2,1)S(1)} all-gather(bf16[64,1024]{1,0:T(8,128)(2,1)S(1)} %get-tuple-element.126), channel_id=13, replica_groups={{160,161,192,193},{162,163,194,195},{164,165,196,197},{166,167,198,199}..., dimensions={0}, use_global_device_ids=true | all-gather | bytes 655360 | tf_op jit(solution)/shard_map/all_gather | solution.py:354
  363.2 7.3 %all-gather.12 = bf16[256,1024]{1,0:T(8,128)(2,1)S(1)} all-gather(bf16[64,1024]{1,0:T(8,128)(2,1)S(1)} %get-tuple-element.131), channel_id=14, replica_groups={{192,193,224,225},{194,195,226,227},{196,197,228,229},{198,199,230,231}..., dimensions={0}, use_global_device_ids=true | all-gather | bytes 655360 | tf_op jit(solution)/shard_map/all_gather | solution.py:354
  370.4 26.1 %all-gather.13 = bf16[256,1024]{1,0:T(8,128)(2,1)S(1)} all-gather(bf16[64,1024]{1,0:T(8,128)(2,1)S(1)} %get-tuple-element.136), channel_id=15, replica_groups={{224,225,256,257},{226,227,258,259},{228,229,260,261},{230,231,262,263}..., dimensions={0}, use_global_device_ids=true | all-gather | bytes 655360 | tf_op jit(solution)/shard_map/all_gather | solution.py:354
  396.6 4.9 shard_map.104
  401.5 7.3 %all-gather.14 = bf16[256,1024]{1,0:T(8,128)(2,1)S(1)} all-gather(bf16[64,1024]{1,0:T(8,128)(2,1)S(1)} %get-tuple-element.141), channel_id=16, replica_groups={{256,257,288,289},{258,259,290,291},{260,261,292,293},{262,263,294,295}..., dimensions={0}, use_global_device_ids=true | all-gather | bytes 655360 | tf_op jit(solution)/shard_map/all_gather | solution.py:354
  409.0 13.8 %all-gather.15 = bf16[256,1024]{1,0:T(8,128)(2,1)S(1)} all-gather(bf16[64,1024]{1,0:T(8,128)(2,1)S(1)} %get-tuple-element.146), channel_id=17, replica_groups={{288,289,320,321},{290,291,322,323},{292,293,324,325},{294,295,326,327}..., dimensions={0}, use_global_device_ids=true | all-gather | bytes 655360 | tf_op jit(solution)/shard_map/all_gather | solution.py:354
  422.9 4.7 shard_map.106
  427.6 7.3 %all-gather.16 = bf16[256,1024]{1,0:T(8,128)(2,1)S(1)} all-gather(bf16[64,1024]{1,0:T(8,128)(2,1)S(1)} %get-tuple-element.151), channel_id=18, replica_groups={{320,321,352,353},{322,323,354,355},{324,325,356,357},{326,327,358,359}..., dimensions={0}, use_global_device_ids=true | all-gather | bytes 655360 | tf_op jit(solution)/shard_map/all_gather | solution.py:354
  434.9 7.3 %all-gather.17 = bf16[256,1024]{1,0:T(8,128)(2,1)S(1)} all-gather(bf16[64,1024]{1,0:T(8,128)(2,1)S(1)} %get-tuple-element.156), channel_id=19, replica_groups={{352,353,384,385},{354,355,386,387},{356,357,388,389},{358,359,390,391}..., dimensions={0}, use_global_device_ids=true | all-gather | bytes 655360 | tf_op jit(solution)/shard_map/all_gather | solution.py:354
  442.1 2.0 copy-done.1
  444.7 7.3 %all-gather.18 = bf16[256,1024]{1,0:T(8,128)(2,1)S(1)} all-gather(bf16[64,1024]{1,0:T(8,128)(2,1)S(1)} %get-tuple-element.161), channel_id=20, replica_groups={{384,385,416,417},{386,387,418,419},{388,389,420,421},{390,391,422,423}..., dimensions={0}, use_global_device_ids=true | all-gather | bytes 655360 | tf_op jit(solution)/shard_map/all_gather | solution.py:354
  452.3 7.3 %all-gather.19 = bf16[256,1024]{1,0:T(8,128)(2,1)S(1)} all-gather(bf16[64,1024]{1,0:T(8,128)(2,1)S(1)} %get-tuple-element.166), channel_id=21, replica_groups={{416,417,448,449},{418,419,450,451},{420,421,452,453},{422,423,454,455}..., dimensions={0}, use_global_device_ids=true | all-gather | bytes 655360 | tf_op jit(solution)/shard_map/all_gather | solution.py:354
  459.5 7.3 %all-gather.20 = bf16[256,1024]{1,0:T(8,128)(2,1)S(1)} all-gather(bf16[64,1024]{1,0:T(8,128)(2,1)S(1)} %get-tuple-element.171), channel_id=22, replica_groups={{448,449,480,481},{450,451,482,483},{452,453,484,485},{454,455,486,487}..., dimensions={0}, use_global_device_ids=true | all-gather | bytes 655360 | tf_op jit(solution)/shard_map/all_gather | solution.py:354
  466.8 7.3 %all-gather.21 = bf16[256,1024]{1,0:T(8,128)(2,1)S(1)} all-gather(bf16[64,1024]{1,0:T(8,128)(2,1)S(1)} %get-tuple-element.176), channel_id=23, replica_groups={{416,417,448,449},{418,419,450,451},{420,421,452,453},{422,423,454,455}..., dimensions={0}, use_global_device_ids=true | all-gather | bytes 655360 | tf_op jit(solution)/shard_map/all_gather | solution.py:354
  474.1 7.3 %all-gather.22 = bf16[256,1024]{1,0:T(8,128)(2,1)S(1)} all-gather(bf16[64,1024]{1,0:T(8,128)(2,1)S(1)} %get-tuple-element.181), channel_id=24, replica_groups={{448,449,480,481},{450,451,482,483},{452,453,484,485},{454,455,486,487}..., dimensions={0}, use_global_device_ids=true | all-gather | bytes 655360 | tf_op jit(solution)/shard_map/all_gather | solution.py:354
  481.3 0.7 collective-permute-start.6
  482.0 0.7 collective-permute-start.5
  483.0 0.9 reshape.74
  483.9 44.8 %all-to-all-start = ((bf16[16,2,2048]{2,1,0:T(2,128)(2,1)}), bf16[16,2,2048]{2,1,0:T(2,128)(2,1)S(1)}, u32[]{:S(2)}, u32[]{:S(2)}) async-start(bf16[16,2,2048]{2,1,0:T(2,128)(2,1)} %reshape.74), calls=%async_computation | async-start | bytes 262144 | tf_op jit(solution)/shard_map/all_to_all | solution.py:363
  528.7 14.7 %all-to-all-done = bf16[16,2,2048]{2,1,0:T(2,128)(2,1)S(1)} async-done(((bf16[16,2,2048]{2,1,0:T(2,128)(2,1)}), bf16[16,2,2048]{2,1,0:T(2,128)(2,1)S(1)}, u32[]{:S(2)}, u32[]{:S(2)}) %all-to-all-start) | async-done | bytes 131104 | tf_op jit(solution)/shard_map/all_to_all | solution.py:363
  543.6 0.6 dynamic-slice_bitcast_fusion
  (68 shorter events, 4.3 us)
Async XLA Ops:
  6.5 136.4 %copy-start.2 = (f32[1,64]{1,0:T(1,128)S(1)}, f32[1,64]{1,0:T(1,128)}, u32[]{:S(2)}) copy-start(f32[1,64]{1,0:T(1,128)} %param.17) | copy-start | bytes 772
  6.5 96.3 %all-gather.29.cloned.1.call-start = ((), (), s32[]{:S(2)}) async-start(), calls=%async_computation.1 | async-start | bytes 4456448 | tf_op jit(solution)/shard_map/all_gather | solution.py:289
  8.4 0.7 collective-permute-start.2
  10.2 171.0 %all-gather.31.cloned.1.call-start = ((), (), s32[]{:S(2)}) async-start(), calls=%async_computation.2 | async-start | bytes 4456448 | tf_op jit(solution)/shard_map/all_gather | solution.py:289
  11.0 246.2 %all-gather.33.cloned.1.call-start = ((), (), s32[]{:S(2)}) async-start(), calls=%async_computation.3 | async-start | bytes 4456448 | tf_op jit(solution)/shard_map/all_gather | solution.py:289
  11.7 322.0 %all-gather.35.cloned.1.call-start = ((), (), s32[]{:S(2)}) async-start(), calls=%async_computation.4 | async-start | bytes 4456448 | tf_op jit(solution)/shard_map/all_gather | solution.py:289
  102.9 154.3 %collective-permute-start.3 = (bf16[16,512,256]{2,1,0:T(8,128)(2,1)}, bf16[16,512,256]{2,1,0:T(8,128)(2,1)}, u32[]{:S(2)}, u32[]{:S(2)}) collective-permute-start(bf16[16,512,256]{2,1,0:T(8,128)(2,1)} %bitcast.58), channel_id=1, source_target_pairs={{384,0},{385,1},{388,4},{389,5},{392,8},{393,9},{396,12},{397,13},... | collective-permute-start | bytes 12582920 | tf_op jit(solution)/shard_map/ppermute | solution.py:292
  138.7 4.3 collective-permute-start.1
  139.4 125.7 %collective-permute-start = (bf16[64,1024]{1,0:T(8,128)(2,1)S(1)}, bf16[64,1024]{1,0:T(8,128)(2,1)S(1)}, u32[]{:S(2)}, u32[]{:S(2)}) collective-permute-start(bf16[64,1024]{1,0:T(8,128)(2,1)S(1)} %copy.119), channel_id=1, source_target_pairs={{32,0},{33,1},{100,4},{101,5},{168,8},{169,9},{236,12},{237,13},{3... | collective-permute-start | bytes 393224 | tf_op jit(solution)/shard_map/ppermute | solution.py:323
  257.2 0.7 copy-start
  333.7 108.4 %collective-permute-start.4 = (bf16[16,512,256]{2,1,0:T(8,128)(2,1)}, bf16[16,512,256]{2,1,0:T(8,128)(2,1)S(1)}, u32[]{:S(2)}, u32[]{:S(2)}) collective-permute-start(bf16[16,512,256]{2,1,0:T(8,128)(2,1)} %shard_map.97.refs_4_), channel_id=1, source_target_pairs={{0,384},{1,385},{4,388},{5,389},{8,392},{9,393},{12,396},{13,397},... | collective-permute-start | bytes 12582920 | tf_op jit(solution)/shard_map/ppermute | solution.py:351
  442.1 2.0 copy-start.1
  481.3 1.4 collective-permute-start.6
  482.0 0.7 collective-permute-start.5
  483.9 59.5 %all-to-all-start = ((bf16[16,2,2048]{2,1,0:T(2,128)(2,1)}), bf16[16,2,2048]{2,1,0:T(2,128)(2,1)S(1)}, u32[]{:S(2)}, u32[]{:S(2)}) async-start(bf16[16,2,2048]{2,1,0:T(2,128)(2,1)} %reshape.74), calls=%async_computation | async-start | bytes 262144 | tf_op jit(solution)/shard_map/all_to_all | solution.py:363
Sparse Core Ops, SparseCore 0:
  10.3 92.5 all-gather.28
  105.0 76.1 all-gather.30
  183.3 73.8 all-gather.32
  259.1 74.5 all-gather.34

commit v5 on v3

--- a/solution.py
+++ b/solution.py
@@ -27,13 +27,9 @@
     state_in,
     keys_in,
     values_in,
-    result,
-    state,
-    last_keys,
-    last_values,
-    scaled,
-    product,
+    *others,
 ):
+    result, state, last_keys, last_values, scaled, product = others[-6:]
     line = lax.axis_index("pp")
     core = lax.axis_index("tp") % 2
     first = (line == slot).astype(jnp.int32)
@@ -90,7 +86,7 @@
         product[head] = lax.dot_general(scaled[...], weights[head], NN, preferred_element_type=jnp.float32)
         return 0
 
-    lax.fori_loop(0, heads, multiply, 0, unroll=4)
+    lax.fori_loop(0, heads, multiply, 0, unroll=8)
 
     def several(index, _):
         pairs = [ABREAST * index + step for step in range(ABREAST)]
@@ -179,7 +175,7 @@
     )(weights)
 
 
-def section(slot, got, gain, weights, edge, spike, out_gain, kept):
+def section(slot, got, gain, weights, edge, spike, out_gain, kept, after):
     rows, width = got.shape[1:]
     return pl.pallas_call(
         functools.partial(section_kernel, slot),
@@ -187,7 +183,7 @@
             jax.ShapeDtypeStruct((rows, width), jnp.bfloat16),
         )
         + tuple(jax.ShapeDtypeStruct(array.shape, array.dtype) for array in kept),
-        in_specs=[pl.BlockSpec(memory_space=pltpu.VMEM)] * 9,
+        in_specs=[pl.BlockSpec(memory_space=pltpu.VMEM)] * (9 + len(after)),
         out_specs=[pl.BlockSpec(memory_space=pltpu.VMEM)] * 4,
         scratch_shapes=[
             pltpu.VMEM((rows, 2 * width), jnp.bfloat16),
@@ -198,7 +194,7 @@
         cost_estimate=pl.CostEstimate(
             flops=2 * rows * weights.size, bytes_accessed=2 * weights.size, transcendentals=0
         ),
-    )(got, gain, weights, edge, spike, out_gain, *kept)
+    )(got, gain, weights, edge, spike, out_gain, *kept, *after)
 
 
 def shards(
@@ -226,33 +222,36 @@
     local = local.reshape(4 * HEAD, 2 * half_width).T
     weights = lax.all_gather(local, "tp", axis_index_groups=same_core)
     weights = hold(pltpu.with_memory_space_constraint(weights, pltpu.HBM))
-    small = jnp.concatenate(
-        [layer_rescale_factor[0], per_group_scale[0], retention_minimum[0], decay_spike[0, :, 0]]
+    gain = layer_rescale_factor
+    out_gain = jnp.tile(per_group_scale, (1, 2))
+    rest = jnp.concatenate([retention_minimum[0], decay_spike[0, :, 0]])
+    parts = []
+    for _ in range(3):
+        part = lax.reduce_precision(rest, 8, 7)
+        parts.append(part.astype(jnp.bfloat16))
+        rest = rest - part
+    parts = jnp.concatenate(parts).reshape(-1, HEAD)
+    extra = parts.shape[0]
+    padding = jnp.zeros((16 - extra, HEAD), jnp.bfloat16)
+    whole = lax.all_gather(
+        jnp.concatenate([entry_stream_rows, parts, padding]), "tp", axis_index_groups=same_core
     )
-    gain = small[None, : 2 * half_width]
-    out_gain = jnp.tile(small[None, 2 * half_width : 2 * half_width + HEAD], (1, 2))
-    small = lax.all_gather(small[2 * half_width + HEAD :], "tp", axis_index_groups=same_core)
+    entering = whole[:, :SEG].transpose(1, 0, 2).reshape(SEG, half_width)
+    small = whole[:, SEG : SEG + extra].astype(jnp.float32).reshape(chips, 3, 3 * HEAD).sum(axis=1)
     edge = small[:, :HEAD].reshape(pairs, 1, 128)
     spike = small[:, HEAD:].reshape(pairs, 2, 2, SEG)
     spike = jnp.broadcast_to(spike.transpose(2, 0, 3, 1)[..., None], (2, pairs, SEG, 2, HEAD))
     spike = spike.reshape(2, pairs, SEG, 128)
     gain, out_gain, edge, spike = lax.optimization_barrier((gain, out_gain, edge, spike))
 
-    def gathered_line(block):
-        whole = lax.all_gather(block, "tp", axis_index_groups=same_core)
-        return whole.transpose(1, 0, 2).reshape(block.shape[0], half_width)
-
     def between(array, pairs_of):
         moves = [
-            (a * members + t, b * members + t)
-            for a, b, z in pairs_of
-            for t in (2 * z, 2 * z + 1)
+            (a * members + 2 * z + c, b * members + 2 * y + c) for a, b, z, y in pairs_of for c in range(2)
         ]
         return lax.ppermute(array, ("pp", "tp"), moves)
 
     micro = sections // 2
-    entering = gathered_line(entry_stream_rows)
-    entry = [between(entering, [(2 * k + u, 0, 2 * k) for k in range(micro)]) for u in range(2)]
+    entry = [between(entering, [(2 * k + u, 0, 2 * k, 2 * k) for k in range(micro)]) for u in range(2)]
 
     def groups(slot):
         paired, found = set(), []
@@ -269,18 +268,33 @@
     current = jnp.zeros((SEG, half_width), jnp.bfloat16)
     kept = (jnp.zeros((pairs, 128, 128), jnp.float32),) + (jnp.zeros((pairs, SEG, 128), jnp.bfloat16),) * 2
     finished = []
+    near = 4 * HEAD
     for slot in range(sections + 2):
         if slot in (0, 2):
             current = jnp.where(line == 0, entry[slot // 2], current)
         got = lax.all_gather(current, ("pp", "tp"), axis_index_groups=groups(slot))
-        current, *kept = section(slot, got, gain, weights, edge, spike, out_gain, kept)
+        after = finished[0] if slot == sections + 1 else ()
+        current, *kept = section(slot, got, gain, weights, edge, spike, out_gain, kept, after)
         if slot in (sections - 1, sections + 1):
             unit = len(finished)
-            finished.append(between(current, [(sections - 1, 2 * k + unit, 2 * k) for k in range(micro)]))
-    mine = jnp.where(line % 2 == 0, finished[0], finished[1])
-    spread = mine.reshape(SEG, chips, HEAD).transpose(1, 0, 2)
-    received = lax.all_to_all(spread, "tp", 0, 0, axis_index_groups=same_core)
-    return lax.dynamic_index_in_dim(received, line // 2 * 2, 0, keepdims=False)
+            finished.append(
+                [
+                    between(
+                        current[:, part * near : part * near + near],
+                        [(sections - 1, 2 * k + unit, 2 * k, 2 * k % 4 + 4 * part) for k in range(micro)],
+                    )
+                    for part in range(chips // 4)
+                ]
+            )
+    mine = [jnp.where(line % 2 == 0, even, odd) for even, odd in zip(*finished)]
+    chip = lax.axis_index("tp") // 2
+    held = mine[0]
+    for part in range(1, chips // 4):
+        held = jnp.where(chip // 4 == part, mine[part], held)
+    close = [[8 * part + 2 * z + c for z in range(4)] for part in range(chips // 4) for c in range(2)]
+    received = lax.all_gather(held, "tp", axis_index_groups=close)
+    received = lax.dynamic_index_in_dim(received, line // 2 * 2 % 4, 0, keepdims=False)
+    return lax.dynamic_slice_in_dim(received, chip % 4 * HEAD, HEAD, 1)
 
 
 def solution(mesh):

time: 465 us -> 460 us (0.989)
  the two profiles are of different devices: /device:TPU:16 before, /device:TPU:18 now
where the time goes in v5:
time: 460 us; the launch traced here: 451 us
  blocking collectives  224 us (49%)
  waiting for transfers between devices  180 us (39%)
  Pallas kernels  16.3 us (4%)
  between operations  14.3 us (3%)
  starting transfers between devices  7.27 us (2%)
  local copies, waits for them, and re-layouts  7.04 us (2%)
    all_gather x18, blocking collectives, shards(): got = lax.all_gather(current, ('pp', 'tp'), axis_index_groups=groups(slot))  172 us
    all_gather x1, waiting for transfers between devices, shards(): weights = lax.all_gather(local, 'tp', axis_index_groups=same_core)  140 us
    ppermute x10, waiting for transfers between devices, between(): return lax.ppermute(array, ('pp', 'tp'), moves)  40.4 us
    all_gather x1, blocking collectives, shards(): lax.all_gather(jnp.concatenate([entry_stream_rows, parts, padding]), 'tp'...  38.9 us
    all_gather x1, blocking collectives, shards(): received = lax.all_gather(held, 'tp', axis_index_groups=close)  13.6 us
    pallas_call x18, Pallas kernels, section(): pl.pallas_call(functools.partial(section_kernel, slot), out_shape=(jax.Sh...  10.3 us
  transfers between devices with their start and end apart: 11, of which 2 were waited for; matrix products, arithmetic and copies ran while one was open for 1% of the time, Pallas kernels for 1%

profile of v5, /device:TPU:18, one launch (start us, length us, event | category | flops | bytes accessed | tf_op | source)
XLA Modules:
  0.0 451.4 jit_solution(7314479353287911046)
XLA Ops:
  6.5 1.3 pad_maximum_fusion
  7.9 1.3 copy.91
  9.2 0.7 pad_maximum_fusion.1
  10.4 0.8 copy.83
  11.3 38.9 %all-gather.21 = bf16[16,80,64]{1,2,0:T(8,128)(2,1)S(1)} all-gather(bf16[1,80,64]{1,2,0:T(8,128)(2,1)S(1)} %bitcast.57), channel_id=2, replica_groups={{0,2,4,6,8,10,12,14,16,18,20,22,24,26,28,30},{1,3,5,7,9,11,13,15,17,19,..., dimensions={0}, use_global_device_ids=true | all-gather | bytes 174080 | tf_op jit(solution)/shard_map/all_gather | solution.py:236
  50.3 0.7 collective-permute-start.1
  51.0 0.7 collective-permute-start
  51.8 0.2 copy.93
  52.3 0.2 copy.90
  52.6 1.2 broadcast_in_dim.20
  53.8 0.6 reshape.41.spike
  54.5 0.7 tile.12
  55.3 10.0 %all-gather.1 = bf16[256,1024]{1,0:T(8,128)(2,1)S(1)} all-gather(bf16[64,1024]{1,0:T(8,128)(2,1)S(1)} %broadcast_select_fusion.1), channel_id=3, replica_groups={{0,1,2,3},{4,5,6,7},{8,9,10,11},{12,13,14,15},{16,17,18,19},{20,21,22,2..., dimensions={0}, use_global_device_ids=true | all-gather | bytes 655360 | tf_op jit(solution)/shard_map/all_gather | solution.py:275
  65.3 140.0 %all-gather.24.cloned.1.call-done = bf16[32768,256]{1,0:T(8,128)(2,1)} async-done(((bf16[2048,256]{1,0:T(8,128)(2,1)}), bf16[32768,256]{1,0:T(8,128)(2,1)}) %all-gather.24.cloned.1.call-update) | async-done | bytes 16777232 | tf_op jit(solution)/shard_map/all_gather | solution.py:223
  205.3 5.9 %shard_map.91.weights = bf16[16,2048,256]{2,1,0:T(8,128)(2,1)S(1)} custom-call(bf16[16,2048,256]{2,1,0:T(8,128)(2,1)} %bitcast.51), custom_call_target="tpu_custom_call" | custom-call | bytes 33554432 | tf_op jit(solution)/shard_map/pallas_call | solution.py:167
  211.4 6.8 %all-gather.3 = bf16[256,1024]{1,0:T(8,128)(2,1)S(1)} all-gather(bf16[64,1024]{1,0:T(8,128)(2,1)S(1)} %get-tuple-element.82), channel_id=5, replica_groups={{0,1,32,33},{2,3,34,35},{4,5,36,37},{6,7,38,39},{8,9,40,41},{10,11,42,4..., dimensions={0}, use_global_device_ids=true | all-gather | bytes 655360 | tf_op jit(solution)/shard_map/all_gather | solution.py:275
  218.2 7.3 %all-gather.4 = bf16[256,1024]{1,0:T(8,128)(2,1)S(1)} all-gather(bf16[64,1024]{1,0:T(8,128)(2,1)S(1)} %broadcast_select_fusion), channel_id=6, replica_groups={{32,33,64,65},{34,35,66,67},{36,37,68,69},{38,39,70,71},{40,41,72,73},{..., dimensions={0}, use_global_device_ids=true | all-gather | bytes 655360 | tf_op jit(solution)/shard_map/all_gather | solution.py:275
  225.4 7.3 %all-gather.5 = bf16[256,1024]{1,0:T(8,128)(2,1)S(1)} all-gather(bf16[64,1024]{1,0:T(8,128)(2,1)S(1)} %get-tuple-element.90), channel_id=7, replica_groups={{64,65,96,97},{66,67,98,99},{68,69,100,101},{70,71,102,103},{72,73,104,..., dimensions={0}, use_global_device_ids=true | all-gather | bytes 655360 | tf_op jit(solution)/shard_map/all_gather | solution.py:275
  232.7 0.4 shard_map.95
  233.2 7.3 %all-gather.6 = bf16[256,1024]{1,0:T(8,128)(2,1)S(1)} all-gather(bf16[64,1024]{1,0:T(8,128)(2,1)S(1)} %get-tuple-element.94), channel_id=8, replica_groups={{96,97,128,129},{98,99,130,131},{100,101,132,133},{102,103,134,135},{10..., dimensions={0}, use_global_device_ids=true | all-gather | bytes 655360 | tf_op jit(solution)/shard_map/all_gather | solution.py:275
  240.4 7.3 %all-gather.7 = bf16[256,1024]{1,0:T(8,128)(2,1)S(1)} all-gather(bf16[64,1024]{1,0:T(8,128)(2,1)S(1)} %get-tuple-element.98), channel_id=9, replica_groups={{128,129,160,161},{130,131,162,163},{132,133,164,165},{134,135,166,167}..., dimensions={0}, use_global_device_ids=true | all-gather | bytes 655360 | tf_op jit(solution)/shard_map/all_gather | solution.py:275
  247.7 7.3 %all-gather.8 = bf16[256,1024]{1,0:T(8,128)(2,1)S(1)} all-gather(bf16[64,1024]{1,0:T(8,128)(2,1)S(1)} %get-tuple-element.102), channel_id=10, replica_groups={{160,161,192,193},{162,163,194,195},{164,165,196,197},{166,167,198,199}..., dimensions={0}, use_global_device_ids=true | all-gather | bytes 655360 | tf_op jit(solution)/shard_map/all_gather | solution.py:275
  255.0 7.3 %all-gather.9 = bf16[256,1024]{1,0:T(8,128)(2,1)S(1)} all-gather(bf16[64,1024]{1,0:T(8,128)(2,1)S(1)} %get-tuple-element.106), channel_id=11, replica_groups={{192,193,224,225},{194,195,226,227},{196,197,228,229},{198,199,230,231}..., dimensions={0}, use_global_device_ids=true | all-gather | bytes 655360 | tf_op jit(solution)/shard_map/all_gather | solution.py:275
  262.4 7.3 %all-gather.10 = bf16[256,1024]{1,0:T(8,128)(2,1)S(1)} all-gather(bf16[64,1024]{1,0:T(8,128)(2,1)S(1)} %get-tuple-element.110), channel_id=12, replica_groups={{224,225,256,257},{226,227,258,259},{228,229,260,261},{230,231,262,263}..., dimensions={0}, use_global_device_ids=true | all-gather | bytes 655360 | tf_op jit(solution)/shard_map/all_gather | solution.py:275
  269.7 43.6 %all-gather.11 = bf16[256,1024]{1,0:T(8,128)(2,1)S(1)} all-gather(bf16[64,1024]{1,0:T(8,128)(2,1)S(1)} %get-tuple-element.114), channel_id=13, replica_groups={{256,257,288,289},{258,259,290,291},{260,261,292,293},{262,263,294,295}..., dimensions={0}, use_global_device_ids=true | all-gather | bytes 655360 | tf_op jit(solution)/shard_map/all_gather | solution.py:275
  313.3 4.5 shard_map.101
  317.8 7.3 %all-gather.12 = bf16[256,1024]{1,0:T(8,128)(2,1)S(1)} all-gather(bf16[64,1024]{1,0:T(8,128)(2,1)S(1)} %get-tuple-element.118), channel_id=14, replica_groups={{288,289,320,321},{290,291,322,323},{292,293,324,325},{294,295,326,327}..., dimensions={0}, use_global_device_ids=true | all-gather | bytes 655360 | tf_op jit(solution)/shard_map/all_gather | solution.py:275
  325.1 0.3 shard_map.102
  325.4 9.4 %all-gather.13 = bf16[256,1024]{1,0:T(8,128)(2,1)S(1)} all-gather(bf16[64,1024]{1,0:T(8,128)(2,1)S(1)} %get-tuple-element.122), channel_id=15, replica_groups={{320,321,352,353},{322,323,354,355},{324,325,356,357},{326,327,358,359}..., dimensions={0}, use_global_device_ids=true | all-gather | bytes 655360 | tf_op jit(solution)/shard_map/all_gather | solution.py:275
  334.8 4.7 %shard_map.103 = (bf16[64,1024]{1,0:T(8,128)(2,1)S(1)}, f32[8,128,128]{2,1,0:T(8,128)S(1)}, bf16[8,64,128]{2,1,0:T(8,128)(2,1)S(1)}, bf16[8,64,128]{2,1,0:T(8,128)(2,1)S(1)}) custom-call(bf16[4,64,1024]{2,1,0:T(8,128)(2,1)S(1)} %bitcast.46, f32[1,2048]{1,0:T(1,128)S(1)} %copy-done, ...), custom_call_target="tpu_custom_call", output_to_operand_aliasing={{1}: (6, {}), {2}: (7, {}), {3}: (8, {})} | custom-call | flops 1073741824 | bytes 16777216 | tf_op jit(solution)/shard_map/pallas_call | solution.py:180
  339.4 7.3 %all-gather.14 = bf16[256,1024]{1,0:T(8,128)(2,1)S(1)} all-gather(bf16[64,1024]{1,0:T(8,128)(2,1)S(1)} %get-tuple-element.126), channel_id=16, replica_groups={{352,353,384,385},{354,355,386,387},{356,357,388,389},{358,359,390,391}..., dimensions={0}, use_global_device_ids=true | all-gather | bytes 655360 | tf_op jit(solution)/shard_map/all_gather | solution.py:275
  346.7 7.3 %all-gather.15 = bf16[256,1024]{1,0:T(8,128)(2,1)S(1)} all-gather(bf16[64,1024]{1,0:T(8,128)(2,1)S(1)} %get-tuple-element.130), channel_id=17, replica_groups={{384,385,416,417},{386,387,418,419},{388,389,420,421},{390,391,422,423}..., dimensions={0}, use_global_device_ids=true | all-gather | bytes 655360 | tf_op jit(solution)/shard_map/all_gather | solution.py:275
  354.0 7.3 %all-gather.16 = bf16[256,1024]{1,0:T(8,128)(2,1)S(1)} all-gather(bf16[64,1024]{1,0:T(8,128)(2,1)S(1)} %get-tuple-element.134), channel_id=18, replica_groups={{416,417,448,449},{418,419,450,451},{420,421,452,453},{422,423,454,455}..., dimensions={0}, use_global_device_ids=true | all-gather | bytes 655360 | tf_op jit(solution)/shard_map/all_gather | solution.py:275
  361.2 7.3 %all-gather.17 = bf16[256,1024]{1,0:T(8,128)(2,1)S(1)} all-gather(bf16[64,1024]{1,0:T(8,128)(2,1)S(1)} %get-tuple-element.138), channel_id=19, replica_groups={{448,449,480,481},{450,451,482,483},{452,453,484,485},{454,455,486,487}..., dimensions={0}, use_global_device_ids=true | all-gather | bytes 655360 | tf_op jit(solution)/shard_map/all_gather | solution.py:275
  368.5 0.2 shard_map.107
  368.8 7.3 %all-gather.18 = bf16[256,1024]{1,0:T(8,128)(2,1)S(1)} all-gather(bf16[64,1024]{1,0:T(8,128)(2,1)S(1)} %get-tuple-element.142), channel_id=20, replica_groups={{416,417,448,449},{418,419,450,451},{420,421,452,453},{422,423,454,455}..., dimensions={0}, use_global_device_ids=true | all-gather | bytes 655360 | tf_op jit(solution)/shard_map/all_gather | solution.py:275
  376.0 0.7 collective-permute-start.2
  376.7 0.7 collective-permute-start.3
  377.4 0.7 collective-permute-start.4
  378.1 0.7 collective-permute-start.5
  378.8 7.3 %all-gather.19 = bf16[256,1024]{1,0:T(8,128)(2,1)S(1)} all-gather(bf16[64,1024]{1,0:T(8,128)(2,1)S(1)} %get-tuple-element.146), channel_id=21, replica_groups={{448,449,480,481},{450,451,482,483},{452,453,484,485},{454,455,486,487}..., dimensions={0}, use_global_device_ids=true | all-gather | bytes 655360 | tf_op jit(solution)/shard_map/all_gather | solution.py:275
  386.1 0.7 collective-permute-start.6
  386.8 0.7 collective-permute-start.7
  387.5 0.7 collective-permute-start.8
  388.1 1.3 collective-permute-start.9
  389.6 40.3 %collective-permute-done.9 = bf16[64,256]{1,0:T(8,128)(2,1)S(1)} collective-permute-done((bf16[64,256]{1,0:T(8,128)(2,1)S(1)}, bf16[64,256]{1,0:T(8,128)(2,1)S(1)}, u32[]{:S(2)}, u32[]{:S(2)}) %collective-permute-start.9) | collective-permute-done | bytes 32800 | tf_op jit(solution)/shard_map/ppermute | solution.py:251
  429.9 13.6 %all-gather.20 = bf16[256,256]{1,0:T(8,128)(2,1)S(1)} all-gather(bf16[64,256]{1,0:T(8,128)(2,1)S(1)} %select_select_fusion), channel_id=22, replica_groups={{0,2,4,6},{1,3,5,7},{8,10,12,14},{9,11,13,15},{16,18,20,22},{17,19,21,2..., dimensions={0}, use_global_device_ids=true | all-gather | bytes 163840 | tf_op jit(solution)/shard_map/all_gather | solution.py:295
  443.5 0.7 dynamic-slice_bitcast_fusion
  (51 shorter events, 1.7 us)
Async XLA Ops:
  6.5 198.8 %all-gather.24.cloned.1.call-start = ((), (), s32[]{:S(2)}) async-start(), calls=%async_computation | async-start | bytes 17825792 | tf_op jit(solution)/shard_map/all_gather | solution.py:223
  50.3 4.9 %collective-permute-start.1 = (bf16[64,1024]{1,0:T(8,128)(2,1)S(1)}, bf16[64,1024]{1,0:T(8,128)(2,1)S(1)}, u32[]{:S(2)}, u32[]{:S(2)}) collective-permute-start(bf16[64,1024]{1,0:T(8,128)(2,1)S(1)} %copy.92), channel_id=1, source_target_pairs={{0,0},{1,1},{68,4},{69,5},{136,8},{137,9},{204,12},{205,13},{272,1... | collective-permute-start | bytes 393224 | tf_op jit(solution)/shard_map/ppermute | solution.py:251
  51.0 167.1 %collective-permute-start = (bf16[64,1024]{1,0:T(8,128)(2,1)S(1)}, bf16[64,1024]{1,0:T(8,128)(2,1)S(1)}, u32[]{:S(2)}, u32[]{:S(2)}) collective-permute-start(bf16[64,1024]{1,0:T(8,128)(2,1)S(1)} %copy.92), channel_id=1, source_target_pairs={{32,0},{33,1},{100,4},{101,5},{168,8},{169,9},{236,12},{237,13},{3... | collective-permute-start | bytes 393224 | tf_op jit(solution)/shard_map/ppermute | solution.py:251
  205.3 6.0 %copy-start = (f32[1,2048]{1,0:T(1,128)S(1)}, f32[1,2048]{1,0:T(1,128)}, u32[]{:S(2)}) copy-start(f32[1,2048]{1,0:T(1,128)} %gain.17) | copy-start | bytes 24580
  376.0 10.0 %collective-permute-start.2 = (bf16[64,256]{1,0:T(8,128)(2,1)S(1)}, bf16[64,256]{1,0:T(8,128)(2,1)S(1)}, u32[]{:S(2)}, u32[]{:S(2)}) collective-permute-start(bf16[64,256]{1,0:T(8,128)(2,1)S(1)} %get-tuple-element.155), channel_id=1, source_target_pairs={{480,24},{481,25},{484,92},{485,93},{488,152},{489,153},{492,220},... | collective-permute-start | bytes 98312 | tf_op jit(solution)/shard_map/ppermute | solution.py:251
  376.7 9.3 %collective-permute-start.3 = (bf16[64,256]{1,0:T(8,128)(2,1)S(1)}, bf16[64,256]{1,0:T(8,128)(2,1)S(1)}, u32[]{:S(2)}, u32[]{:S(2)}) collective-permute-start(bf16[64,256]{1,0:T(8,128)(2,1)S(1)} %get-tuple-element.158), channel_id=1, source_target_pairs={{480,0},{481,1},{484,68},{485,69},{488,128},{489,129},{492,196},{4... | collective-permute-start | bytes 98312 | tf_op jit(solution)/shard_map/ppermute | solution.py:251
  377.4 8.7 %collective-permute-start.4 = (bf16[64,256]{1,0:T(8,128)(2,1)S(1)}, bf16[64,256]{1,0:T(8,128)(2,1)S(1)}, u32[]{:S(2)}, u32[]{:S(2)}) collective-permute-start(bf16[64,256]{1,0:T(8,128)(2,1)S(1)} %get-tuple-element.157), channel_id=1, source_target_pairs={{480,8},{481,9},{484,76},{485,77},{488,136},{489,137},{492,204},{4... | collective-permute-start | bytes 98312 | tf_op jit(solution)/shard_map/ppermute | solution.py:251
  378.1 8.0 %collective-permute-start.5 = (bf16[64,256]{1,0:T(8,128)(2,1)S(1)}, bf16[64,256]{1,0:T(8,128)(2,1)S(1)}, u32[]{:S(2)}, u32[]{:S(2)}) collective-permute-start(bf16[64,256]{1,0:T(8,128)(2,1)S(1)} %get-tuple-element.156), channel_id=1, source_target_pairs={{480,16},{481,17},{484,84},{485,85},{488,144},{489,145},{492,212},... | collective-permute-start | bytes 98312 | tf_op jit(solution)/shard_map/ppermute | solution.py:251
  386.1 3.4 collective-permute-start.6
  386.8 2.7 collective-permute-start.7
  387.5 2.1 collective-permute-start.8
  388.1 41.8 %collective-permute-start.9 = (bf16[64,256]{1,0:T(8,128)(2,1)S(1)}, bf16[64,256]{1,0:T(8,128)(2,1)S(1)}, u32[]{:S(2)}, u32[]{:S(2)}) collective-permute-start(bf16[64,256]{1,0:T(8,128)(2,1)S(1)} %get-tuple-element.152), channel_id=1, source_target_pairs={{480,32},{481,33},{484,100},{485,101},{488,160},{489,161},{492,228... | collective-permute-start | bytes 98312 | tf_op jit(solution)/shard_map/ppermute | solution.py:251
Sparse Core Ops, SparseCore 0:
  9.4 195.8 all-gather.23

commit v6 on v5

--- a/solution.py
+++ b/solution.py
@@ -29,11 +29,28 @@
     values_in,
     *others,
 ):
-    result, state, last_keys, last_values, scaled, product = others[-6:]
+    if slot == 0:
+        source = weights
+        result, weights, state, last_keys, last_values, scaled, product, semaphores = others
+    else:
+        result, state, last_keys, last_values, scaled, product = others[-6:]
     line = lax.axis_index("pp")
     core = lax.axis_index("tp") % 2
     first = (line == slot).astype(jnp.int32)
     pairs = weights.shape[0] // 2
+
+    def ready(head):
+        if slot == 0:
+            pltpu.make_async_copy(source.at[head], weights.at[head], semaphores.at[head]).wait()
+
+    if slot == 0:
+        for head in range(2 * pairs):
+            pltpu.make_async_copy(source.at[head], weights.at[head], semaphores.at[head]).start()
+
+        @pl.when(line != 0)
+        def _():
+            for head in range(2 * pairs):
+                ready(head)
 
     @pl.when(line == slot - 1)
     def _():
@@ -46,12 +63,40 @@
     @pl.when((line == slot) | (line == slot - 2))
     def _():
         run_section(
-            first, core, got, gain, weights, edge, spike, out_gain, result, state, last_keys, last_values, scaled, product
+            first,
+            core,
+            got,
+            gain,
+            weights,
+            edge,
+            spike,
+            out_gain,
+            result,
+            state,
+            last_keys,
+            last_values,
+            scaled,
+            product,
+            ready,
         )
 
 
 def run_section(
-    first, core, got, gain, weights, edge, spike, out_gain, result, state, last_keys, last_values, scaled, product
+    first,
+    core,
+    got,
+    gain,
+    weights,
+    edge,
+    spike,
+    out_gain,
+    result,
+    state,
+    last_keys,
+    last_values,
+    scaled,
+    product,
+    ready,
 ):
     rows, width = got.shape[1:]
     heads = weights.shape[0]
@@ -83,6 +128,7 @@
     mean = jnp.where(same, 1.0 / HEAD, 0.0).astype(jnp.bfloat16)
 
     def multiply(head, _):
+        ready(head)
         product[head] = lax.dot_general(scaled[...], weights[head], NN, preferred_element_type=jnp.float32)
         return 0
 
@@ -153,48 +199,34 @@
     lax.fori_loop(0, heads // 2 // ABREAST, several, 0)
 
 
-def hold_kernel(source, held, semaphores):
-    copies = [
-        pltpu.make_async_copy(source.at[head], held.at[head], semaphores.at[head]) for head in range(source.shape[0])
-    ]
-    for copy in copies:
-        copy.start()
-    for copy in copies:
-        copy.wait()
-
-
-def hold(weights):
-    return pl.pallas_call(
-        hold_kernel,
-        out_shape=pltpu.VMEM(weights.shape, weights.dtype),
-        in_specs=[pl.BlockSpec(memory_space=pltpu.HBM)],
-        out_specs=pl.BlockSpec(memory_space=pltpu.VMEM),
-        scratch_shapes=[pltpu.SemaphoreType.DMA((weights.shape[0],))],
-        compiler_params=pltpu.CompilerParams(vmem_limit_bytes=1 << 20),
-        cost_estimate=pl.CostEstimate(flops=0, bytes_accessed=4 * weights.size, transcendentals=0),
-    )(weights)
-
-
 def section(slot, got, gain, weights, edge, spike, out_gain, kept, after):
     rows, width = got.shape[1:]
-    return pl.pallas_call(
+    everything = [pl.BlockSpec(memory_space=pltpu.VMEM)]
+    outputs = [jax.ShapeDtypeStruct((rows, width), jnp.bfloat16)]
+    scratch = [
+        pltpu.VMEM((rows, 2 * width), jnp.bfloat16),
+        pltpu.VMEM((weights.shape[0], rows, weights.shape[2]), jnp.float32),
+    ]
+    source = everything
+    if slot == 0:
+        source = [pl.BlockSpec(memory_space=pltpu.HBM)]
+        weights = pltpu.with_memory_space_constraint(weights, pltpu.HBM)
+        outputs.append(pltpu.VMEM(weights.shape, weights.dtype))
+        scratch.append(pltpu.SemaphoreType.DMA((weights.shape[0],)))
+    results = pl.pallas_call(
         functools.partial(section_kernel, slot),
-        out_shape=(
-            jax.ShapeDtypeStruct((rows, width), jnp.bfloat16),
-        )
-        + tuple(jax.ShapeDtypeStruct(array.shape, array.dtype) for array in kept),
-        in_specs=[pl.BlockSpec(memory_space=pltpu.VMEM)] * (9 + len(after)),
-        out_specs=[pl.BlockSpec(memory_space=pltpu.VMEM)] * 4,
-        scratch_shapes=[
-            pltpu.VMEM((rows, 2 * width), jnp.bfloat16),
-            pltpu.VMEM((weights.shape[0], rows, weights.shape[2]), jnp.float32),
-        ],
-        input_output_aliases={6: 1, 7: 2, 8: 3},
+        out_shape=outputs + [jax.ShapeDtypeStruct(array.shape, array.dtype) for array in kept],
+        in_specs=everything * 2 + source + everything * (6 + len(after)),
+        out_specs=everything * (len(outputs) + 3),
+        scratch_shapes=scratch,
+        input_output_aliases={6 + index: len(outputs) + index for index in range(3)},
         compiler_params=pltpu.CompilerParams(vmem_limit_bytes=24 << 20),
         cost_estimate=pl.CostEstimate(
             flops=2 * rows * weights.size, bytes_accessed=2 * weights.size, transcendentals=0
         ),
     )(got, gain, weights, edge, spike, out_gain, *kept, *after)
+    held = results[1] if slot == 0 else weights
+    return results[0], held, results[-3:]
 
 
 def shards(
@@ -221,7 +253,6 @@
     )
     local = local.reshape(4 * HEAD, 2 * half_width).T
     weights = lax.all_gather(local, "tp", axis_index_groups=same_core)
-    weights = hold(pltpu.with_memory_space_constraint(weights, pltpu.HBM))
     gain = layer_rescale_factor
     out_gain = jnp.tile(per_group_scale, (1, 2))
     rest = jnp.concatenate([retention_minimum[0], decay_spike[0, :, 0]])
@@ -274,7 +305,7 @@
             current = jnp.where(line == 0, entry[slot // 2], current)
         got = lax.all_gather(current, ("pp", "tp"), axis_index_groups=groups(slot))
         after = finished[0] if slot == sections + 1 else ()
-        current, *kept = section(slot, got, gain, weights, edge, spike, out_gain, kept, after)
+        current, weights, kept = section(slot, got, gain, weights, edge, spike, out_gain, kept, after)
         if slot in (sections - 1, sections + 1):
             unit = len(finished)
             finished.append(
@@ -291,10 +322,22 @@
     held = mine[0]
     for part in range(1, chips // 4):
         held = jnp.where(chip // 4 == part, mine[part], held)
-    close = [[8 * part + 2 * z + c for z in range(4)] for part in range(chips // 4) for c in range(2)]
-    received = lax.all_gather(held, "tp", axis_index_groups=close)
-    received = lax.dynamic_index_in_dim(received, line // 2 * 2 % 4, 0, keepdims=False)
-    return lax.dynamic_slice_in_dim(received, chip % 4 * HEAD, HEAD, 1)
+    origin = line // 2 * 2 % 4
+
+    def chunk(index):
+        return lax.dynamic_slice_in_dim(held, index * HEAD, HEAD, 1)
+
+    out = jnp.where(chip % 4 == origin, chunk(origin), 0)
+    for flip in range(1, 4):
+        moves = [
+            (l * members + 8 * part + 2 * at + c, l * members + 8 * part + 2 * (at ^ flip) + c)
+            for l in range(sections)
+            for at in [l // 2 * 2 % 4]
+            for part in range(chips // 4)
+            for c in range(2)
+        ]
+        out = out + lax.ppermute(chunk(origin ^ flip), ("pp", "tp"), moves)
+    return out
 
 
 def solution(mesh):

time: 460 us -> 452 us (0.983)
  the two profiles are of different devices: /device:TPU:18 before, /device:TPU:30 now
where the time goes in v6:
time: 452 us; the launch traced here: 443 us
  blocking collectives  231 us (51%)
  waiting for transfers between devices  157 us (35%)
  Pallas kernels  16.2 us (4%)
  starting transfers between devices  14.3 us (3%)
  between operations  14.3 us (3%)
  local copies, waits for them, and re-layouts  7.13 us (2%)
    all_gather x18, blocking collectives, shards(): got = lax.all_gather(current, ('pp', 'tp'), axis_index_groups=groups(slot))  192 us
    all_gather x1, waiting for transfers between devices, shards(): weights = lax.all_gather(local, 'tp', axis_index_groups=same_core)  140 us
    all_gather x1, blocking collectives, shards(): lax.all_gather(jnp.concatenate([entry_stream_rows, parts, padding]), 'tp'...  39 us
    pallas_call x18, Pallas kernels, section(): pl.pallas_call(functools.partial(section_kernel, slot), out_shape=outputs...  16.2 us
    ppermute x3, waiting for transfers between devices, shards(): out = out + lax.ppermute(chunk(origin ^ flip), ('pp', 'tp'), moves)  16.1 us
    ppermute x10, starting transfers between devices, between(): return lax.ppermute(array, ('pp', 'tp'), moves)  11.7 us
  transfers between devices with their start and end apart: 14, of which 4 were waited for; matrix products, arithmetic and copies ran while one was open for 1% of the time, Pallas kernels for 1%

profile of v6, /device:TPU:30, one launch (start us, length us, event | category | flops | bytes accessed | tf_op | source)
XLA Modules:
  0.0 443.1 jit_solution(8730256767695654407)
XLA Ops:
  6.5 1.3 pad_maximum_fusion
  7.9 1.3 copy.91
  9.2 0.7 pad_maximum_fusion.1
  10.4 0.8 copy.83
  11.3 39.0 %all-gather.20 = bf16[16,80,64]{1,2,0:T(8,128)(2,1)S(1)} all-gather(bf16[1,80,64]{1,2,0:T(8,128)(2,1)S(1)} %bitcast.53), channel_id=2, replica_groups={{0,2,4,6,8,10,12,14,16,18,20,22,24,26,28,30},{1,3,5,7,9,11,13,15,17,19,..., dimensions={0}, use_global_device_ids=true | all-gather | bytes 174080 | tf_op jit(solution)/shard_map/all_gather | solution.py:267
  50.4 0.7 collective-permute-start.1
  51.1 0.7 collective-permute-start
  52.7 1.2 broadcast_in_dim.24
  53.9 0.6 reshape.40.spike
  54.6 0.7 tile.12
  55.3 10.0 %all-gather.1 = bf16[256,1024]{1,0:T(8,128)(2,1)S(1)} all-gather(bf16[64,1024]{1,0:T(8,128)(2,1)S(1)} %broadcast_select_fusion.1), channel_id=3, replica_groups={{0,1,2,3},{4,5,6,7},{8,9,10,11},{12,13,14,15},{16,17,18,19},{20,21,22,2..., dimensions={0}, use_global_device_ids=true | all-gather | bytes 655360 | tf_op jit(solution)/shard_map/all_gather | solution.py:306
  65.4 139.9 %all-gather.23.cloned.1.call-done = bf16[32768,256]{1,0:T(8,128)(2,1)} async-done(((bf16[2048,256]{1,0:T(8,128)(2,1)}), bf16[32768,256]{1,0:T(8,128)(2,1)}) %all-gather.23.cloned.1.call-update) | async-done | bytes 16777232 | tf_op jit(solution)/shard_map/all_gather | solution.py:255
  205.4 0.7 copy-done
  206.0 5.9 %shard_map.91 = (bf16[64,1024]{1,0:T(8,128)(2,1)S(1)}, bf16[16,2048,256]{2,1,0:T(8,128)(2,1)S(1)}, f32[8,128,128]{2,1,0:T(8,128)S(1)}, bf16[8,64,128]{2,1,0:T(8,128)(2,1)S(1)}, bf16[8,64,128]{2,1,0:T(8,128)(2,1)S(1)}) custom-call(bf16[4,64,1024]{2,1,0:T(8,128)(2,1)S(1)} %bitcast.32, ...), custom_call_target="tpu_custom_call", output_to_operand_aliasing={{2}: (6, {}), {3}: (7, {}), {4}: (8, {})} | custom-call | flops 1073741824 | bytes 16777216 | tf_op jit(solution)/shard_map/pallas_call | solution.py:216
  212.0 6.8 %all-gather.3 = bf16[256,1024]{1,0:T(8,128)(2,1)S(1)} all-gather(bf16[64,1024]{1,0:T(8,128)(2,1)S(1)} %get-tuple-element.83), channel_id=5, replica_groups={{0,1,32,33},{2,3,34,35},{4,5,36,37},{6,7,38,39},{8,9,40,41},{10,11,42,4..., dimensions={0}, use_global_device_ids=true | all-gather | bytes 655360 | tf_op jit(solution)/shard_map/all_gather | solution.py:306
  218.8 7.3 %all-gather.4 = bf16[256,1024]{1,0:T(8,128)(2,1)S(1)} all-gather(bf16[64,1024]{1,0:T(8,128)(2,1)S(1)} %broadcast_select_fusion), channel_id=6, replica_groups={{32,33,64,65},{34,35,66,67},{36,37,68,69},{38,39,70,71},{40,41,72,73},{..., dimensions={0}, use_global_device_ids=true | all-gather | bytes 655360 | tf_op jit(solution)/shard_map/all_gather | solution.py:306
  226.1 7.3 %all-gather.5 = bf16[256,1024]{1,0:T(8,128)(2,1)S(1)} all-gather(bf16[64,1024]{1,0:T(8,128)(2,1)S(1)} %get-tuple-element.92), channel_id=7, replica_groups={{64,65,96,97},{66,67,98,99},{68,69,100,101},{70,71,102,103},{72,73,104,..., dimensions={0}, use_global_device_ids=true | all-gather | bytes 655360 | tf_op jit(solution)/shard_map/all_gather | solution.py:306
  233.3 0.4 shard_map.94
  233.8 7.3 %all-gather.6 = bf16[256,1024]{1,0:T(8,128)(2,1)S(1)} all-gather(bf16[64,1024]{1,0:T(8,128)(2,1)S(1)} %get-tuple-element.96), channel_id=8, replica_groups={{96,97,128,129},{98,99,130,131},{100,101,132,133},{102,103,134,135},{10..., dimensions={0}, use_global_device_ids=true | all-gather | bytes 655360 | tf_op jit(solution)/shard_map/all_gather | solution.py:306
  241.1 7.3 %all-gather.7 = bf16[256,1024]{1,0:T(8,128)(2,1)S(1)} all-gather(bf16[64,1024]{1,0:T(8,128)(2,1)S(1)} %get-tuple-element.100), channel_id=9, replica_groups={{128,129,160,161},{130,131,162,163},{132,133,164,165},{134,135,166,167}..., dimensions={0}, use_global_device_ids=true | all-gather | bytes 655360 | tf_op jit(solution)/shard_map/all_gather | solution.py:306
  248.3 7.3 %all-gather.8 = bf16[256,1024]{1,0:T(8,128)(2,1)S(1)} all-gather(bf16[64,1024]{1,0:T(8,128)(2,1)S(1)} %get-tuple-element.104), channel_id=10, replica_groups={{160,161,192,193},{162,163,194,195},{164,165,196,197},{166,167,198,199}..., dimensions={0}, use_global_device_ids=true | all-gather | bytes 655360 | tf_op jit(solution)/shard_map/all_gather | solution.py:306
  255.6 7.3 %all-gather.9 = bf16[256,1024]{1,0:T(8,128)(2,1)S(1)} all-gather(bf16[64,1024]{1,0:T(8,128)(2,1)S(1)} %get-tuple-element.108), channel_id=11, replica_groups={{192,193,224,225},{194,195,226,227},{196,197,228,229},{198,199,230,231}..., dimensions={0}, use_global_device_ids=true | all-gather | bytes 655360 | tf_op jit(solution)/shard_map/all_gather | solution.py:306
  263.0 7.3 %all-gather.10 = bf16[256,1024]{1,0:T(8,128)(2,1)S(1)} all-gather(bf16[64,1024]{1,0:T(8,128)(2,1)S(1)} %get-tuple-element.112), channel_id=12, replica_groups={{224,225,256,257},{226,227,258,259},{228,229,260,261},{230,231,262,263}..., dimensions={0}, use_global_device_ids=true | all-gather | bytes 655360 | tf_op jit(solution)/shard_map/all_gather | solution.py:306
  270.3 7.3 %all-gather.11 = bf16[256,1024]{1,0:T(8,128)(2,1)S(1)} all-gather(bf16[64,1024]{1,0:T(8,128)(2,1)S(1)} %get-tuple-element.116), channel_id=13, replica_groups={{256,257,288,289},{258,259,290,291},{260,261,292,293},{262,263,294,295}..., dimensions={0}, use_global_device_ids=true | all-gather | bytes 655360 | tf_op jit(solution)/shard_map/all_gather | solution.py:306
  277.6 7.3 %all-gather.12 = bf16[256,1024]{1,0:T(8,128)(2,1)S(1)} all-gather(bf16[64,1024]{1,0:T(8,128)(2,1)S(1)} %get-tuple-element.120), channel_id=14, replica_groups={{288,289,320,321},{290,291,322,323},{292,293,324,325},{294,295,326,327}..., dimensions={0}, use_global_device_ids=true | all-gather | bytes 655360 | tf_op jit(solution)/shard_map/all_gather | solution.py:306
  284.8 7.3 %all-gather.13 = bf16[256,1024]{1,0:T(8,128)(2,1)S(1)} all-gather(bf16[64,1024]{1,0:T(8,128)(2,1)S(1)} %get-tuple-element.124), channel_id=15, replica_groups={{320,321,352,353},{322,323,354,355},{324,325,356,357},{326,327,358,359}..., dimensions={0}, use_global_device_ids=true | all-gather | bytes 655360 | tf_op jit(solution)/shard_map/all_gather | solution.py:306
  292.3 7.3 %all-gather.14 = bf16[256,1024]{1,0:T(8,128)(2,1)S(1)} all-gather(bf16[64,1024]{1,0:T(8,128)(2,1)S(1)} %get-tuple-element.128), channel_id=16, replica_groups={{352,353,384,385},{354,355,386,387},{356,357,388,389},{358,359,390,391}..., dimensions={0}, use_global_device_ids=true | all-gather | bytes 655360 | tf_op jit(solution)/shard_map/all_gather | solution.py:306
  299.6 7.3 %all-gather.15 = bf16[256,1024]{1,0:T(8,128)(2,1)S(1)} all-gather(bf16[64,1024]{1,0:T(8,128)(2,1)S(1)} %get-tuple-element.132), channel_id=17, replica_groups={{384,385,416,417},{386,387,418,419},{388,389,420,421},{390,391,422,423}..., dimensions={0}, use_global_device_ids=true | all-gather | bytes 655360 | tf_op jit(solution)/shard_map/all_gather | solution.py:306
  306.9 7.3 %all-gather.16 = bf16[256,1024]{1,0:T(8,128)(2,1)S(1)} all-gather(bf16[64,1024]{1,0:T(8,128)(2,1)S(1)} %get-tuple-element.136), channel_id=18, replica_groups={{416,417,448,449},{418,419,450,451},{420,421,452,453},{422,423,454,455}..., dimensions={0}, use_global_device_ids=true | all-gather | bytes 655360 | tf_op jit(solution)/shard_map/all_gather | solution.py:306
  314.1 66.1 %all-gather.17 = bf16[256,1024]{1,0:T(8,128)(2,1)S(1)} all-gather(bf16[64,1024]{1,0:T(8,128)(2,1)S(1)} %get-tuple-element.140), channel_id=19, replica_groups={{448,449,480,481},{450,451,482,483},{452,453,484,485},{454,455,486,487}..., dimensions={0}, use_global_device_ids=true | all-gather | bytes 655360 | tf_op jit(solution)/shard_map/all_gather | solution.py:306
  380.2 4.7 %shard_map.106 = (bf16[64,1024]{1,0:T(8,128)(2,1)S(1)}, f32[8,128,128]{2,1,0:T(8,128)S(1)}, bf16[8,64,128]{2,1,0:T(8,128)(2,1)S(1)}, bf16[8,64,128]{2,1,0:T(8,128)(2,1)S(1)}) custom-call(bf16[4,64,1024]{2,1,0:T(8,128)(2,1)S(1)} %bitcast.47, f32[1,2048]{1,0:T(1,128)S(1)} %copy-done, ...), custom_call_target="tpu_custom_call", output_to_operand_aliasing={{1}: (6, {}), {2}: (7, {}), {3}: (8, {})} | custom-call | flops 1073741824 | bytes 16777216 | tf_op jit(solution)/shard_map/pallas_call | solution.py:216
  384.9 7.3 %all-gather.18 = bf16[256,1024]{1,0:T(8,128)(2,1)S(1)} all-gather(bf16[64,1024]{1,0:T(8,128)(2,1)S(1)} %get-tuple-element.144), channel_id=20, replica_groups={{416,417,448,449},{418,419,450,451},{420,421,452,453},{422,423,454,455}..., dimensions={0}, use_global_device_ids=true | all-gather | bytes 655360 | tf_op jit(solution)/shard_map/all_gather | solution.py:306
  392.2 1.3 collective-permute-start.2
  393.5 1.3 collective-permute-start.3
  394.8 1.3 collective-permute-start.4
  396.1 1.3 collective-permute-start.5
  397.7 7.3 %all-gather.19 = bf16[256,1024]{1,0:T(8,128)(2,1)S(1)} all-gather(bf16[64,1024]{1,0:T(8,128)(2,1)S(1)} %get-tuple-element.148), channel_id=21, replica_groups={{448,449,480,481},{450,451,482,483},{452,453,484,485},{454,455,486,487}..., dimensions={0}, use_global_device_ids=true | all-gather | bytes 655360 | tf_op jit(solution)/shard_map/all_gather | solution.py:306
  405.0 4.5 %shard_map.108 = (bf16[64,1024]{1,0:T(8,128)(2,1)S(1)}, f32[8,128,128]{2,1,0:T(8,128)S(1)}, bf16[8,64,128]{2,1,0:T(8,128)(2,1)S(1)}, bf16[8,64,128]{2,1,0:T(8,128)(2,1)S(1)}) custom-call(bf16[4,64,1024]{2,1,0:T(8,128)(2,1)S(1)} %bitcast.31, f32[1,2048]{1,0:T(1,128)S(1)} %copy-done, ...), custom_call_target="tpu_custom_call", output_to_operand_aliasing={{1}: (6, {}), {2}: (7, {}), {3}: (8, {})} | custom-call | flops 1073741824 | bytes 16777216 | tf_op jit(solution)/shard_map/pallas_call | solution.py:216
  409.5 1.3 collective-permute-start.6
  410.8 1.3 collective-permute-start.7
  412.1 1.3 collective-permute-start.8
  413.4 1.3 collective-permute-start.9
  415.0 1.3 collective-permute-done.9
  416.4 0.7 collective-permute-start.10
  417.1 1.3 collective-permute-start.11
  418.4 0.7 collective-permute-start.12
  419.1 16.1 %collective-permute-done.11 = bf16[64,64]{1,0:T(8,128)(2,1)S(1)} collective-permute-done((bf16[64,64]{1,0:T(8,128)(2,1)S(1)}, bf16[64,64]{1,0:T(8,128)(2,1)S(1)}, u32[]{:S(2)}, u32[]{:S(2)}) %collective-permute-start.11) | collective-permute-done | bytes 8224 | tf_op jit(solution)/shard_map/ppermute | solution.py:339
  435.2 0.7 add_add_fusion
  (56 shorter events, 2.8 us)
Async XLA Ops:
  6.5 198.7 %all-gather.23.cloned.1.call-start = ((), (), s32[]{:S(2)}) async-start(), calls=%async_computation | async-start | bytes 17825792 | tf_op jit(solution)/shard_map/all_gather | solution.py:255
  50.4 4.9 %collective-permute-start.1 = (bf16[64,1024]{1,0:T(8,128)(2,1)S(1)}, bf16[64,1024]{1,0:T(8,128)(2,1)S(1)}, u32[]{:S(2)}, u32[]{:S(2)}) collective-permute-start(bf16[64,1024]{1,0:T(8,128)(2,1)S(1)} %copy.92), channel_id=1, source_target_pairs={{0,0},{1,1},{68,4},{69,5},{136,8},{137,9},{204,12},{205,13},{272,1... | collective-permute-start | bytes 393224 | tf_op jit(solution)/shard_map/ppermute | solution.py:282
  51.1 167.7 %collective-permute-start = (bf16[64,1024]{1,0:T(8,128)(2,1)S(1)}, bf16[64,1024]{1,0:T(8,128)(2,1)S(1)}, u32[]{:S(2)}, u32[]{:S(2)}) collective-permute-start(bf16[64,1024]{1,0:T(8,128)(2,1)S(1)} %copy.92), channel_id=1, source_target_pairs={{32,0},{33,1},{100,4},{101,5},{168,8},{169,9},{236,12},{237,13},{3... | collective-permute-start | bytes 393224 | tf_op jit(solution)/shard_map/ppermute | solution.py:282
  205.3 0.7 copy-start
  392.2 12.8 %collective-permute-start.2 = (bf16[64,256]{1,0:T(8,128)(2,1)S(1)}, bf16[64,256]{1,0:T(8,128)(2,1)S(1)}, u32[]{:S(2)}, u32[]{:S(2)}) collective-permute-start(bf16[64,256]{1,0:T(8,128)(2,1)S(1)} %get-tuple-element.157), channel_id=1, source_target_pairs={{480,24},{481,25},{484,92},{485,93},{488,152},{489,153},{492,220},... | collective-permute-start | bytes 98312 | tf_op jit(solution)/shard_map/ppermute | solution.py:282
  393.5 11.5 %collective-permute-start.3 = (bf16[64,256]{1,0:T(8,128)(2,1)S(1)}, bf16[64,256]{1,0:T(8,128)(2,1)S(1)}, u32[]{:S(2)}, u32[]{:S(2)}) collective-permute-start(bf16[64,256]{1,0:T(8,128)(2,1)S(1)} %get-tuple-element.160), channel_id=1, source_target_pairs={{480,0},{481,1},{484,68},{485,69},{488,128},{489,129},{492,196},{4... | collective-permute-start | bytes 98312 | tf_op jit(solution)/shard_map/ppermute | solution.py:282
  394.8 10.2 %collective-permute-start.4 = (bf16[64,256]{1,0:T(8,128)(2,1)S(1)}, bf16[64,256]{1,0:T(8,128)(2,1)S(1)}, u32[]{:S(2)}, u32[]{:S(2)}) collective-permute-start(bf16[64,256]{1,0:T(8,128)(2,1)S(1)} %get-tuple-element.159), channel_id=1, source_target_pairs={{480,8},{481,9},{484,76},{485,77},{488,136},{489,137},{492,204},{4... | collective-permute-start | bytes 98312 | tf_op jit(solution)/shard_map/ppermute | solution.py:282
  396.1 8.9 %collective-permute-start.5 = (bf16[64,256]{1,0:T(8,128)(2,1)S(1)}, bf16[64,256]{1,0:T(8,128)(2,1)S(1)}, u32[]{:S(2)}, u32[]{:S(2)}) collective-permute-start(bf16[64,256]{1,0:T(8,128)(2,1)S(1)} %get-tuple-element.158), channel_id=1, source_target_pairs={{480,16},{481,17},{484,84},{485,85},{488,144},{489,145},{492,212},... | collective-permute-start | bytes 98312 | tf_op jit(solution)/shard_map/ppermute | solution.py:282
  409.5 5.3 %collective-permute-start.6 = (bf16[64,256]{1,0:T(8,128)(2,1)S(1)}, bf16[64,256]{1,0:T(8,128)(2,1)S(1)}, u32[]{:S(2)}, u32[]{:S(2)}) collective-permute-start(bf16[64,256]{1,0:T(8,128)(2,1)S(1)} %get-tuple-element.153), channel_id=1, source_target_pairs={{480,56},{481,57},{484,124},{485,125},{488,184},{489,185},{492,252... | collective-permute-start | bytes 98312 | tf_op jit(solution)/shard_map/ppermute | solution.py:282
  410.8 4.0 collective-permute-start.7
  412.1 2.9 collective-permute-start.8
  413.4 2.9 collective-permute-start.9
  416.4 2.7 collective-permute-start.10
  417.1 18.1 %collective-permute-start.11 = (bf16[64,64]{1,0:T(8,128)(2,1)S(1)}, bf16[64,64]{1,0:T(8,128)(2,1)S(1)}, u32[]{:S(2)}, u32[]{:S(2)}) collective-permute-start(bf16[64,64]{1,0:T(8,128)(2,1)S(1)} %get-tuple-element.163), channel_id=1, source_target_pairs={{0,4},{1,5},{8,12},{9,13},{16,20},{17,21},{24,28},{25,29},{32,36},... | collective-permute-start | bytes 24584 | tf_op jit(solution)/shard_map/ppermute | solution.py:339
  418.4 16.8 %collective-permute-start.12 = (bf16[64,64]{1,0:T(8,128)(2,1)S(1)}, bf16[64,64]{1,0:T(8,128)(2,1)S(1)}, u32[]{:S(2)}, u32[]{:S(2)}) collective-permute-start(bf16[64,64]{1,0:T(8,128)(2,1)S(1)} %get-tuple-element.162), channel_id=1, source_target_pairs={{0,6},{1,7},{8,14},{9,15},{16,22},{17,23},{24,30},{25,31},{32,38},... | collective-permute-start | bytes 24584 | tf_op jit(solution)/shard_map/ppermute | solution.py:339
Sparse Core Ops, SparseCore 0:
  9.4 195.7 all-gather.22

commit v7 on v6

--- a/solution.py
+++ b/solution.py
@@ -132,7 +132,8 @@
         product[head] = lax.dot_general(scaled[...], weights[head], NN, preferred_element_type=jnp.float32)
         return 0
 
-    lax.fori_loop(0, heads, multiply, 0, unroll=8)
+    for head in range(heads):
+        multiply(head, 0)
 
     def several(index, _):
         pairs = [ABREAST * index + step for step in range(ABREAST)]
@@ -196,7 +197,8 @@
             result[:, columns] = (own + mixes[step] * inverse * gates[step]).astype(jnp.bfloat16)
         return 0
 
-    lax.fori_loop(0, heads // 2 // ABREAST, several, 0)
+    for index in range(heads // 2 // ABREAST):
+        several(index, 0)
 
 
 def section(slot, got, gain, weights, edge, spike, out_gain, kept, after):

time: 452 us -> 445 us (0.985)
  blocking collectives: 231 us -> 225 us
    all_gather x18, blocking collectives: 192 us -> 186 us  [shards(): got = lax.all_gather(current, ('pp', 'tp'), axis_index_groups=groups(slot))]
where the time goes in v7:
time: 445 us; the launch traced here: 437 us
  blocking collectives  225 us (51%)
  waiting for transfers between devices  157 us (35%)
  Pallas kernels  15.8 us (4%)
  between operations  14.4 us (3%)
  starting transfers between devices  14.3 us (3%)
  local copies, waits for them, and re-layouts  7.13 us (2%)
    all_gather x18, blocking collectives, shards(): got = lax.all_gather(current, ('pp', 'tp'), axis_index_groups=groups(slot))  186 us
    all_gather x1, waiting for transfers between devices, shards(): weights = lax.all_gather(local, 'tp', axis_index_groups=same_core)  140 us
    all_gather x1, blocking collectives, shards(): lax.all_gather(jnp.concatenate([entry_stream_rows, parts, padding]), 'tp'...  39 us
    ppermute x3, waiting for transfers between devices, shards(): out = out + lax.ppermute(chunk(origin ^ flip), ('pp', 'tp'), moves)  16.1 us
    pallas_call x18, Pallas kernels, section(): pl.pallas_call(functools.partial(section_kernel, slot), out_shape=outputs...  15.8 us
    ppermute x10, starting transfers between devices, between(): return lax.ppermute(array, ('pp', 'tp'), moves)  11.7 us
  transfers between devices with their start and end apart: 14, of which 4 were waited for; matrix products, arithmetic and copies ran while one was open for 1% of the time, Pallas kernels for 1%

profile of v7, /device:TPU:30, one launch (start us, length us, event | category | flops | bytes accessed | tf_op | source)
XLA Modules:
  0.0 436.6 jit_solution(14984198717792178210)
XLA Ops:
  6.5 1.3 pad_maximum_fusion
  7.9 1.3 copy.91
  9.2 0.7 pad_maximum_fusion.1
  10.4 0.8 copy.83
  11.3 39.0 %all-gather.20 = bf16[16,80,64]{1,2,0:T(8,128)(2,1)S(1)} all-gather(bf16[1,80,64]{1,2,0:T(8,128)(2,1)S(1)} %bitcast.53), channel_id=2, replica_groups={{0,2,4,6,8,10,12,14,16,18,20,22,24,26,28,30},{1,3,5,7,9,11,13,15,17,19,..., dimensions={0}, use_global_device_ids=true | all-gather | bytes 174080 | tf_op jit(solution)/shard_map/all_gather | solution.py:269
  50.4 0.7 collective-permute-start.1
  51.1 0.7 collective-permute-start
  52.7 1.2 broadcast_in_dim.24
  53.9 0.6 reshape.40.spike
  54.6 0.7 tile.12
  55.3 10.0 %all-gather.1 = bf16[256,1024]{1,0:T(8,128)(2,1)S(1)} all-gather(bf16[64,1024]{1,0:T(8,128)(2,1)S(1)} %broadcast_select_fusion.1), channel_id=3, replica_groups={{0,1,2,3},{4,5,6,7},{8,9,10,11},{12,13,14,15},{16,17,18,19},{20,21,22,2..., dimensions={0}, use_global_device_ids=true | all-gather | bytes 655360 | tf_op jit(solution)/shard_map/all_gather | solution.py:308
  65.4 139.9 %all-gather.23.cloned.1.call-done = bf16[32768,256]{1,0:T(8,128)(2,1)} async-done(((bf16[2048,256]{1,0:T(8,128)(2,1)}), bf16[32768,256]{1,0:T(8,128)(2,1)}) %all-gather.23.cloned.1.call-update) | async-done | bytes 16777232 | tf_op jit(solution)/shard_map/all_gather | solution.py:257
  205.4 0.7 copy-done
  206.0 5.9 %shard_map.91 = (bf16[64,1024]{1,0:T(8,128)(2,1)S(1)}, bf16[16,2048,256]{2,1,0:T(8,128)(2,1)S(1)}, f32[8,128,128]{2,1,0:T(8,128)S(1)}, bf16[8,64,128]{2,1,0:T(8,128)(2,1)S(1)}, bf16[8,64,128]{2,1,0:T(8,128)(2,1)S(1)}) custom-call(bf16[4,64,1024]{2,1,0:T(8,128)(2,1)S(1)} %bitcast.32, ...), custom_call_target="tpu_custom_call", output_to_operand_aliasing={{2}: (6, {}), {3}: (7, {}), {4}: (8, {})} | custom-call | flops 1073741824 | bytes 16777216 | tf_op jit(solution)/shard_map/pallas_call | solution.py:218
  212.0 6.8 %all-gather.3 = bf16[256,1024]{1,0:T(8,128)(2,1)S(1)} all-gather(bf16[64,1024]{1,0:T(8,128)(2,1)S(1)} %get-tuple-element.83), channel_id=5, replica_groups={{0,1,32,33},{2,3,34,35},{4,5,36,37},{6,7,38,39},{8,9,40,41},{10,11,42,4..., dimensions={0}, use_global_device_ids=true | all-gather | bytes 655360 | tf_op jit(solution)/shard_map/all_gather | solution.py:308
  218.8 7.3 %all-gather.4 = bf16[256,1024]{1,0:T(8,128)(2,1)S(1)} all-gather(bf16[64,1024]{1,0:T(8,128)(2,1)S(1)} %broadcast_select_fusion), channel_id=6, replica_groups={{32,33,64,65},{34,35,66,67},{36,37,68,69},{38,39,70,71},{40,41,72,73},{..., dimensions={0}, use_global_device_ids=true | all-gather | bytes 655360 | tf_op jit(solution)/shard_map/all_gather | solution.py:308
  226.3 7.3 %all-gather.5 = bf16[256,1024]{1,0:T(8,128)(2,1)S(1)} all-gather(bf16[64,1024]{1,0:T(8,128)(2,1)S(1)} %get-tuple-element.92), channel_id=7, replica_groups={{64,65,96,97},{66,67,98,99},{68,69,100,101},{70,71,102,103},{72,73,104,..., dimensions={0}, use_global_device_ids=true | all-gather | bytes 655360 | tf_op jit(solution)/shard_map/all_gather | solution.py:308
  233.5 7.3 %all-gather.6 = bf16[256,1024]{1,0:T(8,128)(2,1)S(1)} all-gather(bf16[64,1024]{1,0:T(8,128)(2,1)S(1)} %get-tuple-element.96), channel_id=8, replica_groups={{96,97,128,129},{98,99,130,131},{100,101,132,133},{102,103,134,135},{10..., dimensions={0}, use_global_device_ids=true | all-gather | bytes 655360 | tf_op jit(solution)/shard_map/all_gather | solution.py:308
  240.8 7.3 %all-gather.7 = bf16[256,1024]{1,0:T(8,128)(2,1)S(1)} all-gather(bf16[64,1024]{1,0:T(8,128)(2,1)S(1)} %get-tuple-element.100), channel_id=9, replica_groups={{128,129,160,161},{130,131,162,163},{132,133,164,165},{134,135,166,167}..., dimensions={0}, use_global_device_ids=true | all-gather | bytes 655360 | tf_op jit(solution)/shard_map/all_gather | solution.py:308
  248.1 0.4 shard_map.96
  248.5 7.3 %all-gather.8 = bf16[256,1024]{1,0:T(8,128)(2,1)S(1)} all-gather(bf16[64,1024]{1,0:T(8,128)(2,1)S(1)} %get-tuple-element.104), channel_id=10, replica_groups={{160,161,192,193},{162,163,194,195},{164,165,196,197},{166,167,198,199}..., dimensions={0}, use_global_device_ids=true | all-gather | bytes 655360 | tf_op jit(solution)/shard_map/all_gather | solution.py:308
  255.8 7.3 %all-gather.9 = bf16[256,1024]{1,0:T(8,128)(2,1)S(1)} all-gather(bf16[64,1024]{1,0:T(8,128)(2,1)S(1)} %get-tuple-element.108), channel_id=11, replica_groups={{192,193,224,225},{194,195,226,227},{196,197,228,229},{198,199,230,231}..., dimensions={0}, use_global_device_ids=true | all-gather | bytes 655360 | tf_op jit(solution)/shard_map/all_gather | solution.py:308
  263.0 7.3 %all-gather.10 = bf16[256,1024]{1,0:T(8,128)(2,1)S(1)} all-gather(bf16[64,1024]{1,0:T(8,128)(2,1)S(1)} %get-tuple-element.112), channel_id=12, replica_groups={{224,225,256,257},{226,227,258,259},{228,229,260,261},{230,231,262,263}..., dimensions={0}, use_global_device_ids=true | all-gather | bytes 655360 | tf_op jit(solution)/shard_map/all_gather | solution.py:308
  270.4 7.3 %all-gather.11 = bf16[256,1024]{1,0:T(8,128)(2,1)S(1)} all-gather(bf16[64,1024]{1,0:T(8,128)(2,1)S(1)} %get-tuple-element.116), channel_id=13, replica_groups={{256,257,288,289},{258,259,290,291},{260,261,292,293},{262,263,294,295}..., dimensions={0}, use_global_device_ids=true | all-gather | bytes 655360 | tf_op jit(solution)/shard_map/all_gather | solution.py:308
  277.7 7.3 %all-gather.12 = bf16[256,1024]{1,0:T(8,128)(2,1)S(1)} all-gather(bf16[64,1024]{1,0:T(8,128)(2,1)S(1)} %get-tuple-element.120), channel_id=14, replica_groups={{288,289,320,321},{290,291,322,323},{292,293,324,325},{294,295,326,327}..., dimensions={0}, use_global_device_ids=true | all-gather | bytes 655360 | tf_op jit(solution)/shard_map/all_gather | solution.py:308
  285.0 7.3 %all-gather.13 = bf16[256,1024]{1,0:T(8,128)(2,1)S(1)} all-gather(bf16[64,1024]{1,0:T(8,128)(2,1)S(1)} %get-tuple-element.124), channel_id=15, replica_groups={{320,321,352,353},{322,323,354,355},{324,325,356,357},{326,327,358,359}..., dimensions={0}, use_global_device_ids=true | all-gather | bytes 655360 | tf_op jit(solution)/shard_map/all_gather | solution.py:308
  292.5 7.3 %all-gather.14 = bf16[256,1024]{1,0:T(8,128)(2,1)S(1)} all-gather(bf16[64,1024]{1,0:T(8,128)(2,1)S(1)} %get-tuple-element.128), channel_id=16, replica_groups={{352,353,384,385},{354,355,386,387},{356,357,388,389},{358,359,390,391}..., dimensions={0}, use_global_device_ids=true | all-gather | bytes 655360 | tf_op jit(solution)/shard_map/all_gather | solution.py:308
  299.7 7.3 %all-gather.15 = bf16[256,1024]{1,0:T(8,128)(2,1)S(1)} all-gather(bf16[64,1024]{1,0:T(8,128)(2,1)S(1)} %get-tuple-element.132), channel_id=17, replica_groups={{384,385,416,417},{386,387,418,419},{388,389,420,421},{390,391,422,423}..., dimensions={0}, use_global_device_ids=true | all-gather | bytes 655360 | tf_op jit(solution)/shard_map/all_gather | solution.py:308
  307.0 7.3 %all-gather.16 = bf16[256,1024]{1,0:T(8,128)(2,1)S(1)} all-gather(bf16[64,1024]{1,0:T(8,128)(2,1)S(1)} %get-tuple-element.136), channel_id=18, replica_groups={{416,417,448,449},{418,419,450,451},{420,421,452,453},{422,423,454,455}..., dimensions={0}, use_global_device_ids=true | all-gather | bytes 655360 | tf_op jit(solution)/shard_map/all_gather | solution.py:308
  314.5 59.9 %all-gather.17 = bf16[256,1024]{1,0:T(8,128)(2,1)S(1)} all-gather(bf16[64,1024]{1,0:T(8,128)(2,1)S(1)} %get-tuple-element.140), channel_id=19, replica_groups={{448,449,480,481},{450,451,482,483},{452,453,484,485},{454,455,486,487}..., dimensions={0}, use_global_device_ids=true | all-gather | bytes 655360 | tf_op jit(solution)/shard_map/all_gather | solution.py:308
  374.4 4.1 shard_map.106
  378.4 7.3 %all-gather.18 = bf16[256,1024]{1,0:T(8,128)(2,1)S(1)} all-gather(bf16[64,1024]{1,0:T(8,128)(2,1)S(1)} %get-tuple-element.144), channel_id=20, replica_groups={{416,417,448,449},{418,419,450,451},{420,421,452,453},{422,423,454,455}..., dimensions={0}, use_global_device_ids=true | all-gather | bytes 655360 | tf_op jit(solution)/shard_map/all_gather | solution.py:308
  385.7 1.3 collective-permute-start.2
  387.0 1.3 collective-permute-start.3
  388.3 1.3 collective-permute-start.4
  389.6 1.3 collective-permute-start.5
  391.2 7.3 %all-gather.19 = bf16[256,1024]{1,0:T(8,128)(2,1)S(1)} all-gather(bf16[64,1024]{1,0:T(8,128)(2,1)S(1)} %get-tuple-element.148), channel_id=21, replica_groups={{448,449,480,481},{450,451,482,483},{452,453,484,485},{454,455,486,487}..., dimensions={0}, use_global_device_ids=true | all-gather | bytes 655360 | tf_op jit(solution)/shard_map/all_gather | solution.py:308
  398.5 4.4 %shard_map.108 = (bf16[64,1024]{1,0:T(8,128)(2,1)S(1)}, f32[8,128,128]{2,1,0:T(8,128)S(1)}, bf16[8,64,128]{2,1,0:T(8,128)(2,1)S(1)}, bf16[8,64,128]{2,1,0:T(8,128)(2,1)S(1)}) custom-call(bf16[4,64,1024]{2,1,0:T(8,128)(2,1)S(1)} %bitcast.31, f32[1,2048]{1,0:T(1,128)S(1)} %copy-done, ...), custom_call_target="tpu_custom_call", output_to_operand_aliasing={{1}: (6, {}), {2}: (7, {}), {3}: (8, {})} | custom-call | flops 1073741824 | bytes 16777216 | tf_op jit(solution)/shard_map/pallas_call | solution.py:218
  402.9 1.3 collective-permute-start.6
  404.2 1.3 collective-permute-start.7
  405.5 1.3 collective-permute-start.8
  406.8 1.3 collective-permute-start.9
  408.4 1.3 collective-permute-done.9
  409.8 0.7 collective-permute-start.10
  410.5 1.3 collective-permute-start.11
  411.8 0.7 collective-permute-start.12
  412.5 16.1 %collective-permute-done.11 = bf16[64,64]{1,0:T(8,128)(2,1)S(1)} collective-permute-done((bf16[64,64]{1,0:T(8,128)(2,1)S(1)}, bf16[64,64]{1,0:T(8,128)(2,1)S(1)}, u32[]{:S(2)}, u32[]{:S(2)}) %collective-permute-start.11) | collective-permute-done | bytes 8224 | tf_op jit(solution)/shard_map/ppermute | solution.py:341
  428.6 0.7 add_add_fusion
  (56 shorter events, 3.2 us)
Async XLA Ops:
  6.5 198.7 %all-gather.23.cloned.1.call-start = ((), (), s32[]{:S(2)}) async-start(), calls=%async_computation | async-start | bytes 17825792 | tf_op jit(solution)/shard_map/all_gather | solution.py:257
  50.4 4.9 %collective-permute-start.1 = (bf16[64,1024]{1,0:T(8,128)(2,1)S(1)}, bf16[64,1024]{1,0:T(8,128)(2,1)S(1)}, u32[]{:S(2)}, u32[]{:S(2)}) collective-permute-start(bf16[64,1024]{1,0:T(8,128)(2,1)S(1)} %copy.92), channel_id=1, source_target_pairs={{0,0},{1,1},{68,4},{69,5},{136,8},{137,9},{204,12},{205,13},{272,1... | collective-permute-start | bytes 393224 | tf_op jit(solution)/shard_map/ppermute | solution.py:284
  51.1 167.7 %collective-permute-start = (bf16[64,1024]{1,0:T(8,128)(2,1)S(1)}, bf16[64,1024]{1,0:T(8,128)(2,1)S(1)}, u32[]{:S(2)}, u32[]{:S(2)}) collective-permute-start(bf16[64,1024]{1,0:T(8,128)(2,1)S(1)} %copy.92), channel_id=1, source_target_pairs={{32,0},{33,1},{100,4},{101,5},{168,8},{169,9},{236,12},{237,13},{3... | collective-permute-start | bytes 393224 | tf_op jit(solution)/shard_map/ppermute | solution.py:284
  205.3 0.7 copy-start
  385.7 12.8 %collective-permute-start.2 = (bf16[64,256]{1,0:T(8,128)(2,1)S(1)}, bf16[64,256]{1,0:T(8,128)(2,1)S(1)}, u32[]{:S(2)}, u32[]{:S(2)}) collective-permute-start(bf16[64,256]{1,0:T(8,128)(2,1)S(1)} %get-tuple-element.157), channel_id=1, source_target_pairs={{480,24},{481,25},{484,92},{485,93},{488,152},{489,153},{492,220},... | collective-permute-start | bytes 98312 | tf_op jit(solution)/shard_map/ppermute | solution.py:284
  387.0 11.5 %collective-permute-start.3 = (bf16[64,256]{1,0:T(8,128)(2,1)S(1)}, bf16[64,256]{1,0:T(8,128)(2,1)S(1)}, u32[]{:S(2)}, u32[]{:S(2)}) collective-permute-start(bf16[64,256]{1,0:T(8,128)(2,1)S(1)} %get-tuple-element.160), channel_id=1, source_target_pairs={{480,0},{481,1},{484,68},{485,69},{488,128},{489,129},{492,196},{4... | collective-permute-start | bytes 98312 | tf_op jit(solution)/shard_map/ppermute | solution.py:284
  388.3 10.2 %collective-permute-start.4 = (bf16[64,256]{1,0:T(8,128)(2,1)S(1)}, bf16[64,256]{1,0:T(8,128)(2,1)S(1)}, u32[]{:S(2)}, u32[]{:S(2)}) collective-permute-start(bf16[64,256]{1,0:T(8,128)(2,1)S(1)} %get-tuple-element.159), channel_id=1, source_target_pairs={{480,8},{481,9},{484,76},{485,77},{488,136},{489,137},{492,204},{4... | collective-permute-start | bytes 98312 | tf_op jit(solution)/shard_map/ppermute | solution.py:284
  389.6 8.9 %collective-permute-start.5 = (bf16[64,256]{1,0:T(8,128)(2,1)S(1)}, bf16[64,256]{1,0:T(8,128)(2,1)S(1)}, u32[]{:S(2)}, u32[]{:S(2)}) collective-permute-start(bf16[64,256]{1,0:T(8,128)(2,1)S(1)} %get-tuple-element.158), channel_id=1, source_target_pairs={{480,16},{481,17},{484,84},{485,85},{488,144},{489,145},{492,212},... | collective-permute-start | bytes 98312 | tf_op jit(solution)/shard_map/ppermute | solution.py:284
  402.9 5.3 %collective-permute-start.6 = (bf16[64,256]{1,0:T(8,128)(2,1)S(1)}, bf16[64,256]{1,0:T(8,128)(2,1)S(1)}, u32[]{:S(2)}, u32[]{:S(2)}) collective-permute-start(bf16[64,256]{1,0:T(8,128)(2,1)S(1)} %get-tuple-element.153), channel_id=1, source_target_pairs={{480,56},{481,57},{484,124},{485,125},{488,184},{489,185},{492,252... | collective-permute-start | bytes 98312 | tf_op jit(solution)/shard_map/ppermute | solution.py:284
  404.2 4.0 collective-permute-start.7
  405.5 2.9 collective-permute-start.8
  406.8 2.9 collective-permute-start.9
  409.8 2.7 collective-permute-start.10
  410.5 18.1 %collective-permute-start.11 = (bf16[64,64]{1,0:T(8,128)(2,1)S(1)}, bf16[64,64]{1,0:T(8,128)(2,1)S(1)}, u32[]{:S(2)}, u32[]{:S(2)}) collective-permute-start(bf16[64,64]{1,0:T(8,128)(2,1)S(1)} %get-tuple-element.163), channel_id=1, source_target_pairs={{0,4},{1,5},{8,12},{9,13},{16,20},{17,21},{24,28},{25,29},{32,36},... | collective-permute-start | bytes 24584 | tf_op jit(solution)/shard_map/ppermute | solution.py:341
  411.8 16.8 %collective-permute-start.12 = (bf16[64,64]{1,0:T(8,128)(2,1)S(1)}, bf16[64,64]{1,0:T(8,128)(2,1)S(1)}, u32[]{:S(2)}, u32[]{:S(2)}) collective-permute-start(bf16[64,64]{1,0:T(8,128)(2,1)S(1)} %get-tuple-element.162), channel_id=1, source_target_pairs={{0,6},{1,7},{8,14},{9,15},{16,22},{17,23},{24,30},{25,31},{32,38},... | collective-permute-start | bytes 24584 | tf_op jit(solution)/shard_map/ppermute | solution.py:341
Sparse Core Ops, SparseCore 0:
  9.4 195.7 all-gather.22
